TPU v7x, 128 devices: a whole 4x4x4 slice. The times are simulated.
128 devices in a mesh: ep: 32 (over z, y, core), tp: 4 (over x).
Axes of the slice: x: 4, y: 4, z: 4, core: 2. Of those that a mesh axis runs over, the one named last changes fastest.
Arguments:
- tokens: bfloat16 [1024, 2048], P('ep'), may hold values from -6 to 6
- kv_cache: bfloat16 [1024, 1024, 512], P('ep', None, 'tp'), may hold values from -320 to 320
- lengths: int32 [1024], P('ep'), may hold values from 1 to 1024, 524288 in all
- attn_gain: float32 [2048], replicated, may hold values from 0.1 to 1.9
- w_query: bfloat16 [2048, 1024], P(None, 'tp'), may hold values from -0.125 to 0.125
- w_key: bfloat16 [2048, 256], P(None, 'tp'), may hold values from -0.125 to 0.125
- w_value: bfloat16 [2048, 256], P(None, 'tp'), may hold values from -0.125 to 0.125
- lambdas: float32 [16], P('tp'), may hold values from 0.3 to 0.8
- head_gain: float32 [64], replicated, may hold values from 0.1 to 1.9
- w_out: bfloat16 [1024, 2048], replicated, may hold values from -0.1875 to 0.1875
- ffn_gain: float32 [2048], replicated, may hold values from 0.1 to 1.9
- w_shared_gate: bfloat16 [2048, 512], P(None, 'tp'), may hold values from -0.125 to 0.125
- w_shared_up: bfloat16 [2048, 512], P(None, 'tp'), may hold values from -0.125 to 0.125
- w_shared_down: bfloat16 [512, 2048], P('tp'), may hold values from -0.25 to 0.25
- routing: int32 [1024, 4], replicated, may hold values from 0 to 127, all different within a row; in each aligned block of 32 rows (0 to 31, 32 to 63, ...) at most 2 rows name the same one
- route_weights: float32 [1024, 4], P('ep'), may hold values from 0.1 to 1
- w_exp_gate: bfloat16 [128, 2048, 512], P(('ep', 'tp')), may hold values from -0.125 to 0.125
- w_exp_up: bfloat16 [128, 2048, 512], P(('ep', 'tp')), may hold values from -0.125 to 0.125
- w_exp_down: bfloat16 [128, 512, 2048], P(('ep', 'tp')), may hold values from -0.25 to 0.25
Outputs:
- mixed: bfloat16 [1024, 2048], P('ep', 'tp')
Inputs may be any that keep to these rules, and one draw needn't show every extreme that they name: `lengths`: A sequence's cache holds its past keys and values at positions below its length, and the new token follows them; some sequence uses all 1024 positions. `routing`: each row names 4 different experts. Within the rows of one group of 32 sequences (aligned blocks) no expert is named by more than 2 rows, and in some blocks an expert is named by exactly 2.
All inputs are finite; a program needn't handle non-finite values. No bound on the sum of `lengths` on one device may be relied on, other than what follows from the above.
Results may differ from a plain program's by a relative error of at most 0.015.
The roundings to bfloat16 on the way count: a program that leaves them out, or rounds other values in their place, can miss the bound.
Values may be sent and summed in bfloat16 or wider, within the bound.
No kernel may reach another device: no remote copies, remote signals or barrier semaphores. Data moves between devices by JAX's collectives and lax.ppermute only.
A program may use at most 128 MiB of HBM per device.

v0:
```python
import jax
import jax.numpy as jnp
from jax import lax
from jax.sharding import PartitionSpec as P

epsilon = 1e-06
neg_fill = -1e30


def in_order(tiles, dim):
    tiles = jnp.moveaxis(tiles, 0, dim)
    lengths = tiles.shape
    return tiles.reshape(*lengths[:dim], lengths[dim] * lengths[dim + 1], *lengths[dim + 2 :])


def sent_to_all(shard, axis):
    copies = jnp.broadcast_to(shard, (lax.axis_size(axis), *shard.shape))
    return lax.all_to_all(copies, axis, split_axis=0, concat_axis=0, tiled=True)


def gathered_copies(shard, axis, dim):
    return in_order(sent_to_all(shard, axis), dim)


def cut_along(shard, dim, count):
    lengths = shard.shape
    tiles = shard.reshape(*lengths[:dim], count, lengths[dim] // count, *lengths[dim + 1 :])
    return jnp.moveaxis(tiles, dim, 0)


def sent_and_summed(shard, axis, dim):
    count = lax.axis_size(axis)
    tiles = lax.all_to_all(cut_along(shard, dim, count), axis, 0, 0, tiled=True)
    return jnp.sum(tiles.astype(jnp.float32), axis=0)


def norm_rows(values, gain_vec):
    widened = values.astype(jnp.float32)
    return (
        widened
        * lax.rsqrt(jnp.mean(widened * widened, axis=-1, keepdims=True) + epsilon)
        * gain_vec
    )


def attention(normed, kv_cache, lengths, w_query, w_key, w_value, lambdas, head_gain):
    seq_count = normed.shape[0]
    v_width = head_gain.shape[0]
    qk_width = v_width // 2
    kv_local = kv_cache.shape[2] // (2 * v_width)
    head_local = lambdas.shape[0]
    group_size = head_local // kv_local
    cache_len = kv_cache.shape[1]
    queries = jnp.dot(normed, w_query, preferred_element_type=jnp.float32).astype(jnp.bfloat16)
    queries = queries.reshape(seq_count, kv_local, group_size, 2, qk_width)
    key_new = jnp.dot(normed, w_key, preferred_element_type=jnp.float32).astype(jnp.bfloat16)
    key_new = key_new.reshape(seq_count, kv_local, 2, qk_width)
    value_new = jnp.dot(normed, w_value, preferred_element_type=jnp.float32).astype(jnp.bfloat16)
    value_new = value_new.reshape(seq_count, kv_local, v_width)
    layout = kv_cache.reshape(seq_count, cache_len, kv_local, 2 * v_width)
    keys_old = layout[..., :v_width].reshape(seq_count, cache_len, kv_local, 2, qk_width)
    values_old = layout[..., v_width:]
    scaling = qk_width ** (-0.5)
    scores_old = (
        jnp.einsum("skgmd,sckmd->skgmc", queries, keys_old, preferred_element_type=jnp.float32)
        * scaling
    )
    scores_new = (
        jnp.einsum("skgmd,skmd->skgm", queries, key_new, preferred_element_type=jnp.float32)
        * scaling
    )
    position = jnp.arange(cache_len, dtype=jnp.int32)
    valid_mask = (position[None, :] < lengths[:, None])[:, None, None, None, :]
    scores_old = jnp.where(valid_mask, scores_old, neg_fill)
    highest = jnp.maximum(jnp.max(scores_old, axis=-1), scores_new)
    expo_old = jnp.where(valid_mask, jnp.exp(scores_old - highest[..., None]), 0.0)
    expo_new = jnp.exp(scores_new - highest)
    totals = jnp.sum(expo_old, axis=-1) + expo_new
    lambda_grid = lambdas.reshape(kv_local, group_size)[None, :, :]
    weight_old = (
        expo_old[..., 0, :] / totals[..., 0, None]
        - lambda_grid[..., None] * expo_old[..., 1, :] / totals[..., 1, None]
    ).astype(jnp.bfloat16)
    weight_new = (
        expo_new[..., 0] / totals[..., 0] - lambda_grid * expo_new[..., 1] / totals[..., 1]
    ).astype(jnp.bfloat16)
    head_mix = jnp.einsum(
        "skgc,sckv->skgv", weight_old, values_old, preferred_element_type=jnp.float32
    )
    head_mix = (
        head_mix
        + weight_new.astype(jnp.float32)[..., None] * value_new.astype(jnp.float32)[:, :, None, :]
    )
    return (
        norm_rows(head_mix, head_gain).astype(jnp.bfloat16).reshape(seq_count, head_local * v_width)
    )


def shards(
    tokens,
    kv_cache,
    lengths,
    attn_gain,
    w_query,
    w_key,
    w_value,
    lambdas,
    head_gain,
    w_out,
    ffn_gain,
    w_shared_gate,
    w_shared_up,
    w_shared_down,
    routing,
    route_weights,
    w_exp_gate,
    w_exp_up,
    w_exp_down,
):
    seq_count = tokens.shape[0]
    width = tokens.shape[1]
    tp_count = lax.axis_size("tp")
    tp_index = lax.axis_index("tp")
    ep_count = lax.axis_size("ep")
    ep_index = lax.axis_index("ep")
    normed = norm_rows(tokens, attn_gain).astype(jnp.bfloat16)
    head_out = attention(normed, kv_cache, lengths, w_query, w_key, w_value, lambdas, head_gain)
    share_rows = head_out.shape[1]
    all_heads = gathered_copies(head_out, "tp", 1)
    pieces = jnp.einsum(
        "stk,tkd->tsd",
        all_heads.reshape(seq_count, tp_count, share_rows),
        w_out.reshape(tp_count, share_rows, -1),
        preferred_element_type=jnp.float32,
    )
    rounded = lax.optimization_barrier(pieces.astype(jnp.bfloat16))
    projected = jnp.sum(rounded.astype(jnp.float32), axis=0)
    residual = (tokens.astype(jnp.float32) + projected).astype(jnp.bfloat16)
    ffn_in = norm_rows(residual, ffn_gain).astype(jnp.bfloat16)
    gate_vals = jnp.dot(ffn_in, w_shared_gate, preferred_element_type=jnp.float32)
    up_vals = jnp.dot(ffn_in, w_shared_up, preferred_element_type=jnp.float32)
    shared_act = (jax.nn.silu(gate_vals) * up_vals).astype(jnp.bfloat16)
    shared_part = jnp.dot(shared_act, w_shared_down, preferred_element_type=jnp.float32)
    top_count = routing.shape[1]
    experts = w_exp_gate.shape[0] * ep_count * tp_count
    capacity = max(2, 2 * seq_count * top_count // experts)
    own_routing = lax.dynamic_slice_in_dim(routing, ep_index * seq_count, seq_count, 0)
    flat_ids = own_routing.reshape(-1)
    onehot = (flat_ids[:, None] == jnp.arange(experts, dtype=jnp.int32)[None, :]).astype(jnp.int32)
    slot_rank = jnp.sum((jnp.cumsum(onehot, axis=0) - onehot) * onehot, axis=1)
    in_column = flat_ids % tp_count == tp_index
    slot_ids = jnp.where(in_column, flat_ids // tp_count * capacity + slot_rank, -1)
    selector = (
        slot_ids[:, None] == jnp.arange(ep_count * capacity, dtype=jnp.int32)[None, :]
    ).astype(jnp.bfloat16)
    dispatch = jnp.sum(selector.reshape(seq_count, top_count, -1), axis=1)
    packed = jnp.einsum("sj,sd->jd", dispatch, ffn_in, preferred_element_type=jnp.float32).astype(
        jnp.bfloat16
    )
    packed = packed.reshape(ep_count, capacity, width)
    arrived = lax.all_to_all(packed, "ep", split_axis=0, concat_axis=0, tiled=True)
    flat_rows = arrived.reshape(-1, width)
    gate_part = jnp.dot(flat_rows, w_exp_gate[0], preferred_element_type=jnp.float32)
    up_part = jnp.dot(flat_rows, w_exp_up[0], preferred_element_type=jnp.float32)
    inner_act = (jax.nn.silu(gate_part) * up_part).astype(jnp.bfloat16)
    result = jnp.dot(inner_act, w_exp_down[0], preferred_element_type=jnp.float32).astype(
        jnp.bfloat16
    )
    computed = result.reshape(arrived.shape)
    returned = lax.all_to_all(computed, "ep", split_axis=0, concat_axis=0, tiled=True)
    routed_rows = jnp.dot(
        selector, returned.reshape(ep_count * capacity, width), preferred_element_type=jnp.float32
    ).reshape(seq_count, top_count, width)
    routed_part = jnp.sum(route_weights[:, :, None] * routed_rows, axis=1)
    combined = sent_and_summed((shared_part + routed_part).astype(jnp.bfloat16), "tp", 1)
    width_share = width // tp_count
    own_resid = lax.dynamic_slice_in_dim(residual, tp_index * width_share, width_share, 1).astype(
        jnp.float32
    )
    return (own_resid + combined).astype(jnp.bfloat16)


def solution(mesh):
    return jax.shard_map(
        shards,
        mesh=mesh,
        in_specs=(
            P("ep", None),
            P("ep", None, "tp"),
            P("ep"),
            P(),
            P(None, "tp"),
            P(None, "tp"),
            P(None, "tp"),
            P("tp"),
            P(),
            P(),
            P(),
            P(None, "tp"),
            P(None, "tp"),
            P("tp", None),
            P(),
            P("ep", None),
            P(("ep", "tp"), None, None),
            P(("ep", "tp"), None, None),
            P(("ep", "tp"), None, None),
        ),
        out_specs=P("ep", "tp"),
        check_vma=False,
    )
```

profile of v0, /device:TPU:1, one launch (start us, length us, event | category | flops | bytes accessed | tf_op | source)
XLA Modules:
  0.0 90.5 jit_solution(2187224256156566289)
XLA Ops:
  0.0 1.2 %fusion.28 = f32[32]{0:T(128)S(1)} fusion(bf16[32,2048]{1,0:T(8,128)(2,1)} %param.19), kind=kLoop, calls=%fused_computation.42 | loop fusion | flops 196576 | bytes 131200 | tf_op jit(solution)/shard_map/reduce_sum | solution.py:41
  1.2 1.6 %convolution_convert_fusion.3 = bf16[32,256]{1,0:T(8,128)(2,1)S(1)} fusion(bf16[2048,256]{1,0:T(8,128)(2,1)} %param.23, bf16[32,2048]{1,0:T(8,128)(2,1)} %param.19, f32[2048]{0:T(1024)} %param.22, f32[32]{0:T(128)S(1)} %add_rsqrt_fusion.2), kind=kOutput, calls=%fused_computation.21 | convolution fusion | flops 33824768 | bytes 1204352 | tf_op jit(solution)/shard_map/dot_general | solution.py:54
  3.0 11.9 %copy.63 = bf16[32,1024,128]{1,2,0:T(8,128)(2,1)} copy(bf16[32,1024,128]{2,1,0:T(8,128)(2,1)} %param.20) | data formatting | bytes 16777216 | tf_op args[1]
  14.9 2.6 %slice.34 = bf16[32,1024,1,64]{1,3,0,2:T(8,128)(2,1)S(1)} slice(bf16[32,1024,1,128]{1,3,0,2:T(8,128)(2,1)} %bitcast.124), slice={[0:32], [0:1024], [0:1], [0:64]} | slice | bytes 8388608 | tf_op jit(solution)/shard_map/slice | solution.py:61
  17.7 1.0 %fusion.81 = (f32[32,4,2]{1,2,0:T(2,128)S(1)}, f32[32,1,4,2,1024]{4,2,3,0,1:T(4,128)S(1)}) fusion(bf16[32,1024,2,32]{1,3,2,0:T(8,128)(2,1)S(1)} %bitcast.126, bf16[32,4,2,32]{3,2,1,0:T(2,128)(2,1)S(1)} %reshape.251, pred[32,1024]{1,0:T(8,128)(4,1)S(1)} %iota_compare_fusion), kind=kOutput, calls=%fused_computation.114 | convolution fusion | flops 17563392 | bytes 5293056 | tf_op jit(solution)/shard_map/skgmd,sckmd->skgmc/dot_general | solution.py:65
  18.8 1.2 %convolution_convert_fusion.5 = bf16[32,64]{1,0:T(8,128)(2,1)S(1)} fusion(bf16[2048,64]{0,1:T(8,128)(2,1)} %param.24, bf16[32,2048]{1,0:T(8,128)(2,1)S(1)} %copy-done.1, f32[2048]{0:T(1024)S(1)} %copy-done.4, f32[32]{0:T(128)S(1)} %add_rsqrt_fusion.2), kind=kOutput, calls=%fused_computation.26 | convolution fusion | flops 8652800 | bytes 405632 | tf_op jit(solution)/shard_map/dot_general | solution.py:56
  20.1 0.2 fusion.46
  20.5 1.7 %fusion.80 = (f32[32,4,2]{1,2,0:T(2,128)S(1)}, f32[32,1,4,2,1024]{4,2,3,0,1:T(4,128)}) fusion(f32[32,1,4,2,1024]{4,2,3,0,1:T(4,128)S(1)} %get-tuple-element.15, f32[32,4,2]{1,2,0:T(2,128)S(1)} %copy.66, pred[32,1024]{1,0:T(8,128)(4,1)S(1)} %iota_compare_fusion), kind=kLoop, calls=%fused_computation.113 | loop fusion | flops 786176 | bytes 2131968 | tf_op jit(solution)/shard_map/reduce_sum | solution.py:78
  22.6 1.2 %fusion.21 = f32[32,64]{1,0:T(8,128)S(1)} fusion(bf16[2048,64]{0,1:T(8,128)(2,1)} %param.25, bf16[32,2048]{1,0:T(8,128)(2,1)S(1)} %copy-done.1, f32[2048]{0:T(1024)S(1)} %copy-done.4, f32[32]{0:T(128)S(1)} %add_rsqrt_fusion.2), kind=kOutput, calls=%fused_computation.25 | convolution fusion | flops 8654848 | bytes 409728 | tf_op jit(solution)/shard_map/dot_general | solution.py:58
  23.9 3.9 %multiply_reduce_fusion = (f32[32,4]{1,0:T(8,128)S(1)}, f32[32,4,64]{2,1,0:T(4,128)S(1)}) fusion(f32[32,64]{1,0:T(8,128)S(1)} %fusion.21, f32[32,4]{1,0:T(8,128)S(1)} %copy.71, bf16[32,1024,1,128]{1,3,0,2:T(8,128)(2,1)} %bitcast.125, f32[32,1,4,2,1024]{4,2,3,0,1:T(4,128)} %get-tuple-element.10, f32[32,4]{1,0:T(8,128)S(1)} %copy.70, f32[4]{0:T(128)S(1)} %copy-done.7, ...), kind=kOutput, calls=%fused_computation.66 | convolution fusion | flops 17465216 | bytes 5285904 | tf_op jit(solution)/shard_map/skgc,sckv->skgv/dot_general | solution.py:87
  28.0 0.6 broadcast_in_dim.45
  28.6 4.8 %all-to-all-start = ((bf16[4,32,256]{2,1,0:T(8,128)(2,1)}), bf16[4,32,256]{2,1,0:T(8,128)(2,1)S(1)}, u32[]{:S(2)}, u32[]{:S(2)}) async-start(bf16[4,32,256]{2,1,0:T(8,128)(2,1)} %broadcast_in_dim.45), calls=%async_computation | async-start | bytes 131072 | tf_op jit(solution)/shard_map/all_to_all | solution.py:18
  33.5 0.8 constant_dynamic-slice_fusion
  34.5 0.2 reduce_window_sum.11
  34.7 0.2 select_reduce_fusion
  35.2 2.8 %all-to-all-done = bf16[4,32,256]{2,1,0:T(8,128)(2,1)S(1)} async-done(((bf16[4,32,256]{2,1,0:T(8,128)(2,1)}), bf16[4,32,256]{2,1,0:T(8,128)(2,1)S(1)}, u32[]{:S(2)}, u32[]{:S(2)}) %all-to-all-start) | async-done | bytes 65568 | tf_op jit(solution)/shard_map/all_to_all | solution.py:18
  37.9 3.0 %convolution_convert_fusion = bf16[4,32,2048]{2,1,0:T(8,128)(2,1)S(1)} fusion(bf16[4,256,2048]{2,1,0:T(8,128)(2,1)} %bitcast.127, bf16[4,32,256]{2,1,0:T(8,128)(2,1)S(1)} %all-to-all-done), kind=kOutput, calls=%fused_computation.3 | convolution fusion | flops 134479872 | bytes 4784128 | tf_op jit(solution)/shard_map/stk,tkd->tsd/dot_general | solution.py:130
  41.2 0.3 convolution_convert_fusion.2
  41.5 0.2 reshape.258
  41.7 18.9 %all_to_all.20 = bf16[32,2,2048]{2,1,0:T(2,128)(2,1)S(1)} all-to-all(bf16[32,2,2048]{2,1,0:T(2,128)(2,1)S(1)} %reshape.258), channel_id=1, replica_groups=mesh['ep'=32,'tp'=4] {'ep'}, dimensions={0} | all-to-all | bytes 524288 | tf_op jit(solution)/shard_map/all_to_all | solution.py:161
  60.7 2.1 %fusion.5 = f32[64,512]{1,0:T(8,128)S(1)} fusion(bf16[64,2048]{1,0:T(8,128)(2,1)S(1)} %reshape.259, bf16[1,2048,512]{2,1,0:T(8,128)(2,1)} %param.35), kind=kOutput, calls=%fused_computation.11 | convolution fusion | flops 134217728 | bytes 2490368 | tf_op jit(solution)/shard_map/dot_general | solution.py:163
  62.8 2.5 %convolution_convert_fusion.1 = bf16[64,2048]{1,0:T(8,128)(2,1)S(1)} fusion(bf16[1,512,2048]{2,1,0:T(8,128)(2,1)S(1)} %copy-done, bf16[64,2048]{1,0:T(8,128)(2,1)S(1)} %reshape.259, bf16[1,2048,512]{2,1,0:T(8,128)(2,1)} %param.36, f32[64,512]{1,0:T(8,128)S(1)} %fusion.5), kind=kOutput, calls=%fused_computation.4 | convolution fusion | flops 268763136 | bytes 4849664 | tf_op jit(solution)/shard_map/dot_general | solution.py:166
  65.3 0.9 reshape.260
  66.2 3.8 %all-to-all-start.2 = ((bf16[32,2,2048]{2,1,0:T(2,128)(2,1)}), bf16[32,2,2048]{2,1,0:T(2,128)(2,1)S(1)}, u32[]{:S(2)}, u32[]{:S(2)}) async-start(bf16[32,2,2048]{2,1,0:T(2,128)(2,1)} %reshape.260), calls=%async_computation.2 | async-start | bytes 524288 | tf_op jit(solution)/shard_map/all_to_all | solution.py:170
  70.0 0.3 fusion.76
  70.3 8.6 %all-to-all-done.2 = bf16[32,2,2048]{2,1,0:T(2,128)(2,1)S(1)} async-done(((bf16[32,2,2048]{2,1,0:T(2,128)(2,1)}), bf16[32,2,2048]{2,1,0:T(2,128)(2,1)S(1)}, u32[]{:S(2)}, u32[]{:S(2)}) %all-to-all-start.2) | async-done | bytes 262176 | tf_op jit(solution)/shard_map/all_to_all | solution.py:170
  79.0 0.3 fusion.8
  79.3 1.6 %fusion.1 = bf16[32,2048]{1,0:T(8,128)(2,1)S(1)} fusion(f32[32,2048]{1,0:T(8,128)S(1)} %fusion.8, bf16[128,2048]{1,0:T(8,128)(2,1)} %param.32, bf16[2048,128]{1,0:T(8,128)(2,1)} %param.31, f32[32,128]{1,0:T(8,128)S(1)} %fusion.76, bf16[32,2048]{1,0:T(8,128)(2,1)S(1)} %get-tuple-element.6, f32[2048]{0:T(1024)S(1)} %copy-done.3, f32[32]{0:T(128)S(1)} %add_rsqrt_fusion.1), kind=kOutput, calls=%fused_computation.7 | convolution fusion | flops 33972224 | bytes 1597568 | tf_op jit(solution)/shard_map/dot_general | solution.py:143
  81.0 0.7 copy.88
  81.7 3.3 %all-to-all-start.3 = ((bf16[4,32,512]{2,1,0:T(8,128)(2,1)}), bf16[4,32,512]{2,1,0:T(8,128)(2,1)S(1)}, u32[]{:S(2)}, u32[]{:S(2)}) async-start(bf16[4,32,512]{2,1,0:T(8,128)(2,1)} %bitcast.123), calls=%async_computation.3 | async-start | bytes 262144 | tf_op jit(solution)/shard_map/all_to_all | solution.py:33
  85.0 4.9 %all-to-all-done.3 = bf16[4,32,512]{2,1,0:T(8,128)(2,1)S(1)} async-done(((bf16[4,32,512]{2,1,0:T(8,128)(2,1)}), bf16[4,32,512]{2,1,0:T(8,128)(2,1)S(1)}, u32[]{:S(2)}, u32[]{:S(2)}) %all-to-all-start.3) | async-done | bytes 131104 | tf_op jit(solution)/shard_map/all_to_all | solution.py:33
  89.9 0.6 add_convert_fusion
  (48 shorter events, 2.4 us)
Async XLA Ops:
  0.0 62.8 %copy-start = (bf16[1,512,2048]{2,1,0:T(8,128)(2,1)S(1)}, bf16[1,512,2048]{2,1,0:T(8,128)(2,1)}, u32[]{:S(2)}) copy-start(bf16[1,512,2048]{2,1,0:T(8,128)(2,1)} %param.37) | copy-start | bytes 6291460
  14.9 2.7 %copy-start.5 = (s32[32]{0:T(128)S(1)}, s32[32]{0:T(128)}, u32[]{:S(2)}) copy-start(s32[32]{0:T(128)} %param.21) | copy-start | bytes 388
  17.6 1.2 %copy-start.1 = (bf16[32,2048]{1,0:T(8,128)(2,1)S(1)}, bf16[32,2048]{1,0:T(8,128)(2,1)}, u32[]{:S(2)}) copy-start(bf16[32,2048]{1,0:T(8,128)(2,1)} %param.19) | copy-start | bytes 393220
  17.6 1.2 %copy-start.4 = (f32[2048]{0:T(1024)S(1)}, f32[2048]{0:T(1024)}, u32[]{:S(2)}) copy-start(f32[2048]{0:T(1024)} %param.22) | copy-start | bytes 24580
  17.7 4.6 %copy-start.7 = (f32[4]{0:T(128)S(1)}, f32[4]{0:T(128)}, u32[]{:S(2)}) copy-start(f32[4]{0:T(128)} %param.26) | copy-start | bytes 52
  23.9 3.9 %copy-start.6 = (f32[64]{0:T(128)S(1)}, f32[64]{0:T(128)}, u32[]{:S(2)}) copy-start(f32[64]{0:T(128)} %param.27) | copy-start | bytes 772
  28.6 9.3 %all-to-all-start = ((bf16[4,32,256]{2,1,0:T(8,128)(2,1)}), bf16[4,32,256]{2,1,0:T(8,128)(2,1)S(1)}, u32[]{:S(2)}, u32[]{:S(2)}) async-start(bf16[4,32,256]{2,1,0:T(8,128)(2,1)} %broadcast_in_dim.45), calls=%async_computation | async-start | bytes 131072 | tf_op jit(solution)/shard_map/all_to_all | solution.py:18
  37.9 3.3 %copy-start.3 = (f32[2048]{0:T(1024)S(1)}, f32[2048]{0:T(1024)}, u32[]{:S(2)}) copy-start(f32[2048]{0:T(1024)} %param.29) | copy-start | bytes 24580
  60.7 9.3 %copy-start.2 = (bf16[2048,128]{1,0:T(8,128)(2,1)S(1)}, bf16[2048,128]{1,0:T(8,128)(2,1)}, u32[]{:S(2)}) copy-start(bf16[2048,128]{1,0:T(8,128)(2,1)} %param.30) | copy-start | bytes 1572868
  60.7 18.3 %copy-start.8 = (f32[32,4]{0,1:T(4,128)S(1)}, f32[32,4]{0,1:T(4,128)}, u32[]{:S(2)}) copy-start(f32[32,4]{0,1:T(4,128)} %param.34) | copy-start | bytes 1540
  66.2 12.7 %all-to-all-start.2 = ((bf16[32,2,2048]{2,1,0:T(2,128)(2,1)}), bf16[32,2,2048]{2,1,0:T(2,128)(2,1)S(1)}, u32[]{:S(2)}, u32[]{:S(2)}) async-start(bf16[32,2,2048]{2,1,0:T(2,128)(2,1)} %reshape.260), calls=%async_computation.2 | async-start | bytes 524288 | tf_op jit(solution)/shard_map/all_to_all | solution.py:170
  81.7 8.2 %all-to-all-start.3 = ((bf16[4,32,512]{2,1,0:T(8,128)(2,1)}), bf16[4,32,512]{2,1,0:T(8,128)(2,1)S(1)}, u32[]{:S(2)}, u32[]{:S(2)}) async-start(bf16[4,32,512]{2,1,0:T(8,128)(2,1)} %bitcast.123), calls=%async_computation.3 | async-start | bytes 262144 | tf_op jit(solution)/shard_map/all_to_all | solution.py:33
where the time goes:
time: 91.5 us; the launch traced here: 90.5 us
  local copies, waits for them, and re-layouts  19.3 us (21%)
  matrix products  19.3 us (21%)
  blocking collectives  18.9 us (21%)
  waiting for transfers between devices  16.3 us (18%)
  starting transfers between devices  11.9 us (13%)
  other arithmetic  4.63 us (5%)
    all_to_all x1, blocking collectives, shards(): lax.all_to_all(packed, 'ep', split_axis=0, concat_axis=0, tiled=True)  18.9 us
    unnamed x20, local copies, waits for them, and re-layouts  12.1 us
    all_to_all x1, waiting for transfers between devices, shards(): lax.all_to_all(computed, 'ep', split_axis=0, concat_axis=0, tiled=True)  8.62 us
    all_to_all x1, waiting for transfers between devices, sent_and_summed(): tiles = lax.all_to_all(cut_along(shard, dim, count), axis, 0, 0, tiled=True)  4.89 us
    all_to_all x1, starting transfers between devices, sent_to_all(): return lax.all_to_all(copies, axis, split_axis=0, concat_axis=0, tiled=True)  4.83 us
    dot_general x1, matrix products, attention(): jnp.einsum('skgc,sckv->skgv', weight_old, values_old, preferred_element_t...  3.87 us
    all_to_all x1, starting transfers between devices, shards(): lax.all_to_all(computed, 'ep', split_axis=0, concat_axis=0, tiled=True)  3.75 us
    all_to_all x1, starting transfers between devices, sent_and_summed(): tiles = lax.all_to_all(cut_along(shard, dim, count), axis, 0, 0, tiled=True)  3.32 us
  transfers between devices with their start and end apart: 3, of which 3 were waited for; matrix products, arithmetic and copies ran while one was open for 2% of the time, Pallas kernels for 0%

commit v1 on v0

--- a/solution.py
+++ b/solution.py
@@ -123,61 +123,77 @@
     tp_index = lax.axis_index("tp")
     ep_count = lax.axis_size("ep")
     ep_index = lax.axis_index("ep")
+    experts = ep_count * tp_count
+    capacity = 2
+    width_share = width // tp_count
     normed = norm_rows(tokens, attn_gain).astype(jnp.bfloat16)
     head_out = attention(normed, kv_cache, lengths, w_query, w_key, w_value, lambdas, head_gain)
     share_rows = head_out.shape[1]
-    all_heads = gathered_copies(head_out, "tp", 1)
-    pieces = jnp.einsum(
-        "stk,tkd->tsd",
-        all_heads.reshape(seq_count, tp_count, share_rows),
-        w_out.reshape(tp_count, share_rows, -1),
-        preferred_element_type=jnp.float32,
-    )
-    rounded = lax.optimization_barrier(pieces.astype(jnp.bfloat16))
-    projected = jnp.sum(rounded.astype(jnp.float32), axis=0)
-    residual = (tokens.astype(jnp.float32) + projected).astype(jnp.bfloat16)
+    own_routing = lax.dynamic_slice_in_dim(routing, ep_index * seq_count, seq_count, 0)
+    hits = own_routing[:, :, None] == jnp.arange(experts, dtype=jnp.int32)[None, None, :]
+    named = jnp.any(hits, axis=1).astype(jnp.bfloat16)
+    earlier = (
+        jnp.arange(seq_count)[:, None] > jnp.arange(seq_count)[None, :]
+    ).astype(jnp.bfloat16)
+    rank = jnp.dot(earlier, named, preferred_element_type=jnp.float32)
+    rank_ok = rank[:, :, None] == jnp.arange(capacity, dtype=jnp.float32)[None, None, :]
+    placed = (named[:, :, None] > 0) & rank_ok
+    dispatch = placed.astype(jnp.bfloat16).reshape(seq_count, experts * capacity)
+    selector = (hits[:, :, :, None] & rank_ok[:, None, :, :]).astype(jnp.bfloat16)
+    selector = selector.reshape(seq_count * hits.shape[1], experts * capacity)
+    own_tokens = lax.dynamic_slice_in_dim(tokens, tp_index * width_share, width_share, 1)
+    rows = jnp.concatenate([head_out, own_tokens], axis=1)
+    packed = jnp.einsum("sj,sd->jd", dispatch, rows, preferred_element_type=jnp.float32).astype(
+        jnp.bfloat16
+    )
+    packed = packed.reshape(experts, capacity, share_rows + width_share)
+    arrived = lax.all_to_all(packed, ("ep", "tp"), split_axis=0, concat_axis=0, tiled=True)
+
+    def project(parts):
+        pieces = jnp.einsum(
+            "tmk,tkd->tmd",
+            parts,
+            w_out.reshape(tp_count, share_rows, -1),
+            preferred_element_type=jnp.float32,
+        )
+        rounded = lax.optimization_barrier(pieces.astype(jnp.bfloat16))
+        return jnp.sum(rounded.astype(jnp.float32), axis=0)
+
+    all_heads = sent_to_all(head_out, "tp")
+    residual = (tokens.astype(jnp.float32) + project(all_heads)).astype(jnp.bfloat16)
     ffn_in = norm_rows(residual, ffn_gain).astype(jnp.bfloat16)
     gate_vals = jnp.dot(ffn_in, w_shared_gate, preferred_element_type=jnp.float32)
     up_vals = jnp.dot(ffn_in, w_shared_up, preferred_element_type=jnp.float32)
     shared_act = (jax.nn.silu(gate_vals) * up_vals).astype(jnp.bfloat16)
     shared_part = jnp.dot(shared_act, w_shared_down, preferred_element_type=jnp.float32)
-    top_count = routing.shape[1]
-    experts = w_exp_gate.shape[0] * ep_count * tp_count
-    capacity = max(2, 2 * seq_count * top_count // experts)
-    own_routing = lax.dynamic_slice_in_dim(routing, ep_index * seq_count, seq_count, 0)
-    flat_ids = own_routing.reshape(-1)
-    onehot = (flat_ids[:, None] == jnp.arange(experts, dtype=jnp.int32)[None, :]).astype(jnp.int32)
-    slot_rank = jnp.sum((jnp.cumsum(onehot, axis=0) - onehot) * onehot, axis=1)
-    in_column = flat_ids % tp_count == tp_index
-    slot_ids = jnp.where(in_column, flat_ids // tp_count * capacity + slot_rank, -1)
-    selector = (
-        slot_ids[:, None] == jnp.arange(ep_count * capacity, dtype=jnp.int32)[None, :]
-    ).astype(jnp.bfloat16)
-    dispatch = jnp.sum(selector.reshape(seq_count, top_count, -1), axis=1)
-    packed = jnp.einsum("sj,sd->jd", dispatch, ffn_in, preferred_element_type=jnp.float32).astype(
+    shared = sent_and_summed(shared_part.astype(jnp.bfloat16), "tp", 1)
+    own_resid = lax.dynamic_slice_in_dim(residual, tp_index * width_share, width_share, 1)
+    base = own_resid.astype(jnp.float32) + shared
+
+    slots = ep_count * capacity
+    parts = arrived.reshape(ep_count, tp_count, capacity, -1).transpose(1, 0, 2, 3)
+    parts = parts.reshape(tp_count, slots, -1)
+    row_tokens = in_order(parts[:, :, share_rows:], 1)
+    row_resid = (row_tokens.astype(jnp.float32) + project(parts[:, :, :share_rows])).astype(
         jnp.bfloat16
     )
-    packed = packed.reshape(ep_count, capacity, width)
-    arrived = lax.all_to_all(packed, "ep", split_axis=0, concat_axis=0, tiled=True)
-    flat_rows = arrived.reshape(-1, width)
+    flat_rows = norm_rows(row_resid, ffn_gain).astype(jnp.bfloat16)
     gate_part = jnp.dot(flat_rows, w_exp_gate[0], preferred_element_type=jnp.float32)
     up_part = jnp.dot(flat_rows, w_exp_up[0], preferred_element_type=jnp.float32)
     inner_act = (jax.nn.silu(gate_part) * up_part).astype(jnp.bfloat16)
     result = jnp.dot(inner_act, w_exp_down[0], preferred_element_type=jnp.float32).astype(
         jnp.bfloat16
     )
-    computed = result.reshape(arrived.shape)
-    returned = lax.all_to_all(computed, "ep", split_axis=0, concat_axis=0, tiled=True)
+    computed = result.reshape(ep_count, capacity, tp_count, width_share).transpose(0, 2, 1, 3)
+    computed = computed.reshape(experts, capacity, width_share)
+    returned = lax.all_to_all(computed, ("ep", "tp"), split_axis=0, concat_axis=0, tiled=True)
     routed_rows = jnp.dot(
-        selector, returned.reshape(ep_count * capacity, width), preferred_element_type=jnp.float32
-    ).reshape(seq_count, top_count, width)
-    routed_part = jnp.sum(route_weights[:, :, None] * routed_rows, axis=1)
-    combined = sent_and_summed((shared_part + routed_part).astype(jnp.bfloat16), "tp", 1)
-    width_share = width // tp_count
-    own_resid = lax.dynamic_slice_in_dim(residual, tp_index * width_share, width_share, 1).astype(
-        jnp.float32
-    )
-    return (own_resid + combined).astype(jnp.bfloat16)
+        selector,
+        returned.reshape(experts * capacity, width_share),
+        preferred_element_type=jnp.float32,
+    ).reshape(seq_count, -1, width_share)
+    routed = jnp.sum(route_weights[:, :, None] * routed_rows, axis=1)
+    return (base + routed).astype(jnp.bfloat16)
 
 
 def solution(mesh):

time: 91.5 us -> 91.5 us (level)
  blocking collectives: 18.9 us -> 0 us
  starting transfers between devices: 11.9 us -> 24.4 us
  waiting for transfers between devices: 16.3 us -> 19.5 us
  matrix products: 19.3 us -> 21 us
  local copies, waits for them, and re-layouts: 19.3 us -> 20.6 us
    all_to_all x1 -> x0, blocking collectives: 18.9 us -> none  [shards(): lax.all_to_all(packed, 'ep', split_axis=0, concat_axis=0, tiled=True)]
    all_to_all x1 -> x2, starting transfers between devices: 3.75 us -> 16.3 us  [the longest x1 10.2 us: shards(): lax.all_to_all(packed, ('ep', 'tp'), split_axis=0, concat_axis=0, tiled=T...]
    all_to_all x1 -> x2, waiting for transfers between devices: 8.62 us -> 17.8 us  [the longest x1 11.1 us: shards(): lax.all_to_all(computed, ('ep', 'tp'), split_axis=0, concat_axis=0, tiled...]
    all_to_all x1, waiting for transfers between devices: 4.89 us -> 0.01 us  [sent_and_summed(): tiles = lax.all_to_all(cut_along(shard, dim, count), axis, 0, 0, tiled=True)]
    dot_general x3 -> x5, matrix products: 3.64 us -> 6.96 us  [the longest x2 6.25 us: project(): jnp.einsum('tmk,tkd->tmd', parts, w_out.reshape(tp_count, share_rows, -1)...]
    dot_general x1, matrix products: 2.12 us -> 0.47 us  [shards(): jnp.dot(flat_rows, w_exp_gate[0], preferred_element_type=jnp.float32)]
    all_to_all x1, waiting for transfers between devices: 2.76 us -> 1.68 us  [sent_to_all(): return lax.all_to_all(copies, axis, split_axis=0, concat_axis=0, tiled=True)]
    unnamed x20 -> x21, local copies, waits for them, and re-layouts: 12.1 us -> 12 us
  transfers between devices with their start and end apart: 3 -> 4, of which waited for: 3 -> 3; matrix products, arithmetic and copies ran while one was open for 2% -> 19% of each run, Pallas kernels for 0% -> 0%
where the time goes in v1:
time: 91.5 us; the launch traced here: 90.6 us
  starting transfers between devices  24.4 us (27%)
  matrix products  21 us (23%)
  local copies, waits for them, and re-layouts  20.6 us (23%)
  waiting for transfers between devices  19.5 us (21%)
  other arithmetic  4.73 us (5%)
    unnamed x21, local copies, waits for them, and re-layouts  12 us
    all_to_all x1, waiting for transfers between devices, shards(): lax.all_to_all(computed, ('ep', 'tp'), split_axis=0, concat_axis=0, tiled...  11.1 us
    all_to_all x1, starting transfers between devices, shards(): lax.all_to_all(packed, ('ep', 'tp'), split_axis=0, concat_axis=0, tiled=T...  10.2 us
    all_to_all x1, waiting for transfers between devices, shards(): lax.all_to_all(packed, ('ep', 'tp'), split_axis=0, concat_axis=0, tiled=T...  6.67 us
    dot_general x2, matrix products, project(): jnp.einsum('tmk,tkd->tmd', parts, w_out.reshape(tp_count, share_rows, -1)...  6.25 us
    all_to_all x1, starting transfers between devices, shards(): lax.all_to_all(computed, ('ep', 'tp'), split_axis=0, concat_axis=0, tiled...  6.04 us
    all_to_all x1, starting transfers between devices, sent_to_all(): return lax.all_to_all(copies, axis, split_axis=0, concat_axis=0, tiled=True)  4.84 us
    dot_general x1, matrix products, attention(): jnp.einsum('skgc,sckv->skgv', weight_old, values_old, preferred_element_t...  3.88 us
  transfers between devices with their start and end apart: 4, of which 3 were waited for; matrix products, arithmetic and copies ran while one was open for 19% of the time, Pallas kernels for 0%

profile of v1, /device:TPU:1, one launch (start us, length us, event | category | flops | bytes accessed | tf_op | source)
XLA Modules:
  0.0 90.6 jit_solution(997212240362119756)
XLA Ops:
  0.0 1.2 %fusion.32 = f32[32]{0:T(128)S(1)} fusion(bf16[32,2048]{1,0:T(8,128)(2,1)} %param.19), kind=kLoop, calls=%fused_computation.52 | loop fusion | flops 196576 | bytes 131200 | tf_op jit(solution)/shard_map/reduce_sum | solution.py:41
  1.2 1.6 %convolution_convert_fusion.5 = bf16[32,256]{1,0:T(8,128)(2,1)S(1)} fusion(bf16[2048,256]{1,0:T(8,128)(2,1)} %param.23, bf16[32,2048]{1,0:T(8,128)(2,1)} %param.19, f32[2048]{0:T(1024)} %param.22, f32[32]{0:T(128)S(1)} %add_rsqrt_fusion.3), kind=kOutput, calls=%fused_computation.23 | convolution fusion | flops 33824768 | bytes 1204352 | tf_op jit(solution)/shard_map/dot_general | solution.py:54
  3.0 11.9 %copy.60 = bf16[32,1024,128]{1,2,0:T(8,128)(2,1)} copy(bf16[32,1024,128]{2,1,0:T(8,128)(2,1)} %param.20) | data formatting | bytes 16777216 | tf_op args[1]
  14.9 2.6 %slice.42 = bf16[32,1024,1,64]{1,3,0,2:T(8,128)(2,1)S(1)} slice(bf16[32,1024,1,128]{1,3,0,2:T(8,128)(2,1)} %bitcast.158), slice={[0:32], [0:1024], [0:1], [0:64]} | slice | bytes 8388608 | tf_op jit(solution)/shard_map/slice | solution.py:61
  17.7 1.0 %fusion.87 = (f32[32,4,2]{1,2,0:T(2,128)S(1)}, f32[32,1,4,2,1024]{4,2,3,0,1:T(4,128)S(1)}) fusion(bf16[32,1024,2,32]{1,3,2,0:T(8,128)(2,1)S(1)} %bitcast.160, bf16[32,4,2,32]{3,2,1,0:T(2,128)(2,1)S(1)} %reshape.231, pred[32,1024]{1,0:T(8,128)(4,1)S(1)} %iota_compare_fusion.1), kind=kOutput, calls=%fused_computation.124 | convolution fusion | flops 17563392 | bytes 5293056 | tf_op jit(solution)/shard_map/skgmd,sckmd->skgmc/dot_general | solution.py:65
  18.8 1.2 %convolution_convert_fusion.7 = bf16[32,64]{1,0:T(8,128)(2,1)S(1)} fusion(bf16[2048,64]{0,1:T(8,128)(2,1)} %param.24, bf16[32,2048]{1,0:T(8,128)(2,1)S(1)} %copy-done.1, f32[2048]{0:T(1024)S(1)} %copy-done.5, f32[32]{0:T(128)S(1)} %add_rsqrt_fusion.3), kind=kOutput, calls=%fused_computation.28 | convolution fusion | flops 8652800 | bytes 405632 | tf_op jit(solution)/shard_map/dot_general | solution.py:56
  20.1 0.2 fusion.55
  20.5 1.7 %fusion.86 = (f32[32,4,2]{1,2,0:T(2,128)S(1)}, f32[32,1,4,2,1024]{4,2,3,0,1:T(4,128)}) fusion(f32[32,1,4,2,1024]{4,2,3,0,1:T(4,128)S(1)} %get-tuple-element.17, f32[32,4,2]{1,2,0:T(2,128)S(1)} %copy.63, pred[32,1024]{1,0:T(8,128)(4,1)S(1)} %iota_compare_fusion.1), kind=kLoop, calls=%fused_computation.123 | loop fusion | flops 786176 | bytes 2131968 | tf_op jit(solution)/shard_map/reduce_sum | solution.py:78
  22.6 1.2 %fusion.21 = f32[32,64]{1,0:T(8,128)S(1)} fusion(bf16[2048,64]{0,1:T(8,128)(2,1)} %param.25, bf16[32,2048]{1,0:T(8,128)(2,1)S(1)} %copy-done.1, f32[2048]{0:T(1024)S(1)} %copy-done.5, f32[32]{0:T(128)S(1)} %add_rsqrt_fusion.3), kind=kOutput, calls=%fused_computation.27 | convolution fusion | flops 8654848 | bytes 409728 | tf_op jit(solution)/shard_map/dot_general | solution.py:58
  23.9 3.9 %multiply_reduce_fusion = (f32[32,4]{1,0:T(8,128)S(1)}, f32[32,4,64]{2,1,0:T(4,128)S(1)}) fusion(f32[32,64]{1,0:T(8,128)S(1)} %fusion.21, f32[32,4]{1,0:T(8,128)S(1)} %copy.68, bf16[32,1024,1,128]{1,3,0,2:T(8,128)(2,1)} %bitcast.159, f32[32,1,4,2,1024]{4,2,3,0,1:T(4,128)} %get-tuple-element.10, f32[32,4]{1,0:T(8,128)S(1)} %copy.67, f32[4]{0:T(128)S(1)} %copy-done.8, ...), kind=kOutput, calls=%fused_computation.80 | convolution fusion | flops 17465216 | bytes 5285904 | tf_op jit(solution)/shard_map/skgc,sckv->skgv/dot_general | solution.py:87
  28.0 0.6 broadcast_in_dim.26
  28.6 4.8 %all-to-all-start = ((bf16[4,32,256]{2,1,0:T(8,128)(2,1)}), bf16[4,32,256]{2,1,0:T(8,128)(2,1)S(1)}, u32[]{:S(2)}, u32[]{:S(2)}) async-start(bf16[4,32,256]{2,1,0:T(8,128)(2,1)} %broadcast_in_dim.26), calls=%async_computation | async-start | bytes 131072 | tf_op jit(solution)/shard_map/all_to_all | solution.py:18
  33.5 0.8 constant_dynamic-slice_fusion.1
  34.3 0.2 fusion.70
  35.1 0.3 convolution_convert_fusion.4
  35.4 0.9 reshape.239
  36.3 1.7 %all-to-all-done = bf16[4,32,256]{2,1,0:T(8,128)(2,1)S(1)} async-done(((bf16[4,32,256]{2,1,0:T(8,128)(2,1)}), bf16[4,32,256]{2,1,0:T(8,128)(2,1)S(1)}, u32[]{:S(2)}, u32[]{:S(2)}) %all-to-all-start) | async-done | bytes 65568 | tf_op jit(solution)/shard_map/all_to_all | solution.py:18
  38.0 10.2 %all-to-all-start.2 = ((bf16[128,2,768]{2,1,0:T(2,128)(2,1)}), bf16[128,2,768]{2,1,0:T(2,128)(2,1)S(1)}, u32[]{:S(2)}, u32[]{:S(2)}) async-start(bf16[128,2,768]{2,1,0:T(2,128)(2,1)} %reshape.239), calls=%async_computation.2 | async-start | bytes 786432 | tf_op jit(solution)/shard_map/all_to_all | solution.py:150
  48.2 3.1 %convolution_convert_fusion.1 = bf16[4,32,2048]{2,1,0:T(8,128)(2,1)S(1)} fusion(bf16[4,32,256]{2,1,0:T(8,128)(2,1)S(1)} %all-to-all-done, bf16[4,256,2048]{2,1,0:T(8,128)(2,1)} %bitcast.156), kind=kOutput, calls=%fused_computation.3 | convolution fusion | flops 134479872 | bytes 4784128 | tf_op jit(solution)/shard_map/tmk,tkd->tmd/dot_general | solution.py:153
  51.5 0.3 fusion.63
  51.8 1.6 %convolution_convert_fusion.3 = bf16[32,2048]{1,0:T(8,128)(2,1)S(1)} fusion(bf16[128,2048]{1,0:T(8,128)(2,1)} %param.32, bf16[2048,128]{1,0:T(8,128)(2,1)} %param.31, bf16[32,2048]{1,0:T(8,128)(2,1)S(1)} %get-tuple-element.6, f32[2048]{0:T(1024)S(1)} %copy-done.4, f32[32]{0:T(128)S(1)} %add_rsqrt_fusion.2, f32[32,128]{1,0:T(8,128)S(1)} %fusion.63), kind=kOutput, calls=%fused_computation.5 | convolution fusion | flops 33906688 | bytes 1335424 | tf_op jit(solution)/shard_map/dot_general | solution.py:168
  53.5 0.7 copy.104
  54.1 6.7 %all-to-all-done.2 = bf16[128,2,768]{2,1,0:T(2,128)(2,1)S(1)} async-done(((bf16[128,2,768]{2,1,0:T(2,128)(2,1)}), bf16[128,2,768]{2,1,0:T(2,128)(2,1)S(1)}, u32[]{:S(2)}, u32[]{:S(2)}) %all-to-all-start.2) | async-done | bytes 393248 | tf_op jit(solution)/shard_map/all_to_all | solution.py:150
  60.8 3.3 %all-to-all-start.1 = ((bf16[4,32,512]{2,1,0:T(8,128)(2,1)}), bf16[4,32,512]{2,1,0:T(8,128)(2,1)S(1)}, u32[]{:S(2)}, u32[]{:S(2)}) async-start(bf16[4,32,512]{2,1,0:T(8,128)(2,1)} %bitcast.155), calls=%async_computation.1 | async-start | bytes 262144 | tf_op jit(solution)/shard_map/all_to_all | solution.py:33
  64.1 0.3 copy.103
  64.6 3.2 %convolution_convert_fusion = bf16[4,64,2048]{2,1,0:T(8,128)(2,1)S(1)} fusion(bf16[4,256,2048]{2,1,0:T(8,128)(2,1)} %bitcast.157, bf16[4,64,768]{2,1,0:T(8,128)(2,1)S(1)} %reshape.241), kind=kOutput, calls=%fused_computation.2 | convolution fusion | flops 268959744 | bytes 5373952 | tf_op jit(solution)/shard_map/tmk,tkd->tmd/dot_general | solution.py:153
  68.3 0.5 fusion.4
  68.8 2.5 %convolution_convert_fusion.2 = bf16[64,2048]{1,0:T(8,128)(2,1)S(1)} fusion(bf16[1,512,2048]{2,1,0:T(8,128)(2,1)S(1)} %copy-done, bf16[64,2048]{1,0:T(8,128)(2,1)S(1)} %bitcast.164, bf16[1,2048,512]{2,1,0:T(8,128)(2,1)} %param.36, f32[64,512]{1,0:T(8,128)S(1)} %fusion.4), kind=kOutput, calls=%fused_computation.4 | convolution fusion | flops 268763136 | bytes 4849664 | tf_op jit(solution)/shard_map/dot_general | solution.py:184
  71.5 0.9 copy.76
  72.4 6.0 %all-to-all-start.3 = ((bf16[128,2,512]{2,1,0:T(2,128)(2,1)}), bf16[128,2,512]{2,1,0:T(2,128)(2,1)S(1)}, u32[]{:S(2)}, u32[]{:S(2)}) async-start(bf16[128,2,512]{2,1,0:T(2,128)(2,1)} %bitcast.28), calls=%async_computation.3 | async-start | bytes 524288 | tf_op jit(solution)/shard_map/all_to_all | solution.py:189
  78.7 11.1 %all-to-all-done.3 = bf16[128,2,512]{2,1,0:T(2,128)(2,1)S(1)} async-done(((bf16[128,2,512]{2,1,0:T(2,128)(2,1)}), bf16[128,2,512]{2,1,0:T(2,128)(2,1)S(1)}, u32[]{:S(2)}, u32[]{:S(2)}) %all-to-all-start.3) | async-done | bytes 262176 | tf_op jit(solution)/shard_map/all_to_all | solution.py:189
  90.0 0.6 add_convert_fusion
  (62 shorter events, 3.4 us)
Async XLA Ops:
  0.0 68.8 %copy-start = (bf16[1,512,2048]{2,1,0:T(8,128)(2,1)S(1)}, bf16[1,512,2048]{2,1,0:T(8,128)(2,1)}, u32[]{:S(2)}) copy-start(bf16[1,512,2048]{2,1,0:T(8,128)(2,1)} %param.37) | copy-start | bytes 6291460
  14.9 2.7 %copy-start.6 = (s32[32]{0:T(128)S(1)}, s32[32]{0:T(128)}, u32[]{:S(2)}) copy-start(s32[32]{0:T(128)} %param.21) | copy-start | bytes 388
  17.6 1.2 %copy-start.1 = (bf16[32,2048]{1,0:T(8,128)(2,1)S(1)}, bf16[32,2048]{1,0:T(8,128)(2,1)}, u32[]{:S(2)}) copy-start(bf16[32,2048]{1,0:T(8,128)(2,1)} %param.19) | copy-start | bytes 393220
  17.6 1.2 %copy-start.5 = (f32[2048]{0:T(1024)S(1)}, f32[2048]{0:T(1024)}, u32[]{:S(2)}) copy-start(f32[2048]{0:T(1024)} %param.22) | copy-start | bytes 24580
  17.7 4.6 %copy-start.8 = (f32[4]{0:T(128)S(1)}, f32[4]{0:T(128)}, u32[]{:S(2)}) copy-start(f32[4]{0:T(128)} %param.26) | copy-start | bytes 52
  23.9 3.9 %copy-start.7 = (f32[64]{0:T(128)S(1)}, f32[64]{0:T(128)}, u32[]{:S(2)}) copy-start(f32[64]{0:T(128)} %param.27) | copy-start | bytes 772
  23.9 12.4 %copy-start.4 = (f32[2048]{0:T(1024)S(1)}, f32[2048]{0:T(1024)}, u32[]{:S(2)}) copy-start(f32[2048]{0:T(1024)} %param.29) | copy-start | bytes 24580
  28.6 9.3 %all-to-all-start = ((bf16[4,32,256]{2,1,0:T(8,128)(2,1)}), bf16[4,32,256]{2,1,0:T(8,128)(2,1)S(1)}, u32[]{:S(2)}, u32[]{:S(2)}) async-start(bf16[4,32,256]{2,1,0:T(8,128)(2,1)} %broadcast_in_dim.26), calls=%async_computation | async-start | bytes 131072 | tf_op jit(solution)/shard_map/all_to_all | solution.py:18
  38.0 22.9 %all-to-all-start.2 = ((bf16[128,2,768]{2,1,0:T(2,128)(2,1)}), bf16[128,2,768]{2,1,0:T(2,128)(2,1)S(1)}, u32[]{:S(2)}, u32[]{:S(2)}) async-start(bf16[128,2,768]{2,1,0:T(2,128)(2,1)} %reshape.239), calls=%async_computation.2 | async-start | bytes 786432 | tf_op jit(solution)/shard_map/all_to_all | solution.py:150
  48.2 3.3 %copy-start.3 = (bf16[2048,128]{1,0:T(8,128)(2,1)S(1)}, bf16[2048,128]{1,0:T(8,128)(2,1)}, u32[]{:S(2)}) copy-start(bf16[2048,128]{1,0:T(8,128)(2,1)} %param.30) | copy-start | bytes 1572868
  60.8 11.6 %all-to-all-start.1 = ((bf16[4,32,512]{2,1,0:T(8,128)(2,1)}), bf16[4,32,512]{2,1,0:T(8,128)(2,1)S(1)}, u32[]{:S(2)}, u32[]{:S(2)}) async-start(bf16[4,32,512]{2,1,0:T(8,128)(2,1)} %bitcast.155), calls=%async_computation.1 | async-start | bytes 262144 | tf_op jit(solution)/shard_map/all_to_all | solution.py:33
  64.6 3.7 %copy-start.2 = (bf16[1,2048,512]{2,1,0:T(8,128)(2,1)S(1)}, bf16[1,2048,512]{2,1,0:T(8,128)(2,1)}, u32[]{:S(2)}) copy-start(bf16[1,2048,512]{2,1,0:T(8,128)(2,1)} %param.35) | copy-start | bytes 6291460
  68.3 21.5 %copy-start.9 = (f32[32,4]{0,1:T(4,128)S(1)}, f32[32,4]{0,1:T(4,128)}, u32[]{:S(2)}) copy-start(f32[32,4]{0,1:T(4,128)} %param.34) | copy-start | bytes 1540
  72.4 17.4 %all-to-all-start.3 = ((bf16[128,2,512]{2,1,0:T(2,128)(2,1)}), bf16[128,2,512]{2,1,0:T(2,128)(2,1)S(1)}, u32[]{:S(2)}, u32[]{:S(2)}) async-start(bf16[128,2,512]{2,1,0:T(2,128)(2,1)} %bitcast.28), calls=%async_computation.3 | async-start | bytes 524288 | tf_op jit(solution)/shard_map/all_to_all | solution.py:189

commit v2 on v0

v2 whole, which is shorter than its diff:
```python
import jax
import jax.numpy as jnp
from jax import lax
from jax.experimental import pallas as pl
from jax.experimental.pallas import tpu as pltpu
from jax.sharding import PartitionSpec as P

epsilon = 1e-06
neg_fill = -1e30
SPAN = 512


def attend_kernel(
    lengths_hbm,
    lambdas_hbm,
    tokens_hbm,
    gain_hbm,
    w_query_hbm,
    w_key_hbm,
    w_value_hbm,
    head_gain_hbm,
    routing_hbm,
    route_weights_hbm,
    kv_hbm,
    message,
    heads,
    combine,
    kv,
    lengths,
    lambdas,
    tokens,
    gain,
    w_query,
    w_key,
    w_value,
    head_gain,
    routing,
    route_weights,
    q8,
    n4,
    spread,
    scores,
    turned,
    mix,
    sems,
    kv_sems,
):
    seqs, _ = tokens.shape
    cache_len = kv.shape[1]
    place = (lax.axis_index("ep"), lax.axis_index("tp"))
    spans = cache_len // SPAN
    rows_all = seqs * 4

    def kv_copy(i):
        part = pl.ds(i * SPAN, SPAN)
        return pltpu.make_async_copy(kv_hbm.at[:, part], kv.at[:, part], kv_sems.at[i])

    base = pl.multiple_of((place[0] // 4) * 128, 128)
    loads = [
        pltpu.make_async_copy(src, dst, sems.at[i])
        for i, (src, dst) in enumerate(
            [
                (tokens_hbm, tokens),
                (gain_hbm, gain),
                (w_query_hbm, w_query),
                (w_key_hbm, w_key),
                (w_value_hbm, w_value),
                (head_gain_hbm, head_gain),
                (routing_hbm.at[:, pl.ds(base, 128)], routing),
                (route_weights_hbm, route_weights),
                (lengths_hbm, lengths),
                (lambdas_hbm, lambdas),
            ]
        )
    ]
    for load in loads:
        load.start()
    for i in range(spans):
        kv_copy(i).start()

    lane = lax.broadcasted_iota(jnp.int32, (1, 128), 1)
    loads[0].wait()
    loads[1].wait()
    wide = tokens[...].astype(jnp.float32)
    scale = lax.rsqrt(jnp.mean(wide * wide, axis=1, keepdims=True) + epsilon)
    normed = (wide * scale * gain[...]).astype(jnp.bfloat16)
    for load in loads[2:]:
        load.wait()

    def rounded(value):
        return value.astype(jnp.bfloat16).astype(jnp.float32)

    def against(weight):
        return rounded(
            lax.dot_general(
                normed,
                weight[...],
                (((1,), (1,)), ((), ())),
                preferred_element_type=jnp.float32,
            )
        )

    queries = rounded(jnp.dot(normed, w_query[...], preferred_element_type=jnp.float32))
    new_row = jnp.concatenate([against(w_key), against(w_value)], axis=1)
    for head in range(4):
        pair = queries[:, 128 * (head // 2) : 128 * (head // 2) + 128]
        if head % 2:
            pair = pltpu.roll(pair, 64, 1)
        for half in range(2):
            own = (lane >= 32 * half) & (lane < 32 * half + 32)
            q8[pl.ds(half * rows_all + head, seqs, stride=4), :] = jnp.where(own, pair, 0.0)
        n4[pl.ds(head, seqs, stride=4), :] = new_row
    query_t = [q8[half * rows_all : (half + 1) * rows_all, :].T for half in range(2)]
    fresh = n4[...]
    fresh_t = fresh.T
    lane_seq = lax.broadcasted_iota(jnp.int32, (64, 128), 1) // 4
    for half in range(2):
        for s in range(seqs):
            spread[s * 64 : (s + 1) * 64, half * 128 : half * 128 + 128] = jnp.where(
                lane_seq == s, query_t[half][:64], 0.0
            ).astype(jnp.bfloat16)

    shift = 128 - (place[0] % 4) * 32
    named = jnp.where(lane < seqs, pltpu.roll(routing[...], shift, 1), -1)
    slot_row = lax.broadcasted_iota(jnp.int32, (256, 128), 0)
    slot_expert = slot_row // 2
    any_at = slot_expert == named[0:1, :]
    for k in range(1, 4):
        any_at = any_at | (slot_expert == named[k : k + 1, :])
    at_row = lax.broadcasted_iota(jnp.int32, (128, 128), 0)
    at_column = lax.broadcasted_iota(jnp.int32, (128, 128), 1)
    before = (at_row < at_column).astype(jnp.float32).astype(jnp.bfloat16)
    rank = jnp.dot(
        any_at.astype(jnp.float32).astype(jnp.bfloat16),
        before,
        preferred_element_type=jnp.float32,
    )
    parity = (slot_row % 2).astype(jnp.float32)
    taken = any_at & (rank == parity)
    picks = jnp.where(taken, 1.0, 0.0).astype(jnp.bfloat16)[:, :seqs]
    amount = jnp.zeros((256, 128), jnp.float32)
    widths = jnp.concatenate([route_weights[...]] * 4, axis=1)
    for k in range(4):
        amount = jnp.where(slot_expert == named[k : k + 1, :], widths[k : k + 1, :], amount)
    amount = jnp.where(taken, amount, 0.0).T[:seqs, :]
    for k in range(3):
        term = amount.astype(jnp.bfloat16)
        combine[k * seqs : (k + 1) * seqs, :] = term
        amount = amount - term.astype(jnp.float32)

    scaling = 32 ** (-0.5)
    count = jnp.zeros((1, 128), jnp.int32)
    for s in range(seqs):
        count = jnp.where(lane // 4 == s, lengths[s], count)
    count = jnp.concatenate([count, count], axis=1)
    lam = jnp.zeros((1, 128), jnp.float32)
    for head in range(4):
        lam = jnp.where(lane % 4 == head, lambdas[head], lam)
    score_new = [
        jnp.sum(query_t[half] * fresh_t, axis=0, keepdims=True) * scaling for half in range(2)
    ]
    score_new = jnp.concatenate(score_new, axis=1)

    position = lax.broadcasted_iota(jnp.int32, (SPAN, 256), 0)
    highest = score_new
    for i in range(spans):
        kv_copy(i).wait()
        cut = slice(i * SPAN, (i + 1) * SPAN)
        part = jnp.concatenate([kv[s, cut, :64] for s in range(seqs)], axis=1)
        found = jnp.dot(part, spread[...], preferred_element_type=jnp.float32) * scaling
        found = jnp.where(position < count - i * SPAN, found, neg_fill)
        scores[i * SPAN : (i + 1) * SPAN, :] = found
        highest = jnp.maximum(highest, jnp.max(found, axis=0, keepdims=True))
    expo_new = jnp.exp(score_new - highest)
    total = expo_new
    for i in range(spans):
        found = scores[i * SPAN : (i + 1) * SPAN, :]
        expo = jnp.where(position < count - i * SPAN, jnp.exp(found - highest), 0.0)
        scores[i * SPAN : (i + 1) * SPAN, :] = expo
        total = total + jnp.sum(expo, axis=0, keepdims=True)
    factor = 1.0 / total
    first = factor[:, :128]
    second = lam * factor[:, 128:]
    for i in range(cache_len // 128):
        expo = scores[i * 128 : (i + 1) * 128, :]
        weight = expo[:, :128] * first - expo[:, 128:] * second
        turned[:, i * 128 : (i + 1) * 128] = weight.T.astype(jnp.bfloat16)
    weight_new = expo_new[:, :128] * first - expo_new[:, 128:] * second
    diagonal = jnp.where(at_row == at_column, weight_new, 0.0).astype(jnp.bfloat16)
    mix_new = jnp.dot(diagonal, fresh.astype(jnp.bfloat16), preferred_element_type=jnp.float32)
    upper = lax.broadcasted_iota(jnp.int32, (8, 1), 0) < 4
    for i in range(seqs // 2):
        both = jnp.concatenate([kv[2 * i], kv[2 * i + 1]], axis=1)
        out = jnp.dot(turned[8 * i : 8 * i + 8, :], both, preferred_element_type=jnp.float32)
        mix[8 * i : 8 * i + 8, :] = jnp.where(upper, out[:, :128], out[:, 128:])

    blend = mix[...] + mix_new
    values = jnp.where(lane >= 64, blend, 0.0)
    power = jnp.sum(values * values, axis=1, keepdims=True) * (1.0 / 64)
    gain2 = jnp.concatenate([head_gain[...], head_gain[...]], axis=1)
    mix[...] = blend * lax.rsqrt(power + epsilon) * gain2
    pieces = []
    for pair in range(2):
        even = mix[pl.ds(2 * pair, seqs, stride=4), :]
        odd = mix[pl.ds(2 * pair + 1, seqs, stride=4), :]
        both = jnp.where(lane < 64, pltpu.roll(even, 64, 1), odd).astype(jnp.bfloat16)
        heads[:, 128 * pair : 128 * pair + 128] = both
        pieces.append(both)
    first = pl.multiple_of(place[1] * 512, 128)
    share = tokens[:, pl.ds(first, 512)]
    source = jnp.concatenate(pieces + [share], axis=1)
    packed = jnp.dot(picks, source, preferred_element_type=jnp.float32).astype(jnp.bfloat16)
    for b in range(6):
        message[b] = packed[:, 128 * b : 128 * b + 128]


def in_hbm(*arrays):
    return [pltpu.with_memory_space_constraint(array, pltpu.HBM) for array in arrays]


def attend(
    tokens, kv_cache, lengths, gain, w_query, w_key, w_value, lambdas, head_gain, routing,
    route_weights,
):
    seqs, width = tokens.shape
    vmem = pl.BlockSpec(memory_space=pltpu.VMEM)
    hbm = pl.BlockSpec(memory_space=pltpu.HBM)
    bf16, f32 = jnp.bfloat16, jnp.float32
    return pl.pallas_call(
        attend_kernel,
        out_shape=(
            jax.ShapeDtypeStruct((6, 256, 128), bf16),
            jax.ShapeDtypeStruct((seqs, 256), bf16),
            jax.ShapeDtypeStruct((3 * seqs, 256), bf16),
        ),
        in_specs=[hbm] * 11,
        out_specs=(vmem, vmem, vmem),
        scratch_shapes=[
            pltpu.VMEM(kv_cache.shape, bf16),
            pltpu.SMEM((seqs,), jnp.int32),
            pltpu.SMEM((4,), f32),
            pltpu.VMEM((seqs, width), bf16),
            pltpu.VMEM((1, width), f32),
            pltpu.VMEM((width, 256), bf16),
            pltpu.VMEM((64, width), bf16),
            pltpu.VMEM((64, width), bf16),
            pltpu.VMEM((1, 64), f32),
            pltpu.VMEM((4, 128), jnp.int32),
            pltpu.VMEM((4, seqs), f32),
            pltpu.VMEM((seqs * 8, 128), f32),
            pltpu.VMEM((seqs * 4, 128), f32),
            pltpu.VMEM((seqs * 64, 256), bf16),
            pltpu.VMEM((kv_cache.shape[1], 256), f32),
            pltpu.VMEM((128, kv_cache.shape[1]), bf16),
            pltpu.VMEM((seqs * 4, 128), f32),
            pltpu.SemaphoreType.DMA((10,)),
            pltpu.SemaphoreType.DMA((kv_cache.shape[1] // SPAN,)),
        ],
        compiler_params=pltpu.CompilerParams(vmem_limit_bytes=24 * 1024 * 1024),
        name="attend",
    )(
        *in_hbm(
            lengths,
            lambdas,
            tokens,
            gain.reshape(1, -1),
            w_query,
            w_key.T,
            w_value.T,
            head_gain.reshape(1, -1),
            routing.T,
            route_weights.T,
            kv_cache,
        )
    )


def expert_kernel(
    rows,
    own_heads,
    heads_1,
    heads_2,
    heads_3,
    tokens,
    ffn_gain,
    w_gate,
    w_shared_gate,
    w_shared_up,
    w_out_hbm,
    w_up_hbm,
    w_down_hbm,
    w_shared_down_hbm,
    results,
    base,
    part_1,
    part_2,
    part_3,
    heads,
    partial,
    resid,
    w_out,
    w_up,
    w_down,
    w_shared_down,
    sems,
):
    slots = rows.shape[1]
    cuts = [pl.ds(256 * t, 256) for t in range(4)]
    loads = [(w_out_hbm.at[cut], w_out.at[cut]) for cut in cuts]
    loads += [(w_up_hbm.at[0], w_up), (w_down_hbm.at[0], w_down)]
    loads += [(w_shared_down_hbm, w_shared_down)]
    loads = [
        pltpu.make_async_copy(source, target, sems.at[i])
        for i, (source, target) in enumerate(loads)
    ]
    for load in loads:
        load.start()
    tp = lax.axis_index("tp")
    heads[tp] = own_heads[...]
    for k, got in enumerate((heads_1, heads_2, heads_3)):
        heads[(tp + 3 - k) % 4] = got[...]
    total = None
    for t in range(4):
        arrived = jnp.concatenate([rows[6 * t], rows[6 * t + 1]], axis=1)
        both = jnp.concatenate([arrived, heads[t]], axis=0)
        loads[t].wait()
        piece = jnp.dot(
            both, w_out[256 * t : 256 * t + 256, :], preferred_element_type=jnp.float32
        )
        piece = piece.astype(jnp.bfloat16).astype(jnp.float32)
        total = piece if total is None else total + piece
    row_tokens = jnp.concatenate([rows[6 * t + b] for t in range(4) for b in range(2, 6)], axis=1)
    all_tokens = jnp.concatenate([row_tokens, tokens[...]], axis=0)
    residual = (all_tokens.astype(jnp.float32) + total).astype(jnp.bfloat16)
    resid[...] = residual[slots:]
    wide = residual.astype(jnp.float32)
    scale = lax.rsqrt(jnp.mean(wide * wide, axis=1, keepdims=True) + epsilon)
    ffn_in = (wide * scale * ffn_gain[...]).astype(jnp.bfloat16)

    def gated(value, gate, up):
        gate_part = jnp.dot(value, gate, preferred_element_type=jnp.float32)
        up_part = jnp.dot(value, up, preferred_element_type=jnp.float32)
        return (gate_part / (1.0 + jnp.exp(-gate_part)) * up_part).astype(jnp.bfloat16)

    loads[4].wait()
    act = gated(ffn_in[:slots], w_gate[0], w_up[...])
    shared_act = gated(ffn_in[slots:], w_shared_gate[...], w_shared_up[...])
    loads[5].wait()
    result = jnp.dot(act, w_down[...], preferred_element_type=jnp.float32).astype(jnp.bfloat16)
    for b in range(16):
        results[b] = result[:, 128 * b : 128 * b + 128]
    loads[6].wait()
    partial[...] = jnp.dot(shared_act, w_shared_down[...], preferred_element_type=jnp.float32)

    def share(source, shift):
        at = pl.multiple_of(((tp + shift) % 4) * 512, 512)
        return source[:, pl.ds(at, 512)]

    base[...] = share(partial, 0) + share(resid, 0).astype(jnp.float32)
    for k, part in enumerate((part_1, part_2, part_3)):
        part[...] = share(partial, k + 1).astype(jnp.bfloat16)


def run_experts(rows, own_heads, got_heads, tokens, ffn_gain, weights):
    w_out, w_gate, w_up, w_down, w_shared_gate, w_shared_up, w_shared_down = weights
    seqs, width = tokens.shape
    vmem = pl.BlockSpec(memory_space=pltpu.VMEM)
    bf16, f32 = jnp.bfloat16, jnp.float32
    part = jax.ShapeDtypeStruct((seqs, 512), bf16)
    return pl.pallas_call(
        expert_kernel,
        out_shape=(
            jax.ShapeDtypeStruct((16, 64, 128), bf16),
            jax.ShapeDtypeStruct((seqs, 512), f32),
            part,
            part,
            part,
        ),
        in_specs=[vmem] * 10 + [pl.BlockSpec(memory_space=pltpu.HBM)] * 4,
        out_specs=(vmem,) * 5,
        scratch_shapes=[
            pltpu.VMEM((4, seqs, 256), bf16),
            pltpu.VMEM((seqs, width), f32),
            pltpu.VMEM((seqs, width), bf16),
            pltpu.VMEM(w_out.shape, bf16),
            pltpu.VMEM(w_up.shape[1:], bf16),
            pltpu.VMEM(w_down.shape[1:], bf16),
            pltpu.VMEM(w_shared_down.shape, bf16),
            pltpu.SemaphoreType.DMA((7,)),
        ],
        compiler_params=pltpu.CompilerParams(vmem_limit_bytes=24 * 1024 * 1024),
        name="run_experts",
    )(
        rows,
        own_heads,
        *got_heads,
        tokens,
        ffn_gain.reshape(1, -1),
        w_gate,
        w_shared_gate,
        w_shared_up,
        *in_hbm(w_out, w_up, w_down, w_shared_down),
    )


def finish_kernel(combine, returned, base, part_1, part_2, part_3, mixed):
    seqs = base.shape[0]
    total = base[...]
    for part in (part_1, part_2, part_3):
        total = total + part[...].astype(jnp.float32)
    arrived = jnp.concatenate([returned[b] for b in range(4)], axis=1)
    routed = jnp.dot(combine[...], arrived, preferred_element_type=jnp.float32)
    for k in range(3):
        total = total + routed[k * seqs : (k + 1) * seqs, :]
    mixed[...] = total.astype(jnp.bfloat16)


def finish(combine, returned, base, parts):
    vmem = pl.BlockSpec(memory_space=pltpu.VMEM)
    return pl.pallas_call(
        finish_kernel,
        out_shape=jax.ShapeDtypeStruct(base.shape, jnp.bfloat16),
        in_specs=[vmem] * 6,
        out_specs=vmem,
        compiler_params=pltpu.CompilerParams(vmem_limit_bytes=4 * 1024 * 1024),
        name="finish",
    )(combine, returned, base, *parts)


def around(value, shift):
    count = lax.axis_size("tp")
    return lax.ppermute(value, "tp", [(i, (i + shift) % count) for i in range(count)])


def shards(
    tokens,
    kv_cache,
    lengths,
    attn_gain,
    w_query,
    w_key,
    w_value,
    lambdas,
    head_gain,
    w_out,
    ffn_gain,
    w_shared_gate,
    w_shared_up,
    w_shared_down,
    routing,
    route_weights,
    w_exp_gate,
    w_exp_up,
    w_exp_down,
):
    everyone = ("ep", "tp")
    message, heads, combine = attend(
        tokens,
        kv_cache,
        lengths,
        attn_gain,
        w_query,
        w_key,
        w_value,
        lambdas,
        head_gain,
        routing,
        route_weights,
    )
    message = message.reshape(6, 128, 2, 128).transpose(1, 0, 2, 3)
    arrived = lax.all_to_all(message, everyone, split_axis=0, concat_axis=0, tiled=True)
    got_heads = [around(heads, k) for k in range(1, 4)]
    rows = arrived.reshape(32, 4, 6, 2, 128).transpose(1, 2, 0, 3, 4).reshape(24, 64, 128)
    results, base, *parts = run_experts(
        rows,
        heads,
        got_heads,
        tokens,
        ffn_gain,
        (w_out, w_exp_gate, w_exp_up, w_exp_down, w_shared_gate, w_shared_up, w_shared_down),
    )
    results = results.reshape(4, 4, 32, 2, 128).transpose(2, 0, 1, 3, 4)
    results = results.reshape(128, 4, 2, 128)
    returned = lax.all_to_all(results, everyone, split_axis=0, concat_axis=0, tiled=True)
    parts = [around(part, k + 1) for k, part in enumerate(parts)]
    returned = returned.transpose(1, 0, 2, 3).reshape(4, 256, 128)
    return finish(combine, returned, base, parts)


def solution(mesh):
    return jax.shard_map(
        shards,
        mesh=mesh,
        in_specs=(
            P("ep", None),
            P("ep", None, "tp"),
            P("ep"),
            P(),
            P(None, "tp"),
            P(None, "tp"),
            P(None, "tp"),
            P("tp"),
            P(),
            P(),
            P(),
            P(None, "tp"),
            P(None, "tp"),
            P("tp", None),
            P(),
            P("ep", None),
            P(("ep", "tp"), None, None),
            P(("ep", "tp"), None, None),
            P(("ep", "tp"), None, None),
        ),
        out_specs=P("ep", "tp"),
        check_vma=False,
    )
```

time: 91.5 us -> 58.5 us (0.64)
  matrix products: 19.3 us -> 0 us
  blocking collectives: 18.9 us -> 0 us
  local copies, waits for them, and re-layouts: 19.3 us -> 3.57 us
  Pallas kernels: 0 us -> 14.6 us
  starting transfers between devices: 11.9 us -> 24.4 us
  other arithmetic: 4.63 us -> 0 us
    dot_general x13 -> x0, matrix products: 19.3 us -> none  [the longest x1 3.87 us: attention(): jnp.einsum('skgc,sckv->skgv', weight_old, values_old, preferred_element_t...]
    all_to_all x1 -> x0, blocking collectives: 18.9 us -> none  [shards(): lax.all_to_all(packed, 'ep', split_axis=0, concat_axis=0, tiled=True)]
    pallas_call x0 -> x3, Pallas kernels: none -> 14.6 us  [the longest x1 9.16 us: attend(): pl.pallas_call(attend_kernel, out_shape=(jax.ShapeDtypeStruct((6, 256, 12...]
    unnamed x20 -> x12, local copies, waits for them, and re-layouts: 12.1 us -> 0.04 us
    ppermute x0 -> x6, starting transfers between devices: none -> 8.78 us  [around(): lax.ppermute(value, 'tp', [(i, (i + shift) % count) for i in range(count)])]
    all_to_all x3 -> x2, starting transfers between devices: 11.9 us -> 15.7 us  [the longest x1 11.9 us: shards(): lax.all_to_all(message, everyone, split_axis=0, concat_axis=0, tiled=True)]
    reduce_sum x7 -> x0, other arithmetic: 3.4 us -> none  [the longest x1 1.7 us: attention(): totals = jnp.sum(expo_old, axis=-1) + expo_new]
    slice x1 -> x0, local copies, waits for them, and re-layouts: 2.65 us -> none  [attention(): layout[..., :v_width].reshape(seq_count, cache_len, kv_local, 2, qk_width)]
  transfers between devices with their start and end apart: 3 -> 8, of which waited for: 3 -> 2; matrix products, arithmetic and copies ran while one was open for 2% -> 3% of each run, Pallas kernels for 0% -> 0%
where the time goes in v2:
time: 58.5 us; the launch traced here: 58.2 us
  starting transfers between devices  24.4 us (42%)
  waiting for transfers between devices  15.5 us (26%)
  Pallas kernels  14.6 us (25%)
  local copies, waits for them, and re-layouts  3.57 us (6%)
    all_to_all x1, starting transfers between devices, shards(): lax.all_to_all(message, everyone, split_axis=0, concat_axis=0, tiled=True)  11.9 us
    pallas_call x1, Pallas kernels, attend(): pl.pallas_call(attend_kernel, out_shape=(jax.ShapeDtypeStruct((6, 256, 12...  9.16 us
    ppermute x6, starting transfers between devices, around(): lax.ppermute(value, 'tp', [(i, (i + shift) % count) for i in range(count)])  8.78 us
    all_to_all x1, waiting for transfers between devices, shards(): lax.all_to_all(message, everyone, split_axis=0, concat_axis=0, tiled=True)  8.77 us
    all_to_all x1, waiting for transfers between devices, shards(): lax.all_to_all(results, everyone, split_axis=0, concat_axis=0, tiled=True)  6.67 us
    pallas_call x1, Pallas kernels, run_experts(): pl.pallas_call(expert_kernel, out_shape=(jax.ShapeDtypeStruct((16, 64, 12...  4.63 us
    all_to_all x1, starting transfers between devices, shards(): lax.all_to_all(results, everyone, split_axis=0, concat_axis=0, tiled=True)  3.78 us
  transfers between devices with their start and end apart: 8, of which 2 were waited for; matrix products, arithmetic and copies ran while one was open for 3% of the time, Pallas kernels for 0%

profile of v2, /device:TPU:1, one launch (start us, length us, event | category | flops | bytes accessed | tf_op | source)
XLA Modules:
  0.0 58.2 jit_solution(13250636962672885392)
XLA Ops:
  0.0 9.2 %attend.1 = (bf16[6,256,128]{2,1,0:T(8,128)(2,1)S(1)}, bf16[32,256]{1,0:T(8,128)(2,1)S(1)}, bf16[96,256]{1,0:T(8,128)(2,1)S(1)}) custom-call(s32[32]{0:T(128)} %lengths_hbm.1, f32[4]{0:T(128)} %lambdas_hbm.1, bf16[32,2048]{1,0:T(8,128)(2,1)} %tokens.1, f32[1,2048]{1,0:T(1,128)} %bitcast.32, bf16[2048,256]{1,0:T(8,128)(2,1)} %w_query_hbm.1, ...), custom_call_target="tpu_custom_call" | custom-call | tf_op jit(solution)/shard_map/attend/pallas_call | solution.py:229
  9.2 0.0 copy-start
  9.2 0.0 copy-start.1
  9.2 0.0 copy-start.2
  9.2 0.0 copy-start.4
  9.2 1.0 %copy.30 = bf16[6,128,2,128]{3,2,0,1:T(2,128)(2,1)} copy(bf16[6,128,2,128]{3,2,1,0:T(2,128)(2,1)S(1)} %bitcast.23) | data formatting | bytes 786432 | tf_op jit(solution)/shard_map/reshape | solution.py:470
  10.2 11.9 %all-to-all-start = ((bf16[128,6,2,128]{3,2,1,0:T(2,128)(2,1)}), bf16[128,6,2,128]{3,2,1,0:T(2,128)(2,1)}, u32[]{:S(2)}, u32[]{:S(2)}) async-start(bf16[128,6,2,128]{3,2,1,0:T(2,128)(2,1)} %bitcast.26), calls=%async_computation | async-start | bytes 786432 | tf_op jit(solution)/shard_map/all_to_all | solution.py:471
  22.1 2.6 %collective-permute-start.2 = (bf16[32,256]{1,0:T(8,128)(2,1)S(1)}, bf16[32,256]{1,0:T(8,128)(2,1)S(1)}, u32[]{:S(2)}, u32[]{:S(2)}) collective-permute-start(bf16[32,256]{1,0:T(8,128)(2,1)S(1)} %get-tuple-element.15.own_heads), channel_id=1, source_target_pairs={{0,3},{1,0},{2,1},{3,2},{4,7},{5,4},{6,5},{7,6},{8,11},{9,8},{10,9... | collective-permute-start | bytes 49160 | tf_op jit(solution)/shard_map/ppermute | solution.py:432
  24.8 0.6 collective-permute-start.1
  25.3 0.6 collective-permute-start
  25.9 8.8 %all-to-all-done = bf16[128,6,2,128]{3,2,1,0:T(2,128)(2,1)} async-done(((bf16[128,6,2,128]{3,2,1,0:T(2,128)(2,1)}), bf16[128,6,2,128]{3,2,1,0:T(2,128)(2,1)}, u32[]{:S(2)}, u32[]{:S(2)}) %all-to-all-start) | async-done | bytes 393248 | tf_op jit(solution)/shard_map/all_to_all | solution.py:471
  34.7 1.1 %copy.25 = bf16[128,6,2,128]{3,0,2,1:T(8,128)(2,1)S(1)} copy(bf16[128,6,2,128]{3,2,1,0:T(2,128)(2,1)} %all-to-all-done) | data formatting | bytes 786432 | tf_op jit(solution)/shard_map/all_to_all | solution.py:471
  35.7 0.4 copy.26
  36.2 0.0 collective-permute-done.2.heads_3
  36.2 0.0 collective-permute-done.1.heads_2
  36.2 0.0 collective-permute-done.heads_1
  36.2 0.0 copy-done.3
  36.2 0.0 copy-done
  36.2 0.0 copy-done.1
  36.2 4.6 %run_experts.1 = (bf16[16,64,128]{2,1,0:T(8,128)(2,1)S(1)}, f32[32,512]{1,0:T(8,128)S(1)}, bf16[32,512]{1,0:T(8,128)(2,1)S(1)}, bf16[32,512]{1,0:T(8,128)(2,1)S(1)}, bf16[32,512]{1,0:T(8,128)(2,1)S(1)}) custom-call(bf16[24,64,128]{2,1,0:T(8,128)(2,1)S(1)} %bitcast.21, bf16[32,256]{1,0:T(8,128)(2,1)S(1)} %get-tuple-element.15.own_heads, ...), custom_call_target="tpu_custom_call" | custom-call | tf_op jit(solution)/shard_map/run_experts/pallas_call | solution.py:370
  40.9 0.0 copy-start.5
  40.9 0.9 %copy.27 = bf16[32,4,4,2,128]{4,3,2,1,0:T(2,128)(2,1)} copy(bf16[32,4,4,2,128]{4,3,0,2,1:T(2,128)(2,1)S(1)} %bitcast.24) | data formatting | bytes 524288 | tf_op jit(solution)/shard_map/transpose | solution.py:482
  41.8 3.8 %all-to-all-start.1 = ((bf16[128,4,2,128]{3,2,1,0:T(2,128)(2,1)}), bf16[128,4,2,128]{3,2,1,0:T(2,128)(2,1)S(1)}, u32[]{:S(2)}, u32[]{:S(2)}) async-start(bf16[128,4,2,128]{3,2,1,0:T(2,128)(2,1)} %bitcast.14), calls=%async_computation.1 | async-start | bytes 524288 | tf_op jit(solution)/shard_map/all_to_all | solution.py:484
  45.5 1.4 %collective-permute-start.3 = (bf16[32,512]{1,0:T(8,128)(2,1)}, bf16[32,512]{1,0:T(8,128)(2,1)S(1)}, u32[]{:S(2)}, u32[]{:S(2)}) collective-permute-start(bf16[32,512]{1,0:T(8,128)(2,1)} %copy-done.5), channel_id=1, source_target_pairs={{0,1},{1,2},{2,3},{3,0},{4,5},{5,6},{6,7},{7,4},{8,9},{9,10},{10,1... | collective-permute-start | bytes 98312 | tf_op jit(solution)/shard_map/ppermute | solution.py:432
  47.0 2.4 %collective-permute-start.4 = (bf16[32,512]{1,0:T(8,128)(2,1)S(1)}, bf16[32,512]{1,0:T(8,128)(2,1)S(1)}, u32[]{:S(2)}, u32[]{:S(2)}) collective-permute-start(bf16[32,512]{1,0:T(8,128)(2,1)S(1)} %get-tuple-element.19), channel_id=1, source_target_pairs={{0,2},{1,3},{2,0},{3,1},{4,6},{5,7},{6,4},{7,5},{8,10},{9,11},{10,... | collective-permute-start | bytes 98312 | tf_op jit(solution)/shard_map/ppermute | solution.py:432
  49.4 1.2 %collective-permute-start.5 = (bf16[32,512]{1,0:T(8,128)(2,1)S(1)}, bf16[32,512]{1,0:T(8,128)(2,1)S(1)}, u32[]{:S(2)}, u32[]{:S(2)}) collective-permute-start(bf16[32,512]{1,0:T(8,128)(2,1)S(1)} %get-tuple-element.20), channel_id=1, source_target_pairs={{0,3},{1,0},{2,1},{3,2},{4,7},{5,4},{6,5},{7,6},{8,11},{9,8},{10,9... | collective-permute-start | bytes 98312 | tf_op jit(solution)/shard_map/ppermute | solution.py:432
  50.5 6.7 %all-to-all-done.1 = bf16[128,4,2,128]{3,2,1,0:T(2,128)(2,1)S(1)} async-done(((bf16[128,4,2,128]{3,2,1,0:T(2,128)(2,1)}), bf16[128,4,2,128]{3,2,1,0:T(2,128)(2,1)S(1)}, u32[]{:S(2)}, u32[]{:S(2)}) %all-to-all-start.1) | async-done | bytes 262176 | tf_op jit(solution)/shard_map/all_to_all | solution.py:484
  57.2 0.2 copy.28
  57.4 0.0 collective-permute-done.3.part_1
  57.4 0.0 collective-permute-done.4.part_2
  57.4 0.0 collective-permute-done.5.part_3
  57.4 0.8 %finish.1 = bf16[32,512]{1,0:T(8,128)(2,1)} custom-call(bf16[96,256]{1,0:T(8,128)(2,1)S(1)} %get-tuple-element.13.combine, bf16[4,256,128]{2,1,0:T(8,128)(2,1)S(1)} %bitcast.22, f32[32,512]{1,0:T(8,128)S(1)} %get-tuple-element.17.base, bf16[32,512]{1,0:T(8,128)(2,1)S(1)} %collective-permute-done.3.part_1, bf16[32,512]{1,0:T(8,128)(2,1)S(1)} %collective-permute-done.4.part_2, ...), custom_call_target="tpu_custom_call" | custom-call | tf_op jit(solution)/shard_map/finish/pallas_call | solution.py:420
  (4 shorter events, 0.0 us)
Async XLA Ops:
  0.0 36.2 %copy-start.3 = (bf16[32,2048]{1,0:T(8,128)(2,1)S(1)}, bf16[32,2048]{1,0:T(8,128)(2,1)}, u32[]{:S(2)}) copy-start(bf16[32,2048]{1,0:T(8,128)(2,1)} %tokens.1) | copy-start | bytes 393220
  9.2 27.0 %copy-start = (bf16[1,2048,512]{2,1,0:T(8,128)(2,1)S(1)}, bf16[1,2048,512]{2,1,0:T(8,128)(2,1)}, u32[]{:S(2)}) copy-start(bf16[1,2048,512]{2,1,0:T(8,128)(2,1)} %w_gate.1) | copy-start | bytes 6291460
  9.2 27.0 %copy-start.1 = (bf16[2048,128]{1,0:T(8,128)(2,1)S(1)}, bf16[2048,128]{1,0:T(8,128)(2,1)}, u32[]{:S(2)}) copy-start(bf16[2048,128]{1,0:T(8,128)(2,1)} %w_shared_gate.1) | copy-start | bytes 1572868
  9.2 27.0 %copy-start.2 = (bf16[2048,128]{1,0:T(8,128)(2,1)S(1)}, bf16[2048,128]{1,0:T(8,128)(2,1)}, u32[]{:S(2)}) copy-start(bf16[2048,128]{1,0:T(8,128)(2,1)} %w_shared_up.1) | copy-start | bytes 1572868
  9.2 27.0 %copy-start.4 = (f32[2048]{0:T(1024)S(1)}, f32[2048]{0:T(1024)}, u32[]{:S(2)}) copy-start(f32[2048]{0:T(1024)} %param.29) | copy-start | bytes 24580
  10.2 24.4 %all-to-all-start = ((bf16[128,6,2,128]{3,2,1,0:T(2,128)(2,1)}), bf16[128,6,2,128]{3,2,1,0:T(2,128)(2,1)}, u32[]{:S(2)}, u32[]{:S(2)}) async-start(bf16[128,6,2,128]{3,2,1,0:T(2,128)(2,1)} %bitcast.26), calls=%async_computation | async-start | bytes 786432 | tf_op jit(solution)/shard_map/all_to_all | solution.py:471
  22.1 14.0 %collective-permute-start.2 = (bf16[32,256]{1,0:T(8,128)(2,1)S(1)}, bf16[32,256]{1,0:T(8,128)(2,1)S(1)}, u32[]{:S(2)}, u32[]{:S(2)}) collective-permute-start(bf16[32,256]{1,0:T(8,128)(2,1)S(1)} %get-tuple-element.15.own_heads), channel_id=1, source_target_pairs={{0,3},{1,0},{2,1},{3,2},{4,7},{5,4},{6,5},{7,6},{8,11},{9,8},{10,9... | collective-permute-start | bytes 49160 | tf_op jit(solution)/shard_map/ppermute | solution.py:432
  24.8 11.4 %collective-permute-start.1 = (bf16[32,256]{1,0:T(8,128)(2,1)S(1)}, bf16[32,256]{1,0:T(8,128)(2,1)S(1)}, u32[]{:S(2)}, u32[]{:S(2)}) collective-permute-start(bf16[32,256]{1,0:T(8,128)(2,1)S(1)} %get-tuple-element.15.own_heads), channel_id=1, source_target_pairs={{0,2},{1,3},{2,0},{3,1},{4,6},{5,7},{6,4},{7,5},{8,10},{9,11},{10,... | collective-permute-start | bytes 49160 | tf_op jit(solution)/shard_map/ppermute | solution.py:432
  25.3 10.8 %collective-permute-start = (bf16[32,256]{1,0:T(8,128)(2,1)S(1)}, bf16[32,256]{1,0:T(8,128)(2,1)S(1)}, u32[]{:S(2)}, u32[]{:S(2)}) collective-permute-start(bf16[32,256]{1,0:T(8,128)(2,1)S(1)} %get-tuple-element.15.own_heads), channel_id=1, source_target_pairs={{0,1},{1,2},{2,3},{3,0},{4,5},{5,6},{6,7},{7,4},{8,9},{9,10},{10,1... | collective-permute-start | bytes 49160 | tf_op jit(solution)/shard_map/ppermute | solution.py:432
  40.9 0.9 %copy-start.5 = (bf16[32,512]{1,0:T(8,128)(2,1)}, bf16[32,512]{1,0:T(8,128)(2,1)S(1)}, u32[]{:S(2)}) copy-start(bf16[32,512]{1,0:T(8,128)(2,1)S(1)} %get-tuple-element.18) | copy-start | bytes 98308
  41.8 15.5 %all-to-all-start.1 = ((bf16[128,4,2,128]{3,2,1,0:T(2,128)(2,1)}), bf16[128,4,2,128]{3,2,1,0:T(2,128)(2,1)S(1)}, u32[]{:S(2)}, u32[]{:S(2)}) async-start(bf16[128,4,2,128]{3,2,1,0:T(2,128)(2,1)} %bitcast.14), calls=%async_computation.1 | async-start | bytes 524288 | tf_op jit(solution)/shard_map/all_to_all | solution.py:484
  45.5 11.9 %collective-permute-start.3 = (bf16[32,512]{1,0:T(8,128)(2,1)}, bf16[32,512]{1,0:T(8,128)(2,1)S(1)}, u32[]{:S(2)}, u32[]{:S(2)}) collective-permute-start(bf16[32,512]{1,0:T(8,128)(2,1)} %copy-done.5), channel_id=1, source_target_pairs={{0,1},{1,2},{2,3},{3,0},{4,5},{5,6},{6,7},{7,4},{8,9},{9,10},{10,1... | collective-permute-start | bytes 98312 | tf_op jit(solution)/shard_map/ppermute | solution.py:432
  47.0 10.4 %collective-permute-start.4 = (bf16[32,512]{1,0:T(8,128)(2,1)S(1)}, bf16[32,512]{1,0:T(8,128)(2,1)S(1)}, u32[]{:S(2)}, u32[]{:S(2)}) collective-permute-start(bf16[32,512]{1,0:T(8,128)(2,1)S(1)} %get-tuple-element.19), channel_id=1, source_target_pairs={{0,2},{1,3},{2,0},{3,1},{4,6},{5,7},{6,4},{7,5},{8,10},{9,11},{10,... | collective-permute-start | bytes 98312 | tf_op jit(solution)/shard_map/ppermute | solution.py:432
  49.4 8.1 %collective-permute-start.5 = (bf16[32,512]{1,0:T(8,128)(2,1)S(1)}, bf16[32,512]{1,0:T(8,128)(2,1)S(1)}, u32[]{:S(2)}, u32[]{:S(2)}) collective-permute-start(bf16[32,512]{1,0:T(8,128)(2,1)S(1)} %get-tuple-element.20), channel_id=1, source_target_pairs={{0,3},{1,0},{2,1},{3,2},{4,7},{5,4},{6,5},{7,6},{8,11},{9,8},{10,9... | collective-permute-start | bytes 98312 | tf_op jit(solution)/shard_map/ppermute | solution.py:432

commit v3 on v2

--- a/solution.py
+++ b/solution.py
@@ -8,6 +8,7 @@
 epsilon = 1e-06
 neg_fill = -1e30
 SPAN = 512
+VMEM_BYTES = 64 * 1024 * 1024 - 65536
 
 
 def attend_kernel(
@@ -23,8 +24,8 @@
     route_weights_hbm,
     kv_hbm,
     message,
-    heads,
-    combine,
+    heads_out,
+    combine_out,
     kv,
     lengths,
     lambdas,
@@ -42,8 +43,13 @@
     scores,
     turned,
     mix,
+    heads,
+    combine,
+    stage,
+    ready,
     sems,
     kv_sems,
+    send_sems,
 ):
     seqs, _ = tokens.shape
     cache_len = kv.shape[1]
@@ -122,31 +128,39 @@
 
     shift = 128 - (place[0] % 4) * 32
     named = jnp.where(lane < seqs, pltpu.roll(routing[...], shift, 1), -1)
-    slot_row = lax.broadcasted_iota(jnp.int32, (256, 128), 0)
-    slot_expert = slot_row // 2
-    any_at = slot_expert == named[0:1, :]
-    for k in range(1, 4):
-        any_at = any_at | (slot_expert == named[k : k + 1, :])
     at_row = lax.broadcasted_iota(jnp.int32, (128, 128), 0)
     at_column = lax.broadcasted_iota(jnp.int32, (128, 128), 1)
+    named_at = [at_row == named[k : k + 1, :] for k in range(4)]
+    any_at = named_at[0] | named_at[1] | named_at[2] | named_at[3]
     before = (at_row < at_column).astype(jnp.float32).astype(jnp.bfloat16)
     rank = jnp.dot(
         any_at.astype(jnp.float32).astype(jnp.bfloat16),
         before,
         preferred_element_type=jnp.float32,
     )
-    parity = (slot_row % 2).astype(jnp.float32)
-    taken = any_at & (rank == parity)
-    picks = jnp.where(taken, 1.0, 0.0).astype(jnp.bfloat16)[:, :seqs]
-    amount = jnp.zeros((256, 128), jnp.float32)
+    amount = jnp.zeros((128, 128), jnp.float32)
     widths = jnp.concatenate([route_weights[...]] * 4, axis=1)
     for k in range(4):
-        amount = jnp.where(slot_expert == named[k : k + 1, :], widths[k : k + 1, :], amount)
-    amount = jnp.where(taken, amount, 0.0).T[:seqs, :]
-    for k in range(3):
-        term = amount.astype(jnp.bfloat16)
-        combine[k * seqs : (k + 1) * seqs, :] = term
-        amount = amount - term.astype(jnp.float32)
+        amount = jnp.where(named_at[k], widths[k : k + 1, :], amount)
+    picks = []
+    for c in range(2):
+        taken = any_at & (rank == float(c))
+        picks.append(jnp.where(taken, 1.0, 0.0).astype(jnp.bfloat16)[:, :seqs])
+        own_amount = jnp.where(taken, amount, 0.0).T[:seqs, :]
+        for k in range(3):
+            term = own_amount.astype(jnp.bfloat16)
+            combine[k * seqs : (k + 1) * seqs, 128 * c : 128 * c + 128] = term
+            own_amount = own_amount - term.astype(jnp.float32)
+
+    def place_rows(source, first):
+        for c in range(2):
+            packed = jnp.dot(picks[c], source, preferred_element_type=jnp.float32)
+            for b in range(source.shape[1] // 128):
+                row = 2 * (first + b) + c
+                stage[pl.ds(row, 128, stride=12), :] = packed[:, 128 * b : 128 * b + 128]
+
+    share = tokens[:, pl.ds(pl.multiple_of(place[1] * 512, 128), 512)]
+    place_rows(share, 2)
 
     scaling = 32 ** (-0.5)
     count = jnp.zeros((1, 128), jnp.int32)
@@ -206,12 +220,23 @@
         both = jnp.where(lane < 64, pltpu.roll(even, 64, 1), odd).astype(jnp.bfloat16)
         heads[:, 128 * pair : 128 * pair + 128] = both
         pieces.append(both)
-    first = pl.multiple_of(place[1] * 512, 128)
-    share = tokens[:, pl.ds(first, 512)]
-    source = jnp.concatenate(pieces + [share], axis=1)
-    packed = jnp.dot(picks, source, preferred_element_type=jnp.float32).astype(jnp.bfloat16)
-    for b in range(6):
-        message[b] = packed[:, 128 * b : 128 * b + 128]
+    extra = [
+        pltpu.make_async_copy(heads, heads_out, send_sems.at[4]),
+        pltpu.make_async_copy(combine, combine_out, send_sems.at[5]),
+    ]
+    for send in extra:
+        send.start()
+    place_rows(jnp.concatenate(pieces, axis=1), 0)
+    sends = []
+    for i in range(4):
+        part = pl.ds(384 * i, 384)
+        ready[part, :] = stage[part, :].astype(jnp.bfloat16)
+        sends.append(
+            pltpu.make_async_copy(ready.at[part], message.at[part], send_sems.at[i])
+        )
+        sends[i].start()
+    for send in sends + extra:
+        send.wait()
 
 
 def in_hbm(*arrays):
@@ -223,18 +248,17 @@
     route_weights,
 ):
     seqs, width = tokens.shape
-    vmem = pl.BlockSpec(memory_space=pltpu.VMEM)
     hbm = pl.BlockSpec(memory_space=pltpu.HBM)
     bf16, f32 = jnp.bfloat16, jnp.float32
     return pl.pallas_call(
         attend_kernel,
         out_shape=(
-            jax.ShapeDtypeStruct((6, 256, 128), bf16),
-            jax.ShapeDtypeStruct((seqs, 256), bf16),
-            jax.ShapeDtypeStruct((3 * seqs, 256), bf16),
+            pltpu.HBM((1536, 128), bf16),
+            pltpu.HBM((seqs, 256), bf16),
+            pltpu.HBM((3 * seqs, 256), bf16),
         ),
         in_specs=[hbm] * 11,
-        out_specs=(vmem, vmem, vmem),
+        out_specs=(hbm, hbm, hbm),
         scratch_shapes=[
             pltpu.VMEM(kv_cache.shape, bf16),
             pltpu.SMEM((seqs,), jnp.int32),
@@ -253,10 +277,15 @@
             pltpu.VMEM((kv_cache.shape[1], 256), f32),
             pltpu.VMEM((128, kv_cache.shape[1]), bf16),
             pltpu.VMEM((seqs * 4, 128), f32),
+            pltpu.VMEM((seqs, 256), bf16),
+            pltpu.VMEM((3 * seqs, 256), bf16),
+            pltpu.VMEM((1536, 128), f32),
+            pltpu.VMEM((1536, 128), bf16),
             pltpu.SemaphoreType.DMA((10,)),
             pltpu.SemaphoreType.DMA((kv_cache.shape[1] // SPAN,)),
+            pltpu.SemaphoreType.DMA((6,)),
         ],
-        compiler_params=pltpu.CompilerParams(vmem_limit_bytes=24 * 1024 * 1024),
+        compiler_params=pltpu.CompilerParams(vmem_limit_bytes=VMEM_BYTES),
         name="attend",
     )(
         *in_hbm(
@@ -281,47 +310,78 @@
     heads_1,
     heads_2,
     heads_3,
-    tokens,
-    ffn_gain,
-    w_gate,
-    w_shared_gate,
-    w_shared_up,
+    tokens_hbm,
+    ffn_gain_hbm,
     w_out_hbm,
+    w_gate_hbm,
     w_up_hbm,
     w_down_hbm,
+    w_shared_gate_hbm,
+    w_shared_up_hbm,
     w_shared_down_hbm,
     results,
-    base,
+    base_out,
     part_1,
     part_2,
     part_3,
     heads,
+    base,
+    parts,
     partial,
     resid,
+    wide_rows,
+    stage,
+    ready,
+    tokens,
+    ffn_gain,
     w_out,
+    w_gate,
     w_up,
     w_down,
+    w_shared_gate,
+    w_shared_up,
     w_shared_down,
     sems,
+    head_sems,
+    send_sems,
 ):
-    slots = rows.shape[1]
-    cuts = [pl.ds(256 * t, 256) for t in range(4)]
-    loads = [(w_out_hbm.at[cut], w_out.at[cut]) for cut in cuts]
-    loads += [(w_up_hbm.at[0], w_up), (w_down_hbm.at[0], w_down)]
-    loads += [(w_shared_down_hbm, w_shared_down)]
+    slots = 64
+    quarters = [pl.ds(256 * t, 256) for t in range(4)]
+    tp = lax.axis_index("tp")
+    loads = [(w_out_hbm.at[quarter], w_out.at[quarter]) for quarter in quarters]
+    gathered = [(own_heads, heads.at[tp])]
+    for k, got in enumerate((heads_1, heads_2, heads_3)):
+        gathered.append((got, heads.at[(tp + 3 - k) % 4]))
+    gathered = [
+        pltpu.make_async_copy(source, target, head_sems.at[i])
+        for i, (source, target) in enumerate(gathered)
+    ]
+    for load in gathered:
+        load.start()
+    loads += [(tokens_hbm, tokens), (ffn_gain_hbm, ffn_gain)]
+    loads += [(w_gate_hbm.at[0], w_gate), (w_up_hbm.at[0], w_up)]
+    loads += [(w_shared_gate_hbm, w_shared_gate), (w_shared_up_hbm, w_shared_up)]
+    loads += [(w_down_hbm.at[0], w_down), (w_shared_down_hbm, w_shared_down)]
     loads = [
         pltpu.make_async_copy(source, target, sems.at[i])
         for i, (source, target) in enumerate(loads)
     ]
     for load in loads:
         load.start()
-    tp = lax.axis_index("tp")
-    heads[tp] = own_heads[...]
-    for k, got in enumerate((heads_1, heads_2, heads_3)):
-        heads[(tp + 3 - k) % 4] = got[...]
+    wide_rows[...] = rows[...].astype(jnp.float32)
+
+    def arrived_rows(t, b):
+        halves = [
+            wide_rows[pl.ds(12 * t + 2 * b + c, 32, stride=48), :].astype(jnp.bfloat16)
+            for c in range(2)
+        ]
+        return jnp.concatenate(halves, axis=0)
+
+    for load in gathered:
+        load.wait()
     total = None
     for t in range(4):
-        arrived = jnp.concatenate([rows[6 * t], rows[6 * t + 1]], axis=1)
+        arrived = jnp.concatenate([arrived_rows(t, 0), arrived_rows(t, 1)], axis=1)
         both = jnp.concatenate([arrived, heads[t]], axis=0)
         loads[t].wait()
         piece = jnp.dot(
@@ -329,7 +389,9 @@
         )
         piece = piece.astype(jnp.bfloat16).astype(jnp.float32)
         total = piece if total is None else total + piece
-    row_tokens = jnp.concatenate([rows[6 * t + b] for t in range(4) for b in range(2, 6)], axis=1)
+    row_tokens = jnp.concatenate([arrived_rows(t, b) for t in range(4) for b in range(2, 6)], axis=1)
+    loads[4].wait()
+    loads[5].wait()
     all_tokens = jnp.concatenate([row_tokens, tokens[...]], axis=0)
     residual = (all_tokens.astype(jnp.float32) + total).astype(jnp.bfloat16)
     resid[...] = residual[slots:]
@@ -342,14 +404,28 @@
         up_part = jnp.dot(value, up, preferred_element_type=jnp.float32)
         return (gate_part / (1.0 + jnp.exp(-gate_part)) * up_part).astype(jnp.bfloat16)
 
-    loads[4].wait()
-    act = gated(ffn_in[:slots], w_gate[0], w_up[...])
+    loads[6].wait()
+    loads[7].wait()
+    act = gated(ffn_in[:slots], w_gate[...], w_up[...])
+    loads[8].wait()
+    loads[9].wait()
     shared_act = gated(ffn_in[slots:], w_shared_gate[...], w_shared_up[...])
-    loads[5].wait()
-    result = jnp.dot(act, w_down[...], preferred_element_type=jnp.float32).astype(jnp.bfloat16)
+    loads[10].wait()
+    result = jnp.dot(act, w_down[...], preferred_element_type=jnp.float32)
     for b in range(16):
-        results[b] = result[:, 128 * b : 128 * b + 128]
-    loads[6].wait()
+        for c in range(2):
+            stage[pl.ds(2 * b + c, 32, stride=32), :] = result[
+                32 * c : 32 * c + 32, 128 * b : 128 * b + 128
+            ]
+    sends = []
+    for i in range(2):
+        half = pl.ds(512 * i, 512)
+        ready[half, :] = stage[half, :].astype(jnp.bfloat16)
+        sends.append(
+            pltpu.make_async_copy(ready.at[half], results.at[half], send_sems.at[i])
+        )
+        sends[i].start()
+    loads[11].wait()
     partial[...] = jnp.dot(shared_act, w_shared_down[...], preferred_element_type=jnp.float32)
 
     def share(source, shift):
@@ -357,8 +433,14 @@
         return source[:, pl.ds(at, 512)]
 
     base[...] = share(partial, 0) + share(resid, 0).astype(jnp.float32)
+    sends.append(pltpu.make_async_copy(base, base_out, send_sems.at[2]))
+    sends[2].start()
     for k, part in enumerate((part_1, part_2, part_3)):
-        part[...] = share(partial, k + 1).astype(jnp.bfloat16)
+        parts[k] = share(partial, k + 1).astype(jnp.bfloat16)
+        sends.append(pltpu.make_async_copy(parts.at[k], part, send_sems.at[3 + k]))
+        sends[3 + k].start()
+    for send in sends:
+        send.wait()
 
 
 def run_experts(rows, own_heads, got_heads, tokens, ffn_gain, weights):
@@ -366,50 +448,95 @@
     seqs, width = tokens.shape
     vmem = pl.BlockSpec(memory_space=pltpu.VMEM)
     bf16, f32 = jnp.bfloat16, jnp.float32
-    part = jax.ShapeDtypeStruct((seqs, 512), bf16)
+    part = pltpu.HBM((seqs, 512), bf16)
+    hbm = pl.BlockSpec(memory_space=pltpu.HBM)
+    either = pl.BlockSpec(memory_space=pl.ANY)
     return pl.pallas_call(
         expert_kernel,
         out_shape=(
-            jax.ShapeDtypeStruct((16, 64, 128), bf16),
-            jax.ShapeDtypeStruct((seqs, 512), f32),
+            pltpu.HBM((1024, 128), bf16),
+            pltpu.HBM((seqs, 512), f32),
             part,
             part,
             part,
         ),
-        in_specs=[vmem] * 10 + [pl.BlockSpec(memory_space=pltpu.HBM)] * 4,
-        out_specs=(vmem,) * 5,
+        in_specs=[vmem] + [either] * 4 + [hbm] * 9,
+        out_specs=(hbm,) * 5,
         scratch_shapes=[
             pltpu.VMEM((4, seqs, 256), bf16),
+            pltpu.VMEM((seqs, 512), f32),
+            pltpu.VMEM((3, seqs, 512), bf16),
             pltpu.VMEM((seqs, width), f32),
             pltpu.VMEM((seqs, width), bf16),
+            pltpu.VMEM((1536, 128), f32),
+            pltpu.VMEM((1024, 128), f32),
+            pltpu.VMEM((1024, 128), bf16),
+            pltpu.VMEM((seqs, width), bf16),
+            pltpu.VMEM((1, width), f32),
             pltpu.VMEM(w_out.shape, bf16),
+            pltpu.VMEM(w_gate.shape[1:], bf16),
             pltpu.VMEM(w_up.shape[1:], bf16),
             pltpu.VMEM(w_down.shape[1:], bf16),
+            pltpu.VMEM(w_shared_gate.shape, bf16),
+            pltpu.VMEM(w_shared_up.shape, bf16),
             pltpu.VMEM(w_shared_down.shape, bf16),
-            pltpu.SemaphoreType.DMA((7,)),
+            pltpu.SemaphoreType.DMA((12,)),
+            pltpu.SemaphoreType.DMA((4,)),
+            pltpu.SemaphoreType.DMA((6,)),
         ],
         compiler_params=pltpu.CompilerParams(vmem_limit_bytes=24 * 1024 * 1024),
         name="run_experts",
     )(
         rows,
-        own_heads,
+        *in_hbm(own_heads),
         *got_heads,
-        tokens,
-        ffn_gain.reshape(1, -1),
-        w_gate,
-        w_shared_gate,
-        w_shared_up,
-        *in_hbm(w_out, w_up, w_down, w_shared_down),
+        *in_hbm(tokens, ffn_gain.reshape(1, -1), *weights),
     )
 
 
-def finish_kernel(combine, returned, base, part_1, part_2, part_3, mixed):
+def finish_kernel(
+    returned,
+    combine_any,
+    base_any,
+    part_1,
+    part_2,
+    part_3,
+    mixed,
+    wide,
+    combine,
+    base,
+    parts,
+    sems,
+):
     seqs = base.shape[0]
+    loads = [(combine_any, combine), (base_any, base)]
+    loads += [(part, parts.at[k]) for k, part in enumerate((part_1, part_2, part_3))]
+    loads = [
+        pltpu.make_async_copy(source, target, sems.at[i])
+        for i, (source, target) in enumerate(loads)
+    ]
+    for load in loads:
+        load.start()
+    wide[...] = returned[...].astype(jnp.float32)
+    arrived = jnp.concatenate(
+        [
+            jnp.concatenate(
+                [
+                    wide[pl.ds(2 * b + c, 128, stride=8), :].astype(jnp.bfloat16)
+                    for b in range(4)
+                ],
+                axis=1,
+            )
+            for c in range(2)
+        ],
+        axis=0,
+    )
+    for load in loads:
+        load.wait()
+    routed = jnp.dot(combine[...], arrived, preferred_element_type=jnp.float32)
     total = base[...]
-    for part in (part_1, part_2, part_3):
-        total = total + part[...].astype(jnp.float32)
-    arrived = jnp.concatenate([returned[b] for b in range(4)], axis=1)
-    routed = jnp.dot(combine[...], arrived, preferred_element_type=jnp.float32)
+    for k in range(3):
+        total = total + parts[k].astype(jnp.float32)
     for k in range(3):
         total = total + routed[k * seqs : (k + 1) * seqs, :]
     mixed[...] = total.astype(jnp.bfloat16)
@@ -420,11 +547,18 @@
     return pl.pallas_call(
         finish_kernel,
         out_shape=jax.ShapeDtypeStruct(base.shape, jnp.bfloat16),
-        in_specs=[vmem] * 6,
+        in_specs=[vmem] + [pl.BlockSpec(memory_space=pl.ANY)] * 5,
         out_specs=vmem,
+        scratch_shapes=[
+            pltpu.VMEM((1024, 128), jnp.float32),
+            pltpu.VMEM(combine.shape, jnp.bfloat16),
+            pltpu.VMEM(base.shape, jnp.float32),
+            pltpu.VMEM((3, *base.shape), jnp.bfloat16),
+            pltpu.SemaphoreType.DMA((5,)),
+        ],
         compiler_params=pltpu.CompilerParams(vmem_limit_bytes=4 * 1024 * 1024),
         name="finish",
-    )(combine, returned, base, *parts)
+    )(returned, *in_hbm(combine, base), *parts)
 
 
 def around(value, shift):
@@ -467,23 +601,30 @@
         routing,
         route_weights,
     )
-    message = message.reshape(6, 128, 2, 128).transpose(1, 0, 2, 3)
+    message = message.reshape(128, 6, 2, 128)
     arrived = lax.all_to_all(message, everyone, split_axis=0, concat_axis=0, tiled=True)
     got_heads = [around(heads, k) for k in range(1, 4)]
-    rows = arrived.reshape(32, 4, 6, 2, 128).transpose(1, 2, 0, 3, 4).reshape(24, 64, 128)
+    rows = arrived.reshape(1536, 128)
     results, base, *parts = run_experts(
         rows,
         heads,
         got_heads,
         tokens,
         ffn_gain,
-        (w_out, w_exp_gate, w_exp_up, w_exp_down, w_shared_gate, w_shared_up, w_shared_down),
+        (
+            w_out,
+            w_exp_gate,
+            w_exp_up,
+            w_exp_down,
+            w_shared_gate,
+            w_shared_up,
+            w_shared_down,
+        ),
     )
-    results = results.reshape(4, 4, 32, 2, 128).transpose(2, 0, 1, 3, 4)
     results = results.reshape(128, 4, 2, 128)
     returned = lax.all_to_all(results, everyone, split_axis=0, concat_axis=0, tiled=True)
     parts = [around(part, k + 1) for k, part in enumerate(parts)]
-    returned = returned.transpose(1, 0, 2, 3).reshape(4, 256, 128)
+    returned = returned.reshape(1024, 128)
     return finish(combine, returned, base, parts)
 
 

time: 58.5 us -> 58.5 us (level)
  local copies, waits for them, and re-layouts: 3.57 us -> 0 us
  Pallas kernels: 14.6 us -> 18 us
    ppermute x6, waiting for transfers between devices: 0.02 us -> 6.17 us  [around(): lax.ppermute(value, 'tp', [(i, (i + shift) % count) for i in range(count)])]
    all_to_all x1, waiting for transfers between devices: 8.77 us -> 5.18 us  [shards(): lax.all_to_all(message, everyone, split_axis=0, concat_axis=0, tiled=True)]
    pallas_call x2, Pallas kernels: 13.8 us -> 16.3 us  [the longest x1 9.9 us: attend(): pl.pallas_call(attend_kernel, out_shape=(pltpu.HBM((1536, 128), bf16), pl...]
    all_to_all x1, waiting for transfers between devices: 6.67 us -> 4.38 us  [shards(): lax.all_to_all(results, everyone, split_axis=0, concat_axis=0, tiled=True)]
    transpose x3 -> x0, local copies, waits for them, and re-layouts: 1.46 us -> none  [the longest x1 0.87 us: shards(): results = results.reshape(4, 4, 32, 2, 128).transpose(2, 0, 1, 3, 4)]
    all_to_all x1 -> x0, local copies, waits for them, and re-layouts: 1.05 us -> none  [shards(): lax.all_to_all(message, everyone, split_axis=0, concat_axis=0, tiled=True)]
    reshape x1 -> x0, local copies, waits for them, and re-layouts: 1.02 us -> none  [shards(): message = message.reshape(6, 128, 2, 128).transpose(1, 0, 2, 3)]
    pallas_call x1, Pallas kernels: 0.8 us -> 1.71 us  [finish(): pl.pallas_call(finish_kernel, out_shape=jax.ShapeDtypeStruct(base.shape,...]
  transfers between devices with their start and end apart: 8 -> 8, of which waited for: 2 -> 8; matrix products, arithmetic and copies ran while one was open for 3% -> 0% of each run, Pallas kernels for 0% -> 0%
where the time goes in v3:
time: 58.5 us; the launch traced here: 58.3 us
  starting transfers between devices  24.5 us (42%)
  Pallas kernels  18 us (31%)
  waiting for transfers between devices  15.7 us (27%)
    all_to_all x1, starting transfers between devices, shards(): lax.all_to_all(message, everyone, split_axis=0, concat_axis=0, tiled=True)  11.5 us
    pallas_call x1, Pallas kernels, attend(): pl.pallas_call(attend_kernel, out_shape=(pltpu.HBM((1536, 128), bf16), pl...  9.9 us
    ppermute x6, starting transfers between devices, around(): lax.ppermute(value, 'tp', [(i, (i + shift) % count) for i in range(count)])  8.78 us
    pallas_call x1, Pallas kernels, run_experts(): pl.pallas_call(expert_kernel, out_shape=(pltpu.HBM((1024, 128), bf16), pl...  6.42 us
    ppermute x6, waiting for transfers between devices, around(): lax.ppermute(value, 'tp', [(i, (i + shift) % count) for i in range(count)])  6.17 us
    all_to_all x1, waiting for transfers between devices, shards(): lax.all_to_all(message, everyone, split_axis=0, concat_axis=0, tiled=True)  5.18 us
    all_to_all x1, waiting for transfers between devices, shards(): lax.all_to_all(results, everyone, split_axis=0, concat_axis=0, tiled=True)  4.38 us
    all_to_all x1, starting transfers between devices, shards(): lax.all_to_all(results, everyone, split_axis=0, concat_axis=0, tiled=True)  4.2 us
  transfers between devices with their start and end apart: 8, of which 8 were waited for; matrix products, arithmetic and copies ran while one was open for 0% of the time, Pallas kernels for 0%

profile of v3, /device:TPU:1, one launch (start us, length us, event | category | flops | bytes accessed | tf_op | source)
XLA Modules:
  0.0 58.3 jit_solution(14457870915888832352)
XLA Ops:
  0.0 9.9 %attend.1 = (bf16[1536,128]{1,0:T(8,128)(2,1)}, bf16[32,256]{1,0:T(8,128)(2,1)}, bf16[96,256]{1,0:T(8,128)(2,1)}) custom-call(s32[32]{0:T(128)} %lengths_hbm.1, f32[4]{0:T(128)} %lambdas_hbm.1, bf16[32,2048]{1,0:T(8,128)(2,1)} %tokens_hbm.3, f32[1,2048]{1,0:T(1,128)} %bitcast.18, bf16[2048,256]{1,0:T(8,128)(2,1)} %w_query_hbm.1, bf16[64,2048]{1,0:T(8,128)(2,1)} %bitcast.15, ...), custom_call_target="tpu_custom_call" | custom-call | tf_op jit(solution)/shard_map/attend/pallas_call | solution.py:253
  9.9 11.5 %all-to-all-start = ((bf16[128,6,2,128]{3,2,1,0:T(2,128)(2,1)}), bf16[128,6,2,128]{3,2,1,0:T(2,128)(2,1)S(1)}, u32[]{:S(2)}, u32[]{:S(2)}) async-start(bf16[128,6,2,128]{3,2,1,0:T(2,128)(2,1)} %bitcast.13), calls=%async_computation | async-start | bytes 786432 | tf_op jit(solution)/shard_map/all_to_all | solution.py:605
  21.4 2.6 %collective-permute-start.2 = (bf16[32,256]{1,0:T(8,128)(2,1)}, bf16[32,256]{1,0:T(8,128)(2,1)S(1)}, u32[]{:S(2)}, u32[]{:S(2)}) collective-permute-start(bf16[32,256]{1,0:T(8,128)(2,1)} %get-tuple-element.14.own_heads), channel_id=1, source_target_pairs={{0,3},{1,0},{2,1},{3,2},{4,7},{5,4},{6,5},{7,6},{8,11},{9,8},{10,9... | collective-permute-start | bytes 49160 | tf_op jit(solution)/shard_map/ppermute | solution.py:566
  24.0 0.6 collective-permute-start.1
  24.6 0.6 collective-permute-start
  25.2 2.1 %collective-permute-done.2.heads_3 = bf16[32,256]{1,0:T(8,128)(2,1)S(1)} collective-permute-done((bf16[32,256]{1,0:T(8,128)(2,1)}, bf16[32,256]{1,0:T(8,128)(2,1)S(1)}, u32[]{:S(2)}, u32[]{:S(2)}) %collective-permute-start.2) | collective-permute-done | bytes 16416 | tf_op jit(solution)/shard_map/ppermute | solution.py:566
  27.3 1.5 %collective-permute-done.1.heads_2 = bf16[32,256]{1,0:T(8,128)(2,1)S(1)} collective-permute-done((bf16[32,256]{1,0:T(8,128)(2,1)}, bf16[32,256]{1,0:T(8,128)(2,1)S(1)}, u32[]{:S(2)}, u32[]{:S(2)}) %collective-permute-start.1) | collective-permute-done | bytes 16416 | tf_op jit(solution)/shard_map/ppermute | solution.py:566
  28.8 0.2 collective-permute-done.heads_1
  29.1 5.2 %all-to-all-done = bf16[128,6,2,128]{3,2,1,0:T(2,128)(2,1)S(1)} async-done(((bf16[128,6,2,128]{3,2,1,0:T(2,128)(2,1)}), bf16[128,6,2,128]{3,2,1,0:T(2,128)(2,1)S(1)}, u32[]{:S(2)}, u32[]{:S(2)}) %all-to-all-start) | async-done | bytes 393248 | tf_op jit(solution)/shard_map/all_to_all | solution.py:605
  34.3 6.4 %run_experts.1 = (bf16[1024,128]{1,0:T(8,128)(2,1)}, f32[32,512]{1,0:T(8,128)}, bf16[32,512]{1,0:T(8,128)(2,1)}, bf16[32,512]{1,0:T(8,128)(2,1)}, bf16[32,512]{1,0:T(8,128)(2,1)}) custom-call(bf16[1536,128]{1,0:T(8,128)(2,1)S(1)} %bitcast.11, bf16[32,256]{1,0:T(8,128)(2,1)} %get-tuple-element.14.own_heads, bf16[32,256]{1,0:T(8,128)(2,1)S(1)} %collective-permute-done.heads_1, ...), custom_call_target="tpu_custom_call" | custom-call | tf_op jit(solution)/shard_map/run_experts/pallas_call | solution.py:454
  40.7 4.2 %all-to-all-start.1 = ((bf16[128,4,2,128]{3,2,1,0:T(2,128)(2,1)}), bf16[128,4,2,128]{3,2,1,0:T(2,128)(2,1)S(1)}, u32[]{:S(2)}, u32[]{:S(2)}) async-start(bf16[128,4,2,128]{3,2,1,0:T(2,128)(2,1)} %bitcast.14), calls=%async_computation.1 | async-start | bytes 524288 | tf_op jit(solution)/shard_map/all_to_all | solution.py:625
  44.9 1.4 %collective-permute-start.3 = (bf16[32,512]{1,0:T(8,128)(2,1)}, bf16[32,512]{1,0:T(8,128)(2,1)S(1)}, u32[]{:S(2)}, u32[]{:S(2)}) collective-permute-start(bf16[32,512]{1,0:T(8,128)(2,1)} %get-tuple-element.18), channel_id=1, source_target_pairs={{0,1},{1,2},{2,3},{3,0},{4,5},{5,6},{6,7},{7,4},{8,9},{9,10},{10,1... | collective-permute-start | bytes 98312 | tf_op jit(solution)/shard_map/ppermute | solution.py:566
  46.3 2.4 %collective-permute-start.4 = (bf16[32,512]{1,0:T(8,128)(2,1)}, bf16[32,512]{1,0:T(8,128)(2,1)S(1)}, u32[]{:S(2)}, u32[]{:S(2)}) collective-permute-start(bf16[32,512]{1,0:T(8,128)(2,1)} %get-tuple-element.19), channel_id=1, source_target_pairs={{0,2},{1,3},{2,0},{3,1},{4,6},{5,7},{6,4},{7,5},{8,10},{9,11},{10,... | collective-permute-start | bytes 98312 | tf_op jit(solution)/shard_map/ppermute | solution.py:566
  48.7 1.2 %collective-permute-start.5 = (bf16[32,512]{1,0:T(8,128)(2,1)}, bf16[32,512]{1,0:T(8,128)(2,1)S(1)}, u32[]{:S(2)}, u32[]{:S(2)}) collective-permute-start(bf16[32,512]{1,0:T(8,128)(2,1)} %get-tuple-element.20), channel_id=1, source_target_pairs={{0,3},{1,0},{2,1},{3,2},{4,7},{5,4},{6,5},{7,6},{8,11},{9,8},{10,9... | collective-permute-start | bytes 98312 | tf_op jit(solution)/shard_map/ppermute | solution.py:566
  49.9 1.0 %collective-permute-done.3.part_1 = bf16[32,512]{1,0:T(8,128)(2,1)S(1)} collective-permute-done((bf16[32,512]{1,0:T(8,128)(2,1)}, bf16[32,512]{1,0:T(8,128)(2,1)S(1)}, u32[]{:S(2)}, u32[]{:S(2)}) %collective-permute-start.3) | collective-permute-done | bytes 32800 | tf_op jit(solution)/shard_map/ppermute | solution.py:566
  50.9 1.0 %collective-permute-done.4.part_2 = bf16[32,512]{1,0:T(8,128)(2,1)S(1)} collective-permute-done((bf16[32,512]{1,0:T(8,128)(2,1)}, bf16[32,512]{1,0:T(8,128)(2,1)S(1)}, u32[]{:S(2)}, u32[]{:S(2)}) %collective-permute-start.4) | collective-permute-done | bytes 32800 | tf_op jit(solution)/shard_map/ppermute | solution.py:566
  52.0 0.2 collective-permute-done.5.part_3
  52.2 4.4 %all-to-all-done.1 = bf16[128,4,2,128]{3,2,1,0:T(2,128)(2,1)S(1)} async-done(((bf16[128,4,2,128]{3,2,1,0:T(2,128)(2,1)}), bf16[128,4,2,128]{3,2,1,0:T(2,128)(2,1)S(1)}, u32[]{:S(2)}, u32[]{:S(2)}) %all-to-all-start.1) | async-done | bytes 262176 | tf_op jit(solution)/shard_map/all_to_all | solution.py:625
  56.6 1.7 %finish.1 = bf16[32,512]{1,0:T(8,128)(2,1)} custom-call(bf16[1024,128]{1,0:T(8,128)(2,1)S(1)} %bitcast.12, bf16[96,256]{1,0:T(8,128)(2,1)} %get-tuple-element.16.combine_any, f32[32,512]{1,0:T(8,128)} %get-tuple-element.17.base_any, bf16[32,512]{1,0:T(8,128)(2,1)S(1)} %collective-permute-done.3.part_1, bf16[32,512]{1,0:T(8,128)(2,1)S(1)} %collective-permute-done.4.part_2, ...), custom_call_target="tpu_custom_call" | custom-call | tf_op jit(solution)/shard_map/finish/pallas_call | solution.py:547
Async XLA Ops:
  9.9 24.4 %all-to-all-start = ((bf16[128,6,2,128]{3,2,1,0:T(2,128)(2,1)}), bf16[128,6,2,128]{3,2,1,0:T(2,128)(2,1)S(1)}, u32[]{:S(2)}, u32[]{:S(2)}) async-start(bf16[128,6,2,128]{3,2,1,0:T(2,128)(2,1)} %bitcast.13), calls=%async_computation | async-start | bytes 786432 | tf_op jit(solution)/shard_map/all_to_all | solution.py:605
  21.4 5.9 %collective-permute-start.2 = (bf16[32,256]{1,0:T(8,128)(2,1)}, bf16[32,256]{1,0:T(8,128)(2,1)S(1)}, u32[]{:S(2)}, u32[]{:S(2)}) collective-permute-start(bf16[32,256]{1,0:T(8,128)(2,1)} %get-tuple-element.14.own_heads), channel_id=1, source_target_pairs={{0,3},{1,0},{2,1},{3,2},{4,7},{5,4},{6,5},{7,6},{8,11},{9,8},{10,9... | collective-permute-start | bytes 49160 | tf_op jit(solution)/shard_map/ppermute | solution.py:566
  24.0 4.8 %collective-permute-start.1 = (bf16[32,256]{1,0:T(8,128)(2,1)}, bf16[32,256]{1,0:T(8,128)(2,1)S(1)}, u32[]{:S(2)}, u32[]{:S(2)}) collective-permute-start(bf16[32,256]{1,0:T(8,128)(2,1)} %get-tuple-element.14.own_heads), channel_id=1, source_target_pairs={{0,2},{1,3},{2,0},{3,1},{4,6},{5,7},{6,4},{7,5},{8,10},{9,11},{10,... | collective-permute-start | bytes 49160 | tf_op jit(solution)/shard_map/ppermute | solution.py:566
  24.6 4.5 %collective-permute-start = (bf16[32,256]{1,0:T(8,128)(2,1)}, bf16[32,256]{1,0:T(8,128)(2,1)S(1)}, u32[]{:S(2)}, u32[]{:S(2)}) collective-permute-start(bf16[32,256]{1,0:T(8,128)(2,1)} %get-tuple-element.14.own_heads), channel_id=1, source_target_pairs={{0,1},{1,2},{2,3},{3,0},{4,5},{5,6},{6,7},{7,4},{8,9},{9,10},{10,1... | collective-permute-start | bytes 49160 | tf_op jit(solution)/shard_map/ppermute | solution.py:566
  40.7 15.9 %all-to-all-start.1 = ((bf16[128,4,2,128]{3,2,1,0:T(2,128)(2,1)}), bf16[128,4,2,128]{3,2,1,0:T(2,128)(2,1)S(1)}, u32[]{:S(2)}, u32[]{:S(2)}) async-start(bf16[128,4,2,128]{3,2,1,0:T(2,128)(2,1)} %bitcast.14), calls=%async_computation.1 | async-start | bytes 524288 | tf_op jit(solution)/shard_map/all_to_all | solution.py:625
  44.9 6.0 %collective-permute-start.3 = (bf16[32,512]{1,0:T(8,128)(2,1)}, bf16[32,512]{1,0:T(8,128)(2,1)S(1)}, u32[]{:S(2)}, u32[]{:S(2)}) collective-permute-start(bf16[32,512]{1,0:T(8,128)(2,1)} %get-tuple-element.18), channel_id=1, source_target_pairs={{0,1},{1,2},{2,3},{3,0},{4,5},{5,6},{6,7},{7,4},{8,9},{9,10},{10,1... | collective-permute-start | bytes 98312 | tf_op jit(solution)/shard_map/ppermute | solution.py:566
  46.3 5.7 %collective-permute-start.4 = (bf16[32,512]{1,0:T(8,128)(2,1)}, bf16[32,512]{1,0:T(8,128)(2,1)S(1)}, u32[]{:S(2)}, u32[]{:S(2)}) collective-permute-start(bf16[32,512]{1,0:T(8,128)(2,1)} %get-tuple-element.19), channel_id=1, source_target_pairs={{0,2},{1,3},{2,0},{3,1},{4,6},{5,7},{6,4},{7,5},{8,10},{9,11},{10,... | collective-permute-start | bytes 98312 | tf_op jit(solution)/shard_map/ppermute | solution.py:566
  48.7 3.5 %collective-permute-start.5 = (bf16[32,512]{1,0:T(8,128)(2,1)}, bf16[32,512]{1,0:T(8,128)(2,1)S(1)}, u32[]{:S(2)}, u32[]{:S(2)}) collective-permute-start(bf16[32,512]{1,0:T(8,128)(2,1)} %get-tuple-element.20), channel_id=1, source_target_pairs={{0,3},{1,0},{2,1},{3,2},{4,7},{5,4},{6,5},{7,6},{8,11},{9,8},{10,9... | collective-permute-start | bytes 98312 | tf_op jit(solution)/shard_map/ppermute | solution.py:566

commit v4 on v3

--- a/solution.py
+++ b/solution.py
@@ -304,8 +304,33 @@
     )
 
 
+def fetch_kernel(after, *refs):
+    count = (len(refs) - 1) // 2
+    loads = [
+        pltpu.make_async_copy(refs[i], refs[count + i], refs[-1].at[i]) for i in range(count)
+    ]
+    for load in loads:
+        load.start()
+    for load in loads:
+        load.wait()
+
+
+def fetch(after, arrays):
+    hbm = pl.BlockSpec(memory_space=pltpu.HBM)
+    return pl.pallas_call(
+        fetch_kernel,
+        out_shape=tuple(jax.ShapeDtypeStruct(a.shape, a.dtype) for a in arrays),
+        in_specs=[hbm] * (1 + len(arrays)),
+        out_specs=(pl.BlockSpec(memory_space=pltpu.VMEM),) * len(arrays),
+        scratch_shapes=[pltpu.SemaphoreType.DMA((len(arrays),))],
+        compiler_params=pltpu.CompilerParams(vmem_limit_bytes=1024 * 1024),
+        name="fetch",
+    )(*in_hbm(after, *arrays))
+
+
 def expert_kernel(
     rows,
+    w_gate,
     own_heads,
     heads_1,
     heads_2,
@@ -313,7 +338,6 @@
     tokens_hbm,
     ffn_gain_hbm,
     w_out_hbm,
-    w_gate_hbm,
     w_up_hbm,
     w_down_hbm,
     w_shared_gate_hbm,
@@ -335,7 +359,6 @@
     tokens,
     ffn_gain,
     w_out,
-    w_gate,
     w_up,
     w_down,
     w_shared_gate,
@@ -359,9 +382,9 @@
     for load in gathered:
         load.start()
     loads += [(tokens_hbm, tokens), (ffn_gain_hbm, ffn_gain)]
-    loads += [(w_gate_hbm.at[0], w_gate), (w_up_hbm.at[0], w_up)]
+    loads += [(w_up_hbm.at[0], w_up), (w_down_hbm.at[0], w_down)]
     loads += [(w_shared_gate_hbm, w_shared_gate), (w_shared_up_hbm, w_shared_up)]
-    loads += [(w_down_hbm.at[0], w_down), (w_shared_down_hbm, w_shared_down)]
+    loads += [(w_shared_down_hbm, w_shared_down)]
     loads = [
         pltpu.make_async_copy(source, target, sems.at[i])
         for i, (source, target) in enumerate(loads)
@@ -405,12 +428,8 @@
         return (gate_part / (1.0 + jnp.exp(-gate_part)) * up_part).astype(jnp.bfloat16)
 
     loads[6].wait()
+    act = gated(ffn_in[:slots], w_gate[0], w_up[...])
     loads[7].wait()
-    act = gated(ffn_in[:slots], w_gate[...], w_up[...])
-    loads[8].wait()
-    loads[9].wait()
-    shared_act = gated(ffn_in[slots:], w_shared_gate[...], w_shared_up[...])
-    loads[10].wait()
     result = jnp.dot(act, w_down[...], preferred_element_type=jnp.float32)
     for b in range(16):
         for c in range(2):
@@ -421,30 +440,31 @@
     for i in range(2):
         half = pl.ds(512 * i, 512)
         ready[half, :] = stage[half, :].astype(jnp.bfloat16)
-        sends.append(
-            pltpu.make_async_copy(ready.at[half], results.at[half], send_sems.at[i])
-        )
+        sends.append(pltpu.make_async_copy(ready.at[half], results.at[half], send_sems.at[i]))
         sends[i].start()
-    loads[11].wait()
+    loads[8].wait()
+    loads[9].wait()
+    shared_act = gated(ffn_in[slots:], w_shared_gate[...], w_shared_up[...])
+    loads[10].wait()
     partial[...] = jnp.dot(shared_act, w_shared_down[...], preferred_element_type=jnp.float32)
 
     def share(source, shift):
         at = pl.multiple_of(((tp + shift) % 4) * 512, 512)
         return source[:, pl.ds(at, 512)]
 
-    base[...] = share(partial, 0) + share(resid, 0).astype(jnp.float32)
-    sends.append(pltpu.make_async_copy(base, base_out, send_sems.at[2]))
-    sends[2].start()
     for k, part in enumerate((part_1, part_2, part_3)):
         parts[k] = share(partial, k + 1).astype(jnp.bfloat16)
-        sends.append(pltpu.make_async_copy(parts.at[k], part, send_sems.at[3 + k]))
-        sends[3 + k].start()
+        sends.append(pltpu.make_async_copy(parts.at[k], part, send_sems.at[2 + k]))
+        sends[2 + k].start()
+    base[...] = share(partial, 0) + share(resid, 0).astype(jnp.float32)
+    sends.append(pltpu.make_async_copy(base, base_out, send_sems.at[5]))
+    sends[5].start()
     for send in sends:
         send.wait()
 
 
-def run_experts(rows, own_heads, got_heads, tokens, ffn_gain, weights):
-    w_out, w_gate, w_up, w_down, w_shared_gate, w_shared_up, w_shared_down = weights
+def run_experts(rows, own_heads, got_heads, tokens, ffn_gain, w_gate, weights):
+    w_out, w_up, w_down, w_shared_gate, w_shared_up, w_shared_down = weights
     seqs, width = tokens.shape
     vmem = pl.BlockSpec(memory_space=pltpu.VMEM)
     bf16, f32 = jnp.bfloat16, jnp.float32
@@ -460,7 +480,7 @@
             part,
             part,
         ),
-        in_specs=[vmem] + [either] * 4 + [hbm] * 9,
+        in_specs=[vmem] * 2 + [either] * 4 + [hbm] * 8,
         out_specs=(hbm,) * 5,
         scratch_shapes=[
             pltpu.VMEM((4, seqs, 256), bf16),
@@ -474,13 +494,12 @@
             pltpu.VMEM((seqs, width), bf16),
             pltpu.VMEM((1, width), f32),
             pltpu.VMEM(w_out.shape, bf16),
-            pltpu.VMEM(w_gate.shape[1:], bf16),
             pltpu.VMEM(w_up.shape[1:], bf16),
             pltpu.VMEM(w_down.shape[1:], bf16),
             pltpu.VMEM(w_shared_gate.shape, bf16),
             pltpu.VMEM(w_shared_up.shape, bf16),
             pltpu.VMEM(w_shared_down.shape, bf16),
-            pltpu.SemaphoreType.DMA((12,)),
+            pltpu.SemaphoreType.DMA((11,)),
             pltpu.SemaphoreType.DMA((4,)),
             pltpu.SemaphoreType.DMA((6,)),
         ],
@@ -488,35 +507,15 @@
         name="run_experts",
     )(
         rows,
+        w_gate,
         *in_hbm(own_heads),
         *got_heads,
         *in_hbm(tokens, ffn_gain.reshape(1, -1), *weights),
     )
 
 
-def finish_kernel(
-    returned,
-    combine_any,
-    base_any,
-    part_1,
-    part_2,
-    part_3,
-    mixed,
-    wide,
-    combine,
-    base,
-    parts,
-    sems,
-):
+def finish_kernel(returned, combine, base, part_1, part_2, part_3, mixed, wide):
     seqs = base.shape[0]
-    loads = [(combine_any, combine), (base_any, base)]
-    loads += [(part, parts.at[k]) for k, part in enumerate((part_1, part_2, part_3))]
-    loads = [
-        pltpu.make_async_copy(source, target, sems.at[i])
-        for i, (source, target) in enumerate(loads)
-    ]
-    for load in loads:
-        load.start()
     wide[...] = returned[...].astype(jnp.float32)
     arrived = jnp.concatenate(
         [
@@ -531,34 +530,26 @@
         ],
         axis=0,
     )
-    for load in loads:
-        load.wait()
     routed = jnp.dot(combine[...], arrived, preferred_element_type=jnp.float32)
     total = base[...]
-    for k in range(3):
-        total = total + parts[k].astype(jnp.float32)
+    for part in (part_1, part_2, part_3):
+        total = total + part[...].astype(jnp.float32)
     for k in range(3):
         total = total + routed[k * seqs : (k + 1) * seqs, :]
     mixed[...] = total.astype(jnp.bfloat16)
 
 
-def finish(combine, returned, base, parts):
+def finish(returned, combine, base, parts):
     vmem = pl.BlockSpec(memory_space=pltpu.VMEM)
     return pl.pallas_call(
         finish_kernel,
         out_shape=jax.ShapeDtypeStruct(base.shape, jnp.bfloat16),
-        in_specs=[vmem] + [pl.BlockSpec(memory_space=pl.ANY)] * 5,
+        in_specs=[vmem] * 6,
         out_specs=vmem,
-        scratch_shapes=[
-            pltpu.VMEM((1024, 128), jnp.float32),
-            pltpu.VMEM(combine.shape, jnp.bfloat16),
-            pltpu.VMEM(base.shape, jnp.float32),
-            pltpu.VMEM((3, *base.shape), jnp.bfloat16),
-            pltpu.SemaphoreType.DMA((5,)),
-        ],
+        scratch_shapes=[pltpu.VMEM((1024, 128), jnp.float32)],
         compiler_params=pltpu.CompilerParams(vmem_limit_bytes=4 * 1024 * 1024),
         name="finish",
-    )(returned, *in_hbm(combine, base), *parts)
+    )(returned, combine, base, *parts)
 
 
 def around(value, shift):
@@ -604,6 +595,7 @@
     message = message.reshape(128, 6, 2, 128)
     arrived = lax.all_to_all(message, everyone, split_axis=0, concat_axis=0, tiled=True)
     got_heads = [around(heads, k) for k in range(1, 4)]
+    (gate,) = fetch(heads, (w_exp_gate,))
     rows = arrived.reshape(1536, 128)
     results, base, *parts = run_experts(
         rows,
@@ -611,21 +603,15 @@
         got_heads,
         tokens,
         ffn_gain,
-        (
-            w_out,
-            w_exp_gate,
-            w_exp_up,
-            w_exp_down,
-            w_shared_gate,
-            w_shared_up,
-            w_shared_down,
-        ),
+        gate,
+        (w_out, w_exp_up, w_exp_down, w_shared_gate, w_shared_up, w_shared_down),
     )
     results = results.reshape(128, 4, 2, 128)
     returned = lax.all_to_all(results, everyone, split_axis=0, concat_axis=0, tiled=True)
     parts = [around(part, k + 1) for k, part in enumerate(parts)]
+    combine, base = fetch(base, (combine, base))
     returned = returned.reshape(1024, 128)
-    return finish(combine, returned, base, parts)
+    return finish(returned, combine, base, parts)
 
 
 def solution(mesh):

time: 58.5 us -> 57.1 us (0.976)
  waiting for transfers between devices: 15.7 us -> 13.2 us
  Pallas kernels: 18 us -> 19.1 us
    ppermute x6, waiting for transfers between devices: 6.17 us -> 3.67 us  [around(): lax.ppermute(value, 'tp', [(i, (i + shift) % count) for i in range(count)])]
    pallas_call x0 -> x2, Pallas kernels: none -> 2.48 us  [fetch(): pl.pallas_call(fetch_kernel, out_shape=tuple((jax.ShapeDtypeStruct(a.shap...]
    pallas_call x1, Pallas kernels: 1.71 us -> 0.87 us  [finish(): pl.pallas_call(finish_kernel, out_shape=jax.ShapeDtypeStruct(base.shape,...]
    pallas_call x1, Pallas kernels: 6.42 us -> 5.83 us  [run_experts(): pl.pallas_call(expert_kernel, out_shape=(pltpu.HBM((1024, 128), bf16), pl...]
  transfers between devices with their start and end apart: 8 -> 8, of which waited for: 8 -> 8; matrix products, arithmetic and copies ran while one was open for 0% -> 0% of each run, Pallas kernels for 0% -> 4%
where the time goes in v4:
time: 57.1 us; the launch traced here: 56.8 us
  starting transfers between devices  24.5 us (43%)
  Pallas kernels  19.1 us (33%)
  waiting for transfers between devices  13.2 us (23%)
    all_to_all x1, starting transfers between devices, shards(): lax.all_to_all(message, everyone, split_axis=0, concat_axis=0, tiled=True)  11.5 us
    pallas_call x1, Pallas kernels, attend(): pl.pallas_call(attend_kernel, out_shape=(pltpu.HBM((1536, 128), bf16), pl...  9.9 us
    ppermute x6, starting transfers between devices, around(): lax.ppermute(value, 'tp', [(i, (i + shift) % count) for i in range(count)])  8.78 us
    pallas_call x1, Pallas kernels, run_experts(): pl.pallas_call(expert_kernel, out_shape=(pltpu.HBM((1024, 128), bf16), pl...  5.83 us
    all_to_all x1, waiting for transfers between devices, shards(): lax.all_to_all(message, everyone, split_axis=0, concat_axis=0, tiled=True)  5.18 us
    all_to_all x1, waiting for transfers between devices, shards(): lax.all_to_all(results, everyone, split_axis=0, concat_axis=0, tiled=True)  4.38 us
    all_to_all x1, starting transfers between devices, shards(): lax.all_to_all(results, everyone, split_axis=0, concat_axis=0, tiled=True)  4.2 us
    ppermute x6, waiting for transfers between devices, around(): lax.ppermute(value, 'tp', [(i, (i + shift) % count) for i in range(count)])  3.67 us
  transfers between devices with their start and end apart: 8, of which 8 were waited for; matrix products, arithmetic and copies ran while one was open for 0% of the time, Pallas kernels for 4%

profile of v4, /device:TPU:1, one launch (start us, length us, event | category | flops | bytes accessed | tf_op | source)
XLA Modules:
  0.0 56.8 jit_solution(10616611504562382246)
XLA Ops:
  0.0 9.9 %attend.1 = (bf16[1536,128]{1,0:T(8,128)(2,1)}, bf16[32,256]{1,0:T(8,128)(2,1)}, bf16[96,256]{1,0:T(8,128)(2,1)}) custom-call(s32[32]{0:T(128)} %lengths_hbm.1, f32[4]{0:T(128)} %lambdas_hbm.1, bf16[32,2048]{1,0:T(8,128)(2,1)} %tokens_hbm.3, f32[1,2048]{1,0:T(1,128)} %bitcast.18, bf16[2048,256]{1,0:T(8,128)(2,1)} %w_query_hbm.1, bf16[64,2048]{1,0:T(8,128)(2,1)} %bitcast.15, ...), custom_call_target="tpu_custom_call" | custom-call | tf_op jit(solution)/shard_map/attend/pallas_call | solution.py:253
  9.9 11.5 %all-to-all-start = ((bf16[128,6,2,128]{3,2,1,0:T(2,128)(2,1)}), bf16[128,6,2,128]{3,2,1,0:T(2,128)(2,1)S(1)}, u32[]{:S(2)}, u32[]{:S(2)}) async-start(bf16[128,6,2,128]{3,2,1,0:T(2,128)(2,1)} %bitcast.13), calls=%async_computation | async-start | bytes 786432 | tf_op jit(solution)/shard_map/all_to_all | solution.py:596
  21.4 2.6 %collective-permute-start.2 = (bf16[32,256]{1,0:T(8,128)(2,1)}, bf16[32,256]{1,0:T(8,128)(2,1)S(1)}, u32[]{:S(2)}, u32[]{:S(2)}) collective-permute-start(bf16[32,256]{1,0:T(8,128)(2,1)} %get-tuple-element.16.after.own_heads), channel_id=1, source_target_pairs={{0,3},{1,0},{2,1},{3,2},{4,7},{5,4},{6,5},{7,6},{8,11},{9,8},{10,9... | collective-permute-start | bytes 49160 | tf_op jit(solution)/shard_map/ppermute | solution.py:557
  24.0 0.6 %collective-permute-start.1 = (bf16[32,256]{1,0:T(8,128)(2,1)}, bf16[32,256]{1,0:T(8,128)(2,1)S(1)}, u32[]{:S(2)}, u32[]{:S(2)}) collective-permute-start(bf16[32,256]{1,0:T(8,128)(2,1)} %get-tuple-element.16.after.own_heads), channel_id=1, source_target_pairs={{0,2},{1,3},{2,0},{3,1},{4,6},{5,7},{6,4},{7,5},{8,10},{9,11},{10,... | collective-permute-start | bytes 49160 | tf_op jit(solution)/shard_map/ppermute | solution.py:557
  24.6 0.6 %collective-permute-start = (bf16[32,256]{1,0:T(8,128)(2,1)}, bf16[32,256]{1,0:T(8,128)(2,1)S(1)}, u32[]{:S(2)}, u32[]{:S(2)}) collective-permute-start(bf16[32,256]{1,0:T(8,128)(2,1)} %get-tuple-element.16.after.own_heads), channel_id=1, source_target_pairs={{0,1},{1,2},{2,3},{3,0},{4,5},{5,6},{6,7},{7,4},{8,9},{9,10},{10,1... | collective-permute-start | bytes 49160 | tf_op jit(solution)/shard_map/ppermute | solution.py:557
  25.2 1.6 %fetch.2.w_gate = bf16[1,2048,512]{2,1,0:T(8,128)(2,1)S(1)} custom-call(bf16[32,256]{1,0:T(8,128)(2,1)} %get-tuple-element.16.after.own_heads, bf16[1,2048,512]{2,1,0:T(8,128)(2,1)} %refs_0_.1), custom_call_target="tpu_custom_call" | custom-call | tf_op jit(solution)/shard_map/fetch/pallas_call | solution.py:320
  26.8 0.5 collective-permute-done.2.heads_3
  27.3 1.5 %collective-permute-done.1.heads_2 = bf16[32,256]{1,0:T(8,128)(2,1)S(1)} collective-permute-done((bf16[32,256]{1,0:T(8,128)(2,1)}, bf16[32,256]{1,0:T(8,128)(2,1)S(1)}, u32[]{:S(2)}, u32[]{:S(2)}) %collective-permute-start.1) | collective-permute-done | bytes 16416 | tf_op jit(solution)/shard_map/ppermute | solution.py:557
  28.8 0.2 collective-permute-done.heads_1
  29.1 5.2 %all-to-all-done = bf16[128,6,2,128]{3,2,1,0:T(2,128)(2,1)S(1)} async-done(((bf16[128,6,2,128]{3,2,1,0:T(2,128)(2,1)}), bf16[128,6,2,128]{3,2,1,0:T(2,128)(2,1)S(1)}, u32[]{:S(2)}, u32[]{:S(2)}) %all-to-all-start) | async-done | bytes 393248 | tf_op jit(solution)/shard_map/all_to_all | solution.py:596
  34.3 5.8 %run_experts.1 = (bf16[1024,128]{1,0:T(8,128)(2,1)}, f32[32,512]{1,0:T(8,128)}, bf16[32,512]{1,0:T(8,128)(2,1)}, bf16[32,512]{1,0:T(8,128)(2,1)}, bf16[32,512]{1,0:T(8,128)(2,1)}) custom-call(bf16[1536,128]{1,0:T(8,128)(2,1)S(1)} %bitcast.11, bf16[1,2048,512]{2,1,0:T(8,128)(2,1)S(1)} %fetch.2.w_gate, bf16[32,256]{1,0:T(8,128)(2,1)} %get-tuple-element.16.after.own_heads, ...), custom_call_target="tpu_custom_call" | custom-call | tf_op jit(solution)/shard_map/run_experts/pallas_call | solution.py:474
  40.1 4.2 %all-to-all-start.1 = ((bf16[128,4,2,128]{3,2,1,0:T(2,128)(2,1)}), bf16[128,4,2,128]{3,2,1,0:T(2,128)(2,1)S(1)}, u32[]{:S(2)}, u32[]{:S(2)}) async-start(bf16[128,4,2,128]{3,2,1,0:T(2,128)(2,1)} %bitcast.14), calls=%async_computation.1 | async-start | bytes 524288 | tf_op jit(solution)/shard_map/all_to_all | solution.py:610
  44.3 1.4 %collective-permute-start.3 = (bf16[32,512]{1,0:T(8,128)(2,1)}, bf16[32,512]{1,0:T(8,128)(2,1)S(1)}, u32[]{:S(2)}, u32[]{:S(2)}) collective-permute-start(bf16[32,512]{1,0:T(8,128)(2,1)} %get-tuple-element.22), channel_id=1, source_target_pairs={{0,1},{1,2},{2,3},{3,0},{4,5},{5,6},{6,7},{7,4},{8,9},{9,10},{10,1... | collective-permute-start | bytes 98312 | tf_op jit(solution)/shard_map/ppermute | solution.py:557
  45.7 2.4 %collective-permute-start.4 = (bf16[32,512]{1,0:T(8,128)(2,1)}, bf16[32,512]{1,0:T(8,128)(2,1)S(1)}, u32[]{:S(2)}, u32[]{:S(2)}) collective-permute-start(bf16[32,512]{1,0:T(8,128)(2,1)} %get-tuple-element.23), channel_id=1, source_target_pairs={{0,2},{1,3},{2,0},{3,1},{4,6},{5,7},{6,4},{7,5},{8,10},{9,11},{10,... | collective-permute-start | bytes 98312 | tf_op jit(solution)/shard_map/ppermute | solution.py:557
  48.1 1.2 %collective-permute-start.5 = (bf16[32,512]{1,0:T(8,128)(2,1)}, bf16[32,512]{1,0:T(8,128)(2,1)S(1)}, u32[]{:S(2)}, u32[]{:S(2)}) collective-permute-start(bf16[32,512]{1,0:T(8,128)(2,1)} %get-tuple-element.24), channel_id=1, source_target_pairs={{0,3},{1,0},{2,1},{3,2},{4,7},{5,4},{6,5},{7,6},{8,11},{9,8},{10,9... | collective-permute-start | bytes 98312 | tf_op jit(solution)/shard_map/ppermute | solution.py:557
  49.3 0.9 %fetch.3 = (bf16[96,256]{1,0:T(8,128)(2,1)S(1)}, f32[32,512]{1,0:T(8,128)S(1)}) custom-call(f32[32,512]{1,0:T(8,128)} %get-tuple-element.18.after.refs_1_, bf16[96,256]{1,0:T(8,128)(2,1)} %get-tuple-element.19.refs_0_, f32[32,512]{1,0:T(8,128)} %get-tuple-element.18.after.refs_1_), custom_call_target="tpu_custom_call" | custom-call | tf_op jit(solution)/shard_map/fetch/pallas_call | solution.py:320
  50.2 0.1 collective-permute-done.3.part_1
  50.3 1.0 %collective-permute-done.4.part_2 = bf16[32,512]{1,0:T(8,128)(2,1)S(1)} collective-permute-done((bf16[32,512]{1,0:T(8,128)(2,1)}, bf16[32,512]{1,0:T(8,128)(2,1)S(1)}, u32[]{:S(2)}, u32[]{:S(2)}) %collective-permute-start.4) | collective-permute-done | bytes 32800 | tf_op jit(solution)/shard_map/ppermute | solution.py:557
  51.4 0.2 collective-permute-done.5.part_3
  51.6 4.4 %all-to-all-done.1 = bf16[128,4,2,128]{3,2,1,0:T(2,128)(2,1)S(1)} async-done(((bf16[128,4,2,128]{3,2,1,0:T(2,128)(2,1)}), bf16[128,4,2,128]{3,2,1,0:T(2,128)(2,1)S(1)}, u32[]{:S(2)}, u32[]{:S(2)}) %all-to-all-start.1) | async-done | bytes 262176 | tf_op jit(solution)/shard_map/all_to_all | solution.py:610
  56.0 0.9 %finish.1 = bf16[32,512]{1,0:T(8,128)(2,1)} custom-call(bf16[1024,128]{1,0:T(8,128)(2,1)S(1)} %bitcast.12, bf16[96,256]{1,0:T(8,128)(2,1)S(1)} %get-tuple-element.20.combine, f32[32,512]{1,0:T(8,128)S(1)} %get-tuple-element.21.base, bf16[32,512]{1,0:T(8,128)(2,1)S(1)} %collective-permute-done.3.part_1, bf16[32,512]{1,0:T(8,128)(2,1)S(1)} %collective-permute-done.4.part_2, ...), custom_call_target="tpu_custom_call" | custom-call | tf_op jit(solution)/shard_map/finish/pallas_call | solution.py:544
Async XLA Ops:
  9.9 24.4 %all-to-all-start = ((bf16[128,6,2,128]{3,2,1,0:T(2,128)(2,1)}), bf16[128,6,2,128]{3,2,1,0:T(2,128)(2,1)S(1)}, u32[]{:S(2)}, u32[]{:S(2)}) async-start(bf16[128,6,2,128]{3,2,1,0:T(2,128)(2,1)} %bitcast.13), calls=%async_computation | async-start | bytes 786432 | tf_op jit(solution)/shard_map/all_to_all | solution.py:596
  21.4 5.9 %collective-permute-start.2 = (bf16[32,256]{1,0:T(8,128)(2,1)}, bf16[32,256]{1,0:T(8,128)(2,1)S(1)}, u32[]{:S(2)}, u32[]{:S(2)}) collective-permute-start(bf16[32,256]{1,0:T(8,128)(2,1)} %get-tuple-element.16.after.own_heads), channel_id=1, source_target_pairs={{0,3},{1,0},{2,1},{3,2},{4,7},{5,4},{6,5},{7,6},{8,11},{9,8},{10,9... | collective-permute-start | bytes 49160 | tf_op jit(solution)/shard_map/ppermute | solution.py:557
  24.0 4.8 %collective-permute-start.1 = (bf16[32,256]{1,0:T(8,128)(2,1)}, bf16[32,256]{1,0:T(8,128)(2,1)S(1)}, u32[]{:S(2)}, u32[]{:S(2)}) collective-permute-start(bf16[32,256]{1,0:T(8,128)(2,1)} %get-tuple-element.16.after.own_heads), channel_id=1, source_target_pairs={{0,2},{1,3},{2,0},{3,1},{4,6},{5,7},{6,4},{7,5},{8,10},{9,11},{10,... | collective-permute-start | bytes 49160 | tf_op jit(solution)/shard_map/ppermute | solution.py:557
  24.6 4.5 %collective-permute-start = (bf16[32,256]{1,0:T(8,128)(2,1)}, bf16[32,256]{1,0:T(8,128)(2,1)S(1)}, u32[]{:S(2)}, u32[]{:S(2)}) collective-permute-start(bf16[32,256]{1,0:T(8,128)(2,1)} %get-tuple-element.16.after.own_heads), channel_id=1, source_target_pairs={{0,1},{1,2},{2,3},{3,0},{4,5},{5,6},{6,7},{7,4},{8,9},{9,10},{10,1... | collective-permute-start | bytes 49160 | tf_op jit(solution)/shard_map/ppermute | solution.py:557
  40.1 15.9 %all-to-all-start.1 = ((bf16[128,4,2,128]{3,2,1,0:T(2,128)(2,1)}), bf16[128,4,2,128]{3,2,1,0:T(2,128)(2,1)S(1)}, u32[]{:S(2)}, u32[]{:S(2)}) async-start(bf16[128,4,2,128]{3,2,1,0:T(2,128)(2,1)} %bitcast.14), calls=%async_computation.1 | async-start | bytes 524288 | tf_op jit(solution)/shard_map/all_to_all | solution.py:610
  44.3 6.0 %collective-permute-start.3 = (bf16[32,512]{1,0:T(8,128)(2,1)}, bf16[32,512]{1,0:T(8,128)(2,1)S(1)}, u32[]{:S(2)}, u32[]{:S(2)}) collective-permute-start(bf16[32,512]{1,0:T(8,128)(2,1)} %get-tuple-element.22), channel_id=1, source_target_pairs={{0,1},{1,2},{2,3},{3,0},{4,5},{5,6},{6,7},{7,4},{8,9},{9,10},{10,1... | collective-permute-start | bytes 98312 | tf_op jit(solution)/shard_map/ppermute | solution.py:557
  45.7 5.7 %collective-permute-start.4 = (bf16[32,512]{1,0:T(8,128)(2,1)}, bf16[32,512]{1,0:T(8,128)(2,1)S(1)}, u32[]{:S(2)}, u32[]{:S(2)}) collective-permute-start(bf16[32,512]{1,0:T(8,128)(2,1)} %get-tuple-element.23), channel_id=1, source_target_pairs={{0,2},{1,3},{2,0},{3,1},{4,6},{5,7},{6,4},{7,5},{8,10},{9,11},{10,... | collective-permute-start | bytes 98312 | tf_op jit(solution)/shard_map/ppermute | solution.py:557
  48.1 3.5 %collective-permute-start.5 = (bf16[32,512]{1,0:T(8,128)(2,1)}, bf16[32,512]{1,0:T(8,128)(2,1)S(1)}, u32[]{:S(2)}, u32[]{:S(2)}) collective-permute-start(bf16[32,512]{1,0:T(8,128)(2,1)} %get-tuple-element.24), channel_id=1, source_target_pairs={{0,3},{1,0},{2,1},{3,2},{4,7},{5,4},{6,5},{7,6},{8,11},{9,8},{10,9... | collective-permute-start | bytes 98312 | tf_op jit(solution)/shard_map/ppermute | solution.py:557

commit v5 on v4

--- a/solution.py
+++ b/solution.py
@@ -42,6 +42,7 @@
     spread,
     scores,
     turned,
+    values,
     mix,
     heads,
     combine,
@@ -53,7 +54,6 @@
 ):
     seqs, _ = tokens.shape
     cache_len = kv.shape[1]
-    place = (lax.axis_index("ep"), lax.axis_index("tp"))
     spans = cache_len // SPAN
     rows_all = seqs * 4
 
@@ -61,7 +61,6 @@
         part = pl.ds(i * SPAN, SPAN)
         return pltpu.make_async_copy(kv_hbm.at[:, part], kv.at[:, part], kv_sems.at[i])
 
-    base = pl.multiple_of((place[0] // 4) * 128, 128)
     loads = [
         pltpu.make_async_copy(src, dst, sems.at[i])
         for i, (src, dst) in enumerate(
@@ -71,8 +70,8 @@
                 (w_query_hbm, w_query),
                 (w_key_hbm, w_key),
                 (w_value_hbm, w_value),
+                (routing_hbm, routing),
                 (head_gain_hbm, head_gain),
-                (routing_hbm.at[:, pl.ds(base, 128)], routing),
                 (route_weights_hbm, route_weights),
                 (lengths_hbm, lengths),
                 (lambdas_hbm, lambdas),
@@ -83,14 +82,13 @@
         load.start()
     for i in range(spans):
         kv_copy(i).start()
-
     lane = lax.broadcasted_iota(jnp.int32, (1, 128), 1)
     loads[0].wait()
     loads[1].wait()
     wide = tokens[...].astype(jnp.float32)
     scale = lax.rsqrt(jnp.mean(wide * wide, axis=1, keepdims=True) + epsilon)
     normed = (wide * scale * gain[...]).astype(jnp.bfloat16)
-    for load in loads[2:]:
+    for load in loads[2:5]:
         load.wait()
 
     def rounded(value):
@@ -126,8 +124,12 @@
                 lane_seq == s, query_t[half][:64], 0.0
             ).astype(jnp.bfloat16)
 
+    for load in loads[5:]:
+        load.wait()
+    place = (lax.axis_index("ep"), lax.axis_index("tp"))
+    base = pl.multiple_of((place[0] // 4) * 128, 128)
     shift = 128 - (place[0] % 4) * 32
-    named = jnp.where(lane < seqs, pltpu.roll(routing[...], shift, 1), -1)
+    named = jnp.where(lane < seqs, pltpu.roll(routing[:, pl.ds(base, 128)], shift, 1), -1)
     at_row = lax.broadcasted_iota(jnp.int32, (128, 128), 0)
     at_column = lax.broadcasted_iota(jnp.int32, (128, 128), 1)
     named_at = [at_row == named[k : k + 1, :] for k in range(4)]
@@ -180,7 +182,13 @@
     for i in range(spans):
         kv_copy(i).wait()
         cut = slice(i * SPAN, (i + 1) * SPAN)
-        part = jnp.concatenate([kv[s, cut, :64] for s in range(seqs)], axis=1)
+        keys = []
+        for pair in range(seqs // 2):
+            one = kv[2 * pair, cut, :]
+            two = pltpu.roll(kv[2 * pair + 1, cut, :], 64, 1)
+            keys.append(jnp.where(lane < 64, one, two))
+            values[pair, cut, :] = jnp.where(lane < 64, two, one)
+        part = jnp.concatenate(keys, axis=1)
         found = jnp.dot(part, spread[...], preferred_element_type=jnp.float32) * scaling
         found = jnp.where(position < count - i * SPAN, found, neg_fill)
         scores[i * SPAN : (i + 1) * SPAN, :] = found
@@ -202,15 +210,18 @@
     weight_new = expo_new[:, :128] * first - expo_new[:, 128:] * second
     diagonal = jnp.where(at_row == at_column, weight_new, 0.0).astype(jnp.bfloat16)
     mix_new = jnp.dot(diagonal, fresh.astype(jnp.bfloat16), preferred_element_type=jnp.float32)
-    upper = lax.broadcasted_iota(jnp.int32, (8, 1), 0) < 4
-    for i in range(seqs // 2):
-        both = jnp.concatenate([kv[2 * i], kv[2 * i + 1]], axis=1)
-        out = jnp.dot(turned[8 * i : 8 * i + 8, :], both, preferred_element_type=jnp.float32)
-        mix[8 * i : 8 * i + 8, :] = jnp.where(upper, out[:, :128], out[:, 128:])
+    row16 = lax.broadcasted_iota(jnp.int32, (16, 1), 0)
+    for i in range(seqs // 4):
+        four = jnp.concatenate([values[2 * i], values[2 * i + 1]], axis=1)
+        out = jnp.dot(turned[16 * i : 16 * i + 16, :], four, preferred_element_type=jnp.float32)
+        left, right = out[:, :128], out[:, 128:]
+        upper = jnp.where(row16 < 4, left, pltpu.roll(left, 64, 1))
+        lower = jnp.where(row16 < 12, right, pltpu.roll(right, 64, 1))
+        mix[16 * i : 16 * i + 16, :] = jnp.where(row16 < 8, upper, lower)
 
     blend = mix[...] + mix_new
-    values = jnp.where(lane >= 64, blend, 0.0)
-    power = jnp.sum(values * values, axis=1, keepdims=True) * (1.0 / 64)
+    own = jnp.where(lane >= 64, blend, 0.0)
+    power = jnp.sum(own * own, axis=1, keepdims=True) * (1.0 / 64)
     gain2 = jnp.concatenate([head_gain[...], head_gain[...]], axis=1)
     mix[...] = blend * lax.rsqrt(power + epsilon) * gain2
     pieces = []
@@ -269,13 +280,14 @@
             pltpu.VMEM((64, width), bf16),
             pltpu.VMEM((64, width), bf16),
             pltpu.VMEM((1, 64), f32),
-            pltpu.VMEM((4, 128), jnp.int32),
+            pltpu.VMEM((4, routing.shape[0]), jnp.int32),
             pltpu.VMEM((4, seqs), f32),
             pltpu.VMEM((seqs * 8, 128), f32),
             pltpu.VMEM((seqs * 4, 128), f32),
             pltpu.VMEM((seqs * 64, 256), bf16),
             pltpu.VMEM((kv_cache.shape[1], 256), f32),
             pltpu.VMEM((128, kv_cache.shape[1]), bf16),
+            pltpu.VMEM((seqs // 2, kv_cache.shape[1], 128), bf16),
             pltpu.VMEM((seqs * 4, 128), f32),
             pltpu.VMEM((seqs, 256), bf16),
             pltpu.VMEM((3 * seqs, 256), bf16),
@@ -331,6 +343,7 @@
 def expert_kernel(
     rows,
     w_gate,
+    w_shared_gate,
     own_heads,
     heads_1,
     heads_2,
@@ -340,7 +353,6 @@
     w_out_hbm,
     w_up_hbm,
     w_down_hbm,
-    w_shared_gate_hbm,
     w_shared_up_hbm,
     w_shared_down_hbm,
     results,
@@ -361,7 +373,6 @@
     w_out,
     w_up,
     w_down,
-    w_shared_gate,
     w_shared_up,
     w_shared_down,
     sems,
@@ -370,21 +381,16 @@
 ):
     slots = 64
     quarters = [pl.ds(256 * t, 256) for t in range(4)]
-    tp = lax.axis_index("tp")
-    loads = [(w_out_hbm.at[quarter], w_out.at[quarter]) for quarter in quarters]
-    gathered = [(own_heads, heads.at[tp])]
-    for k, got in enumerate((heads_1, heads_2, heads_3)):
-        gathered.append((got, heads.at[(tp + 3 - k) % 4]))
     gathered = [
-        pltpu.make_async_copy(source, target, head_sems.at[i])
-        for i, (source, target) in enumerate(gathered)
+        pltpu.make_async_copy(got, heads.at[k], head_sems.at[k])
+        for k, got in enumerate((own_heads, heads_1, heads_2, heads_3))
     ]
     for load in gathered:
         load.start()
+    loads = [(w_out_hbm.at[quarter], w_out.at[quarter]) for quarter in quarters]
     loads += [(tokens_hbm, tokens), (ffn_gain_hbm, ffn_gain)]
     loads += [(w_up_hbm.at[0], w_up), (w_down_hbm.at[0], w_down)]
-    loads += [(w_shared_gate_hbm, w_shared_gate), (w_shared_up_hbm, w_shared_up)]
-    loads += [(w_shared_down_hbm, w_shared_down)]
+    loads += [(w_shared_up_hbm, w_shared_up), (w_shared_down_hbm, w_shared_down)]
     loads = [
         pltpu.make_async_copy(source, target, sems.at[i])
         for i, (source, target) in enumerate(loads)
@@ -402,10 +408,11 @@
 
     for load in gathered:
         load.wait()
+    tp = lax.axis_index("tp")
     total = None
     for t in range(4):
         arrived = jnp.concatenate([arrived_rows(t, 0), arrived_rows(t, 1)], axis=1)
-        both = jnp.concatenate([arrived, heads[t]], axis=0)
+        both = jnp.concatenate([arrived, heads[(tp + 4 - t) % 4]], axis=0)
         loads[t].wait()
         piece = jnp.dot(
             both, w_out[256 * t : 256 * t + 256, :], preferred_element_type=jnp.float32
@@ -443,9 +450,8 @@
         sends.append(pltpu.make_async_copy(ready.at[half], results.at[half], send_sems.at[i]))
         sends[i].start()
     loads[8].wait()
+    shared_act = gated(ffn_in[slots:], w_shared_gate[...], w_shared_up[...])
     loads[9].wait()
-    shared_act = gated(ffn_in[slots:], w_shared_gate[...], w_shared_up[...])
-    loads[10].wait()
     partial[...] = jnp.dot(shared_act, w_shared_down[...], preferred_element_type=jnp.float32)
 
     def share(source, shift):
@@ -463,8 +469,8 @@
         send.wait()
 
 
-def run_experts(rows, own_heads, got_heads, tokens, ffn_gain, w_gate, weights):
-    w_out, w_up, w_down, w_shared_gate, w_shared_up, w_shared_down = weights
+def run_experts(rows, own_heads, got_heads, tokens, ffn_gain, early, weights):
+    w_out, w_up, w_down, w_shared_up, w_shared_down = weights
     seqs, width = tokens.shape
     vmem = pl.BlockSpec(memory_space=pltpu.VMEM)
     bf16, f32 = jnp.bfloat16, jnp.float32
@@ -480,7 +486,7 @@
             part,
             part,
         ),
-        in_specs=[vmem] * 2 + [either] * 4 + [hbm] * 8,
+        in_specs=[vmem] * 3 + [either] * 4 + [hbm] * 7,
         out_specs=(hbm,) * 5,
         scratch_shapes=[
             pltpu.VMEM((4, seqs, 256), bf16),
@@ -496,10 +502,9 @@
             pltpu.VMEM(w_out.shape, bf16),
             pltpu.VMEM(w_up.shape[1:], bf16),
             pltpu.VMEM(w_down.shape[1:], bf16),
-            pltpu.VMEM(w_shared_gate.shape, bf16),
             pltpu.VMEM(w_shared_up.shape, bf16),
             pltpu.VMEM(w_shared_down.shape, bf16),
-            pltpu.SemaphoreType.DMA((11,)),
+            pltpu.SemaphoreType.DMA((10,)),
             pltpu.SemaphoreType.DMA((4,)),
             pltpu.SemaphoreType.DMA((6,)),
         ],
@@ -507,7 +512,7 @@
         name="run_experts",
     )(
         rows,
-        w_gate,
+        *early,
         *in_hbm(own_heads),
         *got_heads,
         *in_hbm(tokens, ffn_gain.reshape(1, -1), *weights),
@@ -595,7 +600,7 @@
     message = message.reshape(128, 6, 2, 128)
     arrived = lax.all_to_all(message, everyone, split_axis=0, concat_axis=0, tiled=True)
     got_heads = [around(heads, k) for k in range(1, 4)]
-    (gate,) = fetch(heads, (w_exp_gate,))
+    early = fetch(heads, (w_exp_gate, w_shared_gate))
     rows = arrived.reshape(1536, 128)
     results, base, *parts = run_experts(
         rows,
@@ -603,8 +608,8 @@
         got_heads,
         tokens,
         ffn_gain,
-        gate,
-        (w_out, w_exp_up, w_exp_down, w_shared_gate, w_shared_up, w_shared_down),
+        early,
+        (w_out, w_exp_up, w_exp_down, w_shared_up, w_shared_down),
     )
     results = results.reshape(128, 4, 2, 128)
     returned = lax.all_to_all(results, everyone, split_axis=0, concat_axis=0, tiled=True)

time: 57.1 us -> 54.8 us (0.960)
  Pallas kernels: 19.1 us -> 16.9 us
    pallas_call x1, Pallas kernels: 9.9 us -> 7.61 us  [attend(): pl.pallas_call(attend_kernel, out_shape=(pltpu.HBM((1536, 128), bf16), pl...]
  transfers between devices with their start and end apart: 8 -> 8, of which waited for: 8 -> 8; matrix products, arithmetic and copies ran while one was open for 0% -> 0% of each run, Pallas kernels for 4% -> 5%
where the time goes in v5:
time: 54.8 us; the launch traced here: 54.5 us
  starting transfers between devices  24.5 us (45%)
  Pallas kernels  16.9 us (31%)
  waiting for transfers between devices  13.1 us (24%)
    all_to_all x1, starting transfers between devices, shards(): lax.all_to_all(message, everyone, split_axis=0, concat_axis=0, tiled=True)  11.5 us
    ppermute x6, starting transfers between devices, around(): lax.ppermute(value, 'tp', [(i, (i + shift) % count) for i in range(count)])  8.78 us
    pallas_call x1, Pallas kernels, attend(): pl.pallas_call(attend_kernel, out_shape=(pltpu.HBM((1536, 128), bf16), pl...  7.61 us
    pallas_call x1, Pallas kernels, run_experts(): pl.pallas_call(expert_kernel, out_shape=(pltpu.HBM((1024, 128), bf16), pl...  5.8 us
    all_to_all x1, waiting for transfers between devices, shards(): lax.all_to_all(message, everyone, split_axis=0, concat_axis=0, tiled=True)  5.18 us
    all_to_all x1, waiting for transfers between devices, shards(): lax.all_to_all(results, everyone, split_axis=0, concat_axis=0, tiled=True)  4.38 us
    all_to_all x1, starting transfers between devices, shards(): lax.all_to_all(results, everyone, split_axis=0, concat_axis=0, tiled=True)  4.2 us
    ppermute x6, waiting for transfers between devices, around(): lax.ppermute(value, 'tp', [(i, (i + shift) % count) for i in range(count)])  3.58 us
  transfers between devices with their start and end apart: 8, of which 8 were waited for; matrix products, arithmetic and copies ran while one was open for 0% of the time, Pallas kernels for 5%

profile of v5, /device:TPU:1, one launch (start us, length us, event | category | flops | bytes accessed | tf_op | source)
XLA Modules:
  0.0 54.5 jit_solution(8422701974894438887)
XLA Ops:
  0.0 7.6 %attend.1 = (bf16[1536,128]{1,0:T(8,128)(2,1)}, bf16[32,256]{1,0:T(8,128)(2,1)}, bf16[96,256]{1,0:T(8,128)(2,1)}) custom-call(s32[32]{0:T(128)} %lengths_hbm.1, f32[4]{0:T(128)} %lambdas_hbm.1, bf16[32,2048]{1,0:T(8,128)(2,1)} %tokens_hbm.3, f32[1,2048]{1,0:T(1,128)} %bitcast.18, bf16[2048,256]{1,0:T(8,128)(2,1)} %w_query_hbm.1, bf16[64,2048]{1,0:T(8,128)(2,1)} %bitcast.15, ...), custom_call_target="tpu_custom_call" | custom-call | tf_op jit(solution)/shard_map/attend/pallas_call | solution.py:264
  7.6 11.5 %all-to-all-start = ((bf16[128,6,2,128]{3,2,1,0:T(2,128)(2,1)}), bf16[128,6,2,128]{3,2,1,0:T(2,128)(2,1)S(1)}, u32[]{:S(2)}, u32[]{:S(2)}) async-start(bf16[128,6,2,128]{3,2,1,0:T(2,128)(2,1)} %bitcast.13), calls=%async_computation | async-start | bytes 786432 | tf_op jit(solution)/shard_map/all_to_all | solution.py:601
  19.1 2.6 %collective-permute-start.2 = (bf16[32,256]{1,0:T(8,128)(2,1)}, bf16[32,256]{1,0:T(8,128)(2,1)S(1)}, u32[]{:S(2)}, u32[]{:S(2)}) collective-permute-start(bf16[32,256]{1,0:T(8,128)(2,1)} %get-tuple-element.18.after.own_heads), channel_id=1, source_target_pairs={{0,3},{1,0},{2,1},{3,2},{4,7},{5,4},{6,5},{7,6},{8,11},{9,8},{10,9... | collective-permute-start | bytes 49160 | tf_op jit(solution)/shard_map/ppermute | solution.py:562
  21.7 0.6 %collective-permute-start.1 = (bf16[32,256]{1,0:T(8,128)(2,1)}, bf16[32,256]{1,0:T(8,128)(2,1)S(1)}, u32[]{:S(2)}, u32[]{:S(2)}) collective-permute-start(bf16[32,256]{1,0:T(8,128)(2,1)} %get-tuple-element.18.after.own_heads), channel_id=1, source_target_pairs={{0,2},{1,3},{2,0},{3,1},{4,6},{5,7},{6,4},{7,5},{8,10},{9,11},{10,... | collective-permute-start | bytes 49160 | tf_op jit(solution)/shard_map/ppermute | solution.py:562
  22.3 0.6 %collective-permute-start = (bf16[32,256]{1,0:T(8,128)(2,1)}, bf16[32,256]{1,0:T(8,128)(2,1)S(1)}, u32[]{:S(2)}, u32[]{:S(2)}) collective-permute-start(bf16[32,256]{1,0:T(8,128)(2,1)} %get-tuple-element.18.after.own_heads), channel_id=1, source_target_pairs={{0,1},{1,2},{2,3},{3,0},{4,5},{5,6},{6,7},{7,4},{8,9},{9,10},{10,1... | collective-permute-start | bytes 49160 | tf_op jit(solution)/shard_map/ppermute | solution.py:562
  22.9 1.7 %fetch.2 = (bf16[1,2048,512]{2,1,0:T(8,128)(2,1)S(1)}, bf16[2048,128]{1,0:T(8,128)(2,1)S(1)}) custom-call(bf16[32,256]{1,0:T(8,128)(2,1)} %get-tuple-element.18.after.own_heads, bf16[1,2048,512]{2,1,0:T(8,128)(2,1)} %refs_0_.1, bf16[2048,128]{1,0:T(8,128)(2,1)} %refs_1_.1), custom_call_target="tpu_custom_call" | custom-call | tf_op jit(solution)/shard_map/fetch/pallas_call | solution.py:332
  24.6 0.4 collective-permute-done.2.heads_3
  25.0 1.5 %collective-permute-done.1.heads_2 = bf16[32,256]{1,0:T(8,128)(2,1)S(1)} collective-permute-done((bf16[32,256]{1,0:T(8,128)(2,1)}, bf16[32,256]{1,0:T(8,128)(2,1)S(1)}, u32[]{:S(2)}, u32[]{:S(2)}) %collective-permute-start.1) | collective-permute-done | bytes 16416 | tf_op jit(solution)/shard_map/ppermute | solution.py:562
  26.5 0.2 collective-permute-done.heads_1
  26.8 5.2 %all-to-all-done = bf16[128,6,2,128]{3,2,1,0:T(2,128)(2,1)S(1)} async-done(((bf16[128,6,2,128]{3,2,1,0:T(2,128)(2,1)}), bf16[128,6,2,128]{3,2,1,0:T(2,128)(2,1)S(1)}, u32[]{:S(2)}, u32[]{:S(2)}) %all-to-all-start) | async-done | bytes 393248 | tf_op jit(solution)/shard_map/all_to_all | solution.py:601
  32.0 5.8 %run_experts.1 = (bf16[1024,128]{1,0:T(8,128)(2,1)}, f32[32,512]{1,0:T(8,128)}, bf16[32,512]{1,0:T(8,128)(2,1)}, bf16[32,512]{1,0:T(8,128)(2,1)}, bf16[32,512]{1,0:T(8,128)(2,1)}) custom-call(bf16[1536,128]{1,0:T(8,128)(2,1)S(1)} %bitcast.11, bf16[1,2048,512]{2,1,0:T(8,128)(2,1)S(1)} %get-tuple-element.19.w_gate, ...), custom_call_target="tpu_custom_call" | custom-call | tf_op jit(solution)/shard_map/run_experts/pallas_call | solution.py:480
  37.8 4.2 %all-to-all-start.1 = ((bf16[128,4,2,128]{3,2,1,0:T(2,128)(2,1)}), bf16[128,4,2,128]{3,2,1,0:T(2,128)(2,1)S(1)}, u32[]{:S(2)}, u32[]{:S(2)}) async-start(bf16[128,4,2,128]{3,2,1,0:T(2,128)(2,1)} %bitcast.14), calls=%async_computation.1 | async-start | bytes 524288 | tf_op jit(solution)/shard_map/all_to_all | solution.py:615
  42.0 1.4 %collective-permute-start.3 = (bf16[32,512]{1,0:T(8,128)(2,1)}, bf16[32,512]{1,0:T(8,128)(2,1)S(1)}, u32[]{:S(2)}, u32[]{:S(2)}) collective-permute-start(bf16[32,512]{1,0:T(8,128)(2,1)} %get-tuple-element.26), channel_id=1, source_target_pairs={{0,1},{1,2},{2,3},{3,0},{4,5},{5,6},{6,7},{7,4},{8,9},{9,10},{10,1... | collective-permute-start | bytes 98312 | tf_op jit(solution)/shard_map/ppermute | solution.py:562
  43.4 2.4 %collective-permute-start.4 = (bf16[32,512]{1,0:T(8,128)(2,1)}, bf16[32,512]{1,0:T(8,128)(2,1)S(1)}, u32[]{:S(2)}, u32[]{:S(2)}) collective-permute-start(bf16[32,512]{1,0:T(8,128)(2,1)} %get-tuple-element.27), channel_id=1, source_target_pairs={{0,2},{1,3},{2,0},{3,1},{4,6},{5,7},{6,4},{7,5},{8,10},{9,11},{10,... | collective-permute-start | bytes 98312 | tf_op jit(solution)/shard_map/ppermute | solution.py:562
  45.8 1.2 %collective-permute-start.5 = (bf16[32,512]{1,0:T(8,128)(2,1)}, bf16[32,512]{1,0:T(8,128)(2,1)S(1)}, u32[]{:S(2)}, u32[]{:S(2)}) collective-permute-start(bf16[32,512]{1,0:T(8,128)(2,1)} %get-tuple-element.28), channel_id=1, source_target_pairs={{0,3},{1,0},{2,1},{3,2},{4,7},{5,4},{6,5},{7,6},{8,11},{9,8},{10,9... | collective-permute-start | bytes 98312 | tf_op jit(solution)/shard_map/ppermute | solution.py:562
  47.0 0.9 %fetch.3 = (bf16[96,256]{1,0:T(8,128)(2,1)S(1)}, f32[32,512]{1,0:T(8,128)S(1)}) custom-call(f32[32,512]{1,0:T(8,128)} %get-tuple-element.22.after.refs_1_, bf16[96,256]{1,0:T(8,128)(2,1)} %get-tuple-element.23.refs_0_, f32[32,512]{1,0:T(8,128)} %get-tuple-element.22.after.refs_1_), custom_call_target="tpu_custom_call" | custom-call | tf_op jit(solution)/shard_map/fetch/pallas_call | solution.py:332
  47.9 0.1 collective-permute-done.3.part_1
  48.0 1.0 %collective-permute-done.4.part_2 = bf16[32,512]{1,0:T(8,128)(2,1)S(1)} collective-permute-done((bf16[32,512]{1,0:T(8,128)(2,1)}, bf16[32,512]{1,0:T(8,128)(2,1)S(1)}, u32[]{:S(2)}, u32[]{:S(2)}) %collective-permute-start.4) | collective-permute-done | bytes 32800 | tf_op jit(solution)/shard_map/ppermute | solution.py:562
  49.1 0.2 collective-permute-done.5.part_3
  49.3 4.4 %all-to-all-done.1 = bf16[128,4,2,128]{3,2,1,0:T(2,128)(2,1)S(1)} async-done(((bf16[128,4,2,128]{3,2,1,0:T(2,128)(2,1)}), bf16[128,4,2,128]{3,2,1,0:T(2,128)(2,1)S(1)}, u32[]{:S(2)}, u32[]{:S(2)}) %all-to-all-start.1) | async-done | bytes 262176 | tf_op jit(solution)/shard_map/all_to_all | solution.py:615
  53.7 0.9 %finish.1 = bf16[32,512]{1,0:T(8,128)(2,1)} custom-call(bf16[1024,128]{1,0:T(8,128)(2,1)S(1)} %bitcast.12, bf16[96,256]{1,0:T(8,128)(2,1)S(1)} %get-tuple-element.24.combine, f32[32,512]{1,0:T(8,128)S(1)} %get-tuple-element.25.base, bf16[32,512]{1,0:T(8,128)(2,1)S(1)} %collective-permute-done.3.part_1, bf16[32,512]{1,0:T(8,128)(2,1)S(1)} %collective-permute-done.4.part_2, ...), custom_call_target="tpu_custom_call" | custom-call | tf_op jit(solution)/shard_map/finish/pallas_call | solution.py:549
Async XLA Ops:
  7.6 24.4 %all-to-all-start = ((bf16[128,6,2,128]{3,2,1,0:T(2,128)(2,1)}), bf16[128,6,2,128]{3,2,1,0:T(2,128)(2,1)S(1)}, u32[]{:S(2)}, u32[]{:S(2)}) async-start(bf16[128,6,2,128]{3,2,1,0:T(2,128)(2,1)} %bitcast.13), calls=%async_computation | async-start | bytes 786432 | tf_op jit(solution)/shard_map/all_to_all | solution.py:601
  19.1 5.9 %collective-permute-start.2 = (bf16[32,256]{1,0:T(8,128)(2,1)}, bf16[32,256]{1,0:T(8,128)(2,1)S(1)}, u32[]{:S(2)}, u32[]{:S(2)}) collective-permute-start(bf16[32,256]{1,0:T(8,128)(2,1)} %get-tuple-element.18.after.own_heads), channel_id=1, source_target_pairs={{0,3},{1,0},{2,1},{3,2},{4,7},{5,4},{6,5},{7,6},{8,11},{9,8},{10,9... | collective-permute-start | bytes 49160 | tf_op jit(solution)/shard_map/ppermute | solution.py:562
  21.7 4.8 %collective-permute-start.1 = (bf16[32,256]{1,0:T(8,128)(2,1)}, bf16[32,256]{1,0:T(8,128)(2,1)S(1)}, u32[]{:S(2)}, u32[]{:S(2)}) collective-permute-start(bf16[32,256]{1,0:T(8,128)(2,1)} %get-tuple-element.18.after.own_heads), channel_id=1, source_target_pairs={{0,2},{1,3},{2,0},{3,1},{4,6},{5,7},{6,4},{7,5},{8,10},{9,11},{10,... | collective-permute-start | bytes 49160 | tf_op jit(solution)/shard_map/ppermute | solution.py:562
  22.3 4.5 %collective-permute-start = (bf16[32,256]{1,0:T(8,128)(2,1)}, bf16[32,256]{1,0:T(8,128)(2,1)S(1)}, u32[]{:S(2)}, u32[]{:S(2)}) collective-permute-start(bf16[32,256]{1,0:T(8,128)(2,1)} %get-tuple-element.18.after.own_heads), channel_id=1, source_target_pairs={{0,1},{1,2},{2,3},{3,0},{4,5},{5,6},{6,7},{7,4},{8,9},{9,10},{10,1... | collective-permute-start | bytes 49160 | tf_op jit(solution)/shard_map/ppermute | solution.py:562
  37.8 15.9 %all-to-all-start.1 = ((bf16[128,4,2,128]{3,2,1,0:T(2,128)(2,1)}), bf16[128,4,2,128]{3,2,1,0:T(2,128)(2,1)S(1)}, u32[]{:S(2)}, u32[]{:S(2)}) async-start(bf16[128,4,2,128]{3,2,1,0:T(2,128)(2,1)} %bitcast.14), calls=%async_computation.1 | async-start | bytes 524288 | tf_op jit(solution)/shard_map/all_to_all | solution.py:615
  42.0 6.0 %collective-permute-start.3 = (bf16[32,512]{1,0:T(8,128)(2,1)}, bf16[32,512]{1,0:T(8,128)(2,1)S(1)}, u32[]{:S(2)}, u32[]{:S(2)}) collective-permute-start(bf16[32,512]{1,0:T(8,128)(2,1)} %get-tuple-element.26), channel_id=1, source_target_pairs={{0,1},{1,2},{2,3},{3,0},{4,5},{5,6},{6,7},{7,4},{8,9},{9,10},{10,1... | collective-permute-start | bytes 98312 | tf_op jit(solution)/shard_map/ppermute | solution.py:562
  43.4 5.7 %collective-permute-start.4 = (bf16[32,512]{1,0:T(8,128)(2,1)}, bf16[32,512]{1,0:T(8,128)(2,1)S(1)}, u32[]{:S(2)}, u32[]{:S(2)}) collective-permute-start(bf16[32,512]{1,0:T(8,128)(2,1)} %get-tuple-element.27), channel_id=1, source_target_pairs={{0,2},{1,3},{2,0},{3,1},{4,6},{5,7},{6,4},{7,5},{8,10},{9,11},{10,... | collective-permute-start | bytes 98312 | tf_op jit(solution)/shard_map/ppermute | solution.py:562
  45.8 3.5 %collective-permute-start.5 = (bf16[32,512]{1,0:T(8,128)(2,1)}, bf16[32,512]{1,0:T(8,128)(2,1)S(1)}, u32[]{:S(2)}, u32[]{:S(2)}) collective-permute-start(bf16[32,512]{1,0:T(8,128)(2,1)} %get-tuple-element.28), channel_id=1, source_target_pairs={{0,3},{1,0},{2,1},{3,2},{4,7},{5,4},{6,5},{7,6},{8,11},{9,8},{10,9... | collective-permute-start | bytes 98312 | tf_op jit(solution)/shard_map/ppermute | solution.py:562

commit v6 on v5

--- a/solution.py
+++ b/solution.py
@@ -343,7 +343,6 @@
 def expert_kernel(
     rows,
     w_gate,
-    w_shared_gate,
     own_heads,
     heads_1,
     heads_2,
@@ -353,6 +352,7 @@
     w_out_hbm,
     w_up_hbm,
     w_down_hbm,
+    w_shared_gate_hbm,
     w_shared_up_hbm,
     w_shared_down_hbm,
     results,
@@ -373,6 +373,7 @@
     w_out,
     w_up,
     w_down,
+    w_shared_gate,
     w_shared_up,
     w_shared_down,
     sems,
@@ -389,8 +390,9 @@
         load.start()
     loads = [(w_out_hbm.at[quarter], w_out.at[quarter]) for quarter in quarters]
     loads += [(tokens_hbm, tokens), (ffn_gain_hbm, ffn_gain)]
+    loads += [(w_shared_gate_hbm, w_shared_gate), (w_shared_up_hbm, w_shared_up)]
     loads += [(w_up_hbm.at[0], w_up), (w_down_hbm.at[0], w_down)]
-    loads += [(w_shared_up_hbm, w_shared_up), (w_shared_down_hbm, w_shared_down)]
+    loads += [(w_shared_down_hbm, w_shared_down)]
     loads = [
         pltpu.make_async_copy(source, target, sems.at[i])
         for i, (source, target) in enumerate(loads)
@@ -435,8 +437,11 @@
         return (gate_part / (1.0 + jnp.exp(-gate_part)) * up_part).astype(jnp.bfloat16)
 
     loads[6].wait()
+    loads[7].wait()
+    shared_act = gated(ffn_in[slots:], w_shared_gate[...], w_shared_up[...])
+    loads[8].wait()
     act = gated(ffn_in[:slots], w_gate[0], w_up[...])
-    loads[7].wait()
+    loads[9].wait()
     result = jnp.dot(act, w_down[...], preferred_element_type=jnp.float32)
     for b in range(16):
         for c in range(2):
@@ -449,9 +454,7 @@
         ready[half, :] = stage[half, :].astype(jnp.bfloat16)
         sends.append(pltpu.make_async_copy(ready.at[half], results.at[half], send_sems.at[i]))
         sends[i].start()
-    loads[8].wait()
-    shared_act = gated(ffn_in[slots:], w_shared_gate[...], w_shared_up[...])
-    loads[9].wait()
+    loads[10].wait()
     partial[...] = jnp.dot(shared_act, w_shared_down[...], preferred_element_type=jnp.float32)
 
     def share(source, shift):
@@ -469,8 +472,8 @@
         send.wait()
 
 
-def run_experts(rows, own_heads, got_heads, tokens, ffn_gain, early, weights):
-    w_out, w_up, w_down, w_shared_up, w_shared_down = weights
+def run_experts(rows, own_heads, got_heads, tokens, ffn_gain, w_gate, weights):
+    w_out, w_up, w_down, w_shared_gate, w_shared_up, w_shared_down = weights
     seqs, width = tokens.shape
     vmem = pl.BlockSpec(memory_space=pltpu.VMEM)
     bf16, f32 = jnp.bfloat16, jnp.float32
@@ -486,7 +489,7 @@
             part,
             part,
         ),
-        in_specs=[vmem] * 3 + [either] * 4 + [hbm] * 7,
+        in_specs=[vmem] * 2 + [either] * 4 + [hbm] * 8,
         out_specs=(hbm,) * 5,
         scratch_shapes=[
             pltpu.VMEM((4, seqs, 256), bf16),
@@ -502,9 +505,10 @@
             pltpu.VMEM(w_out.shape, bf16),
             pltpu.VMEM(w_up.shape[1:], bf16),
             pltpu.VMEM(w_down.shape[1:], bf16),
+            pltpu.VMEM(w_shared_gate.shape, bf16),
             pltpu.VMEM(w_shared_up.shape, bf16),
             pltpu.VMEM(w_shared_down.shape, bf16),
-            pltpu.SemaphoreType.DMA((10,)),
+            pltpu.SemaphoreType.DMA((11,)),
             pltpu.SemaphoreType.DMA((4,)),
             pltpu.SemaphoreType.DMA((6,)),
         ],
@@ -512,7 +516,7 @@
         name="run_experts",
     )(
         rows,
-        *early,
+        w_gate,
         *in_hbm(own_heads),
         *got_heads,
         *in_hbm(tokens, ffn_gain.reshape(1, -1), *weights),
@@ -600,7 +604,7 @@
     message = message.reshape(128, 6, 2, 128)
     arrived = lax.all_to_all(message, everyone, split_axis=0, concat_axis=0, tiled=True)
     got_heads = [around(heads, k) for k in range(1, 4)]
-    early = fetch(heads, (w_exp_gate, w_shared_gate))
+    (gate,) = fetch(heads, (w_exp_gate,))
     rows = arrived.reshape(1536, 128)
     results, base, *parts = run_experts(
         rows,
@@ -608,8 +612,8 @@
         got_heads,
         tokens,
         ffn_gain,
-        early,
-        (w_out, w_exp_up, w_exp_down, w_shared_up, w_shared_down),
+        gate,
+        (w_out, w_exp_up, w_exp_down, w_shared_gate, w_shared_up, w_shared_down),
     )
     results = results.reshape(128, 4, 2, 128)
     returned = lax.all_to_all(results, everyone, split_axis=0, concat_axis=0, tiled=True)

time: 54.8 us -> 54.8 us (level)
  no operation moved by 1% of the time
where the time goes in v6:
time: 54.8 us; the launch traced here: 54.6 us
  starting transfers between devices  24.5 us (45%)
  Pallas kernels  16.8 us (31%)
  waiting for transfers between devices  13.2 us (24%)
    all_to_all x1, starting transfers between devices, shards(): lax.all_to_all(message, everyone, split_axis=0, concat_axis=0, tiled=True)  11.5 us
    ppermute x6, starting transfers between devices, around(): lax.ppermute(value, 'tp', [(i, (i + shift) % count) for i in range(count)])  8.78 us
    pallas_call x1, Pallas kernels, attend(): pl.pallas_call(attend_kernel, out_shape=(pltpu.HBM((1536, 128), bf16), pl...  7.61 us
    pallas_call x1, Pallas kernels, run_experts(): pl.pallas_call(expert_kernel, out_shape=(pltpu.HBM((1024, 128), bf16), pl...  5.83 us
    all_to_all x1, waiting for transfers between devices, shards(): lax.all_to_all(message, everyone, split_axis=0, concat_axis=0, tiled=True)  5.18 us
    all_to_all x1, waiting for transfers between devices, shards(): lax.all_to_all(results, everyone, split_axis=0, concat_axis=0, tiled=True)  4.38 us
    all_to_all x1, starting transfers between devices, shards(): lax.all_to_all(results, everyone, split_axis=0, concat_axis=0, tiled=True)  4.2 us
    ppermute x6, waiting for transfers between devices, around(): lax.ppermute(value, 'tp', [(i, (i + shift) % count) for i in range(count)])  3.67 us
  transfers between devices with their start and end apart: 8, of which 8 were waited for; matrix products, arithmetic and copies ran while one was open for 0% of the time, Pallas kernels for 5%

profile of v6, /device:TPU:1, one launch (start us, length us, event | category | flops | bytes accessed | tf_op | source)
XLA Modules:
  0.0 54.6 jit_solution(6401730077813006610)
XLA Ops:
  0.0 7.6 %attend.1 = (bf16[1536,128]{1,0:T(8,128)(2,1)}, bf16[32,256]{1,0:T(8,128)(2,1)}, bf16[96,256]{1,0:T(8,128)(2,1)}) custom-call(s32[32]{0:T(128)} %lengths_hbm.1, f32[4]{0:T(128)} %lambdas_hbm.1, bf16[32,2048]{1,0:T(8,128)(2,1)} %tokens_hbm.3, f32[1,2048]{1,0:T(1,128)} %bitcast.18, bf16[2048,256]{1,0:T(8,128)(2,1)} %w_query_hbm.1, bf16[64,2048]{1,0:T(8,128)(2,1)} %bitcast.15, ...), custom_call_target="tpu_custom_call" | custom-call | tf_op jit(solution)/shard_map/attend/pallas_call | solution.py:264
  7.6 11.5 %all-to-all-start = ((bf16[128,6,2,128]{3,2,1,0:T(2,128)(2,1)}), bf16[128,6,2,128]{3,2,1,0:T(2,128)(2,1)S(1)}, u32[]{:S(2)}, u32[]{:S(2)}) async-start(bf16[128,6,2,128]{3,2,1,0:T(2,128)(2,1)} %bitcast.13), calls=%async_computation | async-start | bytes 786432 | tf_op jit(solution)/shard_map/all_to_all | solution.py:605
  19.1 2.6 %collective-permute-start.2 = (bf16[32,256]{1,0:T(8,128)(2,1)}, bf16[32,256]{1,0:T(8,128)(2,1)S(1)}, u32[]{:S(2)}, u32[]{:S(2)}) collective-permute-start(bf16[32,256]{1,0:T(8,128)(2,1)} %get-tuple-element.16.after.own_heads), channel_id=1, source_target_pairs={{0,3},{1,0},{2,1},{3,2},{4,7},{5,4},{6,5},{7,6},{8,11},{9,8},{10,9... | collective-permute-start | bytes 49160 | tf_op jit(solution)/shard_map/ppermute | solution.py:566
  21.7 0.6 %collective-permute-start.1 = (bf16[32,256]{1,0:T(8,128)(2,1)}, bf16[32,256]{1,0:T(8,128)(2,1)S(1)}, u32[]{:S(2)}, u32[]{:S(2)}) collective-permute-start(bf16[32,256]{1,0:T(8,128)(2,1)} %get-tuple-element.16.after.own_heads), channel_id=1, source_target_pairs={{0,2},{1,3},{2,0},{3,1},{4,6},{5,7},{6,4},{7,5},{8,10},{9,11},{10,... | collective-permute-start | bytes 49160 | tf_op jit(solution)/shard_map/ppermute | solution.py:566
  22.3 0.6 %collective-permute-start = (bf16[32,256]{1,0:T(8,128)(2,1)}, bf16[32,256]{1,0:T(8,128)(2,1)S(1)}, u32[]{:S(2)}, u32[]{:S(2)}) collective-permute-start(bf16[32,256]{1,0:T(8,128)(2,1)} %get-tuple-element.16.after.own_heads), channel_id=1, source_target_pairs={{0,1},{1,2},{2,3},{3,0},{4,5},{5,6},{6,7},{7,4},{8,9},{9,10},{10,1... | collective-permute-start | bytes 49160 | tf_op jit(solution)/shard_map/ppermute | solution.py:566
  22.9 1.6 %fetch.2.w_gate = bf16[1,2048,512]{2,1,0:T(8,128)(2,1)S(1)} custom-call(bf16[32,256]{1,0:T(8,128)(2,1)} %get-tuple-element.16.after.own_heads, bf16[1,2048,512]{2,1,0:T(8,128)(2,1)} %refs_0_.1), custom_call_target="tpu_custom_call" | custom-call | tf_op jit(solution)/shard_map/fetch/pallas_call | solution.py:332
  24.5 0.5 collective-permute-done.2.heads_3
  25.0 1.5 %collective-permute-done.1.heads_2 = bf16[32,256]{1,0:T(8,128)(2,1)S(1)} collective-permute-done((bf16[32,256]{1,0:T(8,128)(2,1)}, bf16[32,256]{1,0:T(8,128)(2,1)S(1)}, u32[]{:S(2)}, u32[]{:S(2)}) %collective-permute-start.1) | collective-permute-done | bytes 16416 | tf_op jit(solution)/shard_map/ppermute | solution.py:566
  26.5 0.2 collective-permute-done.heads_1
  26.8 5.2 %all-to-all-done = bf16[128,6,2,128]{3,2,1,0:T(2,128)(2,1)S(1)} async-done(((bf16[128,6,2,128]{3,2,1,0:T(2,128)(2,1)}), bf16[128,6,2,128]{3,2,1,0:T(2,128)(2,1)S(1)}, u32[]{:S(2)}, u32[]{:S(2)}) %all-to-all-start) | async-done | bytes 393248 | tf_op jit(solution)/shard_map/all_to_all | solution.py:605
  32.0 5.8 %run_experts.1 = (bf16[1024,128]{1,0:T(8,128)(2,1)}, f32[32,512]{1,0:T(8,128)}, bf16[32,512]{1,0:T(8,128)(2,1)}, bf16[32,512]{1,0:T(8,128)(2,1)}, bf16[32,512]{1,0:T(8,128)(2,1)}) custom-call(bf16[1536,128]{1,0:T(8,128)(2,1)S(1)} %bitcast.11, bf16[1,2048,512]{2,1,0:T(8,128)(2,1)S(1)} %fetch.2.w_gate, bf16[32,256]{1,0:T(8,128)(2,1)} %get-tuple-element.16.after.own_heads, ...), custom_call_target="tpu_custom_call" | custom-call | tf_op jit(solution)/shard_map/run_experts/pallas_call | solution.py:483
  37.8 4.2 %all-to-all-start.1 = ((bf16[128,4,2,128]{3,2,1,0:T(2,128)(2,1)}), bf16[128,4,2,128]{3,2,1,0:T(2,128)(2,1)S(1)}, u32[]{:S(2)}, u32[]{:S(2)}) async-start(bf16[128,4,2,128]{3,2,1,0:T(2,128)(2,1)} %bitcast.14), calls=%async_computation.1 | async-start | bytes 524288 | tf_op jit(solution)/shard_map/all_to_all | solution.py:619
  42.0 1.4 %collective-permute-start.3 = (bf16[32,512]{1,0:T(8,128)(2,1)}, bf16[32,512]{1,0:T(8,128)(2,1)S(1)}, u32[]{:S(2)}, u32[]{:S(2)}) collective-permute-start(bf16[32,512]{1,0:T(8,128)(2,1)} %get-tuple-element.22), channel_id=1, source_target_pairs={{0,1},{1,2},{2,3},{3,0},{4,5},{5,6},{6,7},{7,4},{8,9},{9,10},{10,1... | collective-permute-start | bytes 98312 | tf_op jit(solution)/shard_map/ppermute | solution.py:566
  43.4 2.4 %collective-permute-start.4 = (bf16[32,512]{1,0:T(8,128)(2,1)}, bf16[32,512]{1,0:T(8,128)(2,1)S(1)}, u32[]{:S(2)}, u32[]{:S(2)}) collective-permute-start(bf16[32,512]{1,0:T(8,128)(2,1)} %get-tuple-element.23), channel_id=1, source_target_pairs={{0,2},{1,3},{2,0},{3,1},{4,6},{5,7},{6,4},{7,5},{8,10},{9,11},{10,... | collective-permute-start | bytes 98312 | tf_op jit(solution)/shard_map/ppermute | solution.py:566
  45.8 1.2 %collective-permute-start.5 = (bf16[32,512]{1,0:T(8,128)(2,1)}, bf16[32,512]{1,0:T(8,128)(2,1)S(1)}, u32[]{:S(2)}, u32[]{:S(2)}) collective-permute-start(bf16[32,512]{1,0:T(8,128)(2,1)} %get-tuple-element.24), channel_id=1, source_target_pairs={{0,3},{1,0},{2,1},{3,2},{4,7},{5,4},{6,5},{7,6},{8,11},{9,8},{10,9... | collective-permute-start | bytes 98312 | tf_op jit(solution)/shard_map/ppermute | solution.py:566
  47.0 0.9 %fetch.3 = (bf16[96,256]{1,0:T(8,128)(2,1)S(1)}, f32[32,512]{1,0:T(8,128)S(1)}) custom-call(f32[32,512]{1,0:T(8,128)} %get-tuple-element.18.after.refs_1_, bf16[96,256]{1,0:T(8,128)(2,1)} %get-tuple-element.19.refs_0_, f32[32,512]{1,0:T(8,128)} %get-tuple-element.18.after.refs_1_), custom_call_target="tpu_custom_call" | custom-call | tf_op jit(solution)/shard_map/fetch/pallas_call | solution.py:332
  47.9 0.1 collective-permute-done.3.part_1
  48.0 1.0 %collective-permute-done.4.part_2 = bf16[32,512]{1,0:T(8,128)(2,1)S(1)} collective-permute-done((bf16[32,512]{1,0:T(8,128)(2,1)}, bf16[32,512]{1,0:T(8,128)(2,1)S(1)}, u32[]{:S(2)}, u32[]{:S(2)}) %collective-permute-start.4) | collective-permute-done | bytes 32800 | tf_op jit(solution)/shard_map/ppermute | solution.py:566
  49.1 0.2 collective-permute-done.5.part_3
  49.3 4.4 %all-to-all-done.1 = bf16[128,4,2,128]{3,2,1,0:T(2,128)(2,1)S(1)} async-done(((bf16[128,4,2,128]{3,2,1,0:T(2,128)(2,1)}), bf16[128,4,2,128]{3,2,1,0:T(2,128)(2,1)S(1)}, u32[]{:S(2)}, u32[]{:S(2)}) %all-to-all-start.1) | async-done | bytes 262176 | tf_op jit(solution)/shard_map/all_to_all | solution.py:619
  53.7 0.9 %finish.1 = bf16[32,512]{1,0:T(8,128)(2,1)} custom-call(bf16[1024,128]{1,0:T(8,128)(2,1)S(1)} %bitcast.12, bf16[96,256]{1,0:T(8,128)(2,1)S(1)} %get-tuple-element.20.combine, f32[32,512]{1,0:T(8,128)S(1)} %get-tuple-element.21.base, bf16[32,512]{1,0:T(8,128)(2,1)S(1)} %collective-permute-done.3.part_1, bf16[32,512]{1,0:T(8,128)(2,1)S(1)} %collective-permute-done.4.part_2, ...), custom_call_target="tpu_custom_call" | custom-call | tf_op jit(solution)/shard_map/finish/pallas_call | solution.py:553
Async XLA Ops:
  7.6 24.4 %all-to-all-start = ((bf16[128,6,2,128]{3,2,1,0:T(2,128)(2,1)}), bf16[128,6,2,128]{3,2,1,0:T(2,128)(2,1)S(1)}, u32[]{:S(2)}, u32[]{:S(2)}) async-start(bf16[128,6,2,128]{3,2,1,0:T(2,128)(2,1)} %bitcast.13), calls=%async_computation | async-start | bytes 786432 | tf_op jit(solution)/shard_map/all_to_all | solution.py:605
  19.1 5.9 %collective-permute-start.2 = (bf16[32,256]{1,0:T(8,128)(2,1)}, bf16[32,256]{1,0:T(8,128)(2,1)S(1)}, u32[]{:S(2)}, u32[]{:S(2)}) collective-permute-start(bf16[32,256]{1,0:T(8,128)(2,1)} %get-tuple-element.16.after.own_heads), channel_id=1, source_target_pairs={{0,3},{1,0},{2,1},{3,2},{4,7},{5,4},{6,5},{7,6},{8,11},{9,8},{10,9... | collective-permute-start | bytes 49160 | tf_op jit(solution)/shard_map/ppermute | solution.py:566
  21.7 4.8 %collective-permute-start.1 = (bf16[32,256]{1,0:T(8,128)(2,1)}, bf16[32,256]{1,0:T(8,128)(2,1)S(1)}, u32[]{:S(2)}, u32[]{:S(2)}) collective-permute-start(bf16[32,256]{1,0:T(8,128)(2,1)} %get-tuple-element.16.after.own_heads), channel_id=1, source_target_pairs={{0,2},{1,3},{2,0},{3,1},{4,6},{5,7},{6,4},{7,5},{8,10},{9,11},{10,... | collective-permute-start | bytes 49160 | tf_op jit(solution)/shard_map/ppermute | solution.py:566
  22.3 4.5 %collective-permute-start = (bf16[32,256]{1,0:T(8,128)(2,1)}, bf16[32,256]{1,0:T(8,128)(2,1)S(1)}, u32[]{:S(2)}, u32[]{:S(2)}) collective-permute-start(bf16[32,256]{1,0:T(8,128)(2,1)} %get-tuple-element.16.after.own_heads), channel_id=1, source_target_pairs={{0,1},{1,2},{2,3},{3,0},{4,5},{5,6},{6,7},{7,4},{8,9},{9,10},{10,1... | collective-permute-start | bytes 49160 | tf_op jit(solution)/shard_map/ppermute | solution.py:566
  37.8 15.9 %all-to-all-start.1 = ((bf16[128,4,2,128]{3,2,1,0:T(2,128)(2,1)}), bf16[128,4,2,128]{3,2,1,0:T(2,128)(2,1)S(1)}, u32[]{:S(2)}, u32[]{:S(2)}) async-start(bf16[128,4,2,128]{3,2,1,0:T(2,128)(2,1)} %bitcast.14), calls=%async_computation.1 | async-start | bytes 524288 | tf_op jit(solution)/shard_map/all_to_all | solution.py:619
  42.0 6.0 %collective-permute-start.3 = (bf16[32,512]{1,0:T(8,128)(2,1)}, bf16[32,512]{1,0:T(8,128)(2,1)S(1)}, u32[]{:S(2)}, u32[]{:S(2)}) collective-permute-start(bf16[32,512]{1,0:T(8,128)(2,1)} %get-tuple-element.22), channel_id=1, source_target_pairs={{0,1},{1,2},{2,3},{3,0},{4,5},{5,6},{6,7},{7,4},{8,9},{9,10},{10,1... | collective-permute-start | bytes 98312 | tf_op jit(solution)/shard_map/ppermute | solution.py:566
  43.4 5.7 %collective-permute-start.4 = (bf16[32,512]{1,0:T(8,128)(2,1)}, bf16[32,512]{1,0:T(8,128)(2,1)S(1)}, u32[]{:S(2)}, u32[]{:S(2)}) collective-permute-start(bf16[32,512]{1,0:T(8,128)(2,1)} %get-tuple-element.23), channel_id=1, source_target_pairs={{0,2},{1,3},{2,0},{3,1},{4,6},{5,7},{6,4},{7,5},{8,10},{9,11},{10,... | collective-permute-start | bytes 98312 | tf_op jit(solution)/shard_map/ppermute | solution.py:566
  45.8 3.5 %collective-permute-start.5 = (bf16[32,512]{1,0:T(8,128)(2,1)}, bf16[32,512]{1,0:T(8,128)(2,1)S(1)}, u32[]{:S(2)}, u32[]{:S(2)}) collective-permute-start(bf16[32,512]{1,0:T(8,128)(2,1)} %get-tuple-element.24), channel_id=1, source_target_pairs={{0,3},{1,0},{2,1},{3,2},{4,7},{5,4},{6,5},{7,6},{8,11},{9,8},{10,9... | collective-permute-start | bytes 98312 | tf_op jit(solution)/shard_map/ppermute | solution.py:566
